TPU v7x, 32 devices: a whole 2x2x4 slice. The times are simulated.
32 devices in a mesh: sp: 8 (over z, x), tp: 4 (over y, core).
Axes of the slice: x: 2, y: 2, z: 4, core: 2. Of those that a mesh axis runs over, the one named last changes fastest.
Arguments:
- tokens: bfloat16 [1024, 2048], P(('sp', 'tp')), may hold values from -6 to 6
- conv_input: bfloat16 [2048, 512], P(None, 'tp'), may hold values from -0.125 to 0.125
- conv_gate: bfloat16 [2048, 512], P(None, 'tp'), may hold values from -0.125 to 0.125
- query_weight: bfloat16 [2048, 1024], P(None, 'tp'), may hold values from -0.125 to 0.125
- key_weight: bfloat16 [2048, 512], P(None, 'tp'), may hold values from -0.125 to 0.125
- value_weight: bfloat16 [2048, 512], P(None, 'tp'), may hold values from -0.125 to 0.125
- conv_taps: float32 [31, 512], P(None, 'tp'), may hold values from -4.5 to 4.5
- conv_gain: float32 [512], P('tp'), may hold values from 0.1 to 1.9
- key_offsets: bfloat16 [1024, 8], P('sp', 'tp'), may hold values from -16 to 2
- stick_gain: float32 [1024], P('tp'), may hold values from 0.1 to 1.9
- conv_output: bfloat16 [512, 2048], P('tp'), may hold values from -0.15625 to 0.15625
- stick_output: bfloat16 [1024, 2048], P('tp'), may hold values from -0.15625 to 0.15625
Outputs:
- mixed: bfloat16 [1024, 2048], P(('sp', 'tp'))
All inputs are finite; a program needn't handle non-finite values.
Results may differ from a plain program's by a relative error of at most 0.013.
Values may be sent and summed in bfloat16 or wider, within the bound.
No kernel may reach another device: no remote copies, remote signals or barrier semaphores. Data moves between devices by JAX's collectives and lax.ppermute only.
A program may use at most 64 MiB of HBM per device.

v0:
```python
import jax
import jax.numpy as jnp
from jax import lax
from jax.sharding import PartitionSpec as P

HEAD_DIM = 128


norm_eps = 1e-05


def from_behind(value, axis, by):
    count = lax.axis_size(axis)
    pairs = [(i, i + by) for i in range(count) if 0 <= i + by < count]
    return lax.ppermute(value, axis, pairs)


def span_of(shard_count, tok_rows):
    widest = max(1, min(1024 // tok_rows, 8, shard_count // 4))
    chosen = 1
    for divisor in range(1, shard_count + 1):
        if shard_count % divisor == 0 and divisor <= widest:
            chosen = divisor
    return chosen


def stick_logs(queries, key_rows, offset_list, first_key, first_query):
    key_count = key_rows.shape[0]
    kv_local = queries.shape[1]
    per_group = queries.shape[2]
    scores = jnp.einsum("tkgd,skd->kgts", queries, key_rows, preferred_element_type=jnp.float32)
    scores = scores * queries.shape[3] ** (-0.5)
    shifts = jnp.transpose(
        offset_list.astype(jnp.float32).reshape(key_count, kv_local, per_group), (1, 2, 0)
    )
    scores = scores + shifts[:, :, None, :]
    key_pos = first_key + lax.iota(jnp.int32, key_count)
    query_pos = first_query + lax.iota(jnp.int32, queries.shape[0])
    allowed = key_pos[None, :] < query_pos[:, None]
    log_keep = jnp.where(allowed, jax.nn.log_sigmoid(-scores), 0.0)
    return (scores, allowed, log_keep)


def shards(
    tokens,
    conv_input,
    conv_gate,
    query_weight,
    key_weight,
    value_weight,
    conv_taps,
    conv_gain,
    key_offsets,
    stick_gain,
    conv_output,
    stick_output,
):
    matrices = (conv_input, conv_gate, query_weight, key_weight, value_weight)
    row_piece = lax.all_gather(tokens, "tp", axis=0, tiled=True)
    projected = jnp.concatenate(
        [
            jnp.dot(row_piece, matrix, preferred_element_type=jnp.float32).astype(jnp.bfloat16)
            for matrix in matrices
        ],
        axis=1,
    )
    tok_rows = projected.shape[0]
    channels = conv_input.shape[1]
    query_cols = query_weight.shape[1]
    kv_cols = key_weight.shape[1]
    conv_values = projected[:, :channels]
    conv_gates = projected[:, channels : 2 * channels]
    blended = (
        conv_values.astype(jnp.float32) * jax.nn.sigmoid(conv_gates.astype(jnp.float32))
    ).astype(jnp.bfloat16)
    reach_rows = conv_taps.shape[0] - 1
    earlier = from_behind(blended[tok_rows - reach_rows :], "sp", 1)
    widened = jnp.concatenate([earlier, blended], axis=0).astype(jnp.float32)
    conv_field = conv_taps[0] * widened[0:tok_rows]
    for tap_index in range(1, reach_rows + 1):
        conv_field = conv_field + conv_taps[tap_index] * widened[tap_index : tap_index + tok_rows]
    all_channels = channels * lax.axis_size("tp")
    channel_sum, channel_squares = lax.psum(
        (jnp.sum(conv_field, axis=1), jnp.sum(conv_field * conv_field, axis=1)), "tp"
    )
    center = channel_sum / all_channels
    spread = channel_squares / all_channels - center * center
    normalized = (conv_field - center[:, None]) * lax.rsqrt(spread[:, None] + norm_eps) * conv_gain
    conv_mix = jax.nn.silu(normalized).astype(jnp.bfloat16)
    kv_local = kv_cols // HEAD_DIM
    per_group = query_cols // kv_cols
    begin_query = 2 * channels
    begin_key = begin_query + query_cols
    begin_value = begin_key + kv_cols
    queries = projected[:, begin_query:begin_key].reshape(tok_rows, kv_local, per_group, HEAD_DIM)
    key_rows = projected[:, begin_key:begin_value].reshape(tok_rows, kv_local, HEAD_DIM)
    value_rows = projected[:, begin_value : begin_value + kv_cols].reshape(
        tok_rows, kv_local, HEAD_DIM
    )
    first_query = lax.axis_index("sp") * tok_rows
    empty_output = jnp.zeros((kv_local, per_group, tok_rows, HEAD_DIM), jnp.float32)
    all_keys, all_offsets, all_values = (
        lax.all_gather(key_rows, "sp", axis=0, tiled=True),
        lax.all_gather(key_offsets, "sp", axis=0, tiled=True),
        lax.all_gather(value_rows, "sp", axis=0, tiled=True),
    )
    span_count = span_of(lax.axis_size("sp"), tok_rows)
    length = span_count * tok_rows
    own_group = lax.axis_index("sp") // span_count

    def walk_back(turn_no, carried):
        output, log_carry = carried
        begin_row = (own_group - turn_no) * length
        key_slice = lax.dynamic_slice_in_dim(all_keys, begin_row, length, 0)
        offset_slice = lax.dynamic_slice_in_dim(all_offsets, begin_row, length, 0)
        value_slice = lax.dynamic_slice_in_dim(all_values, begin_row, length, 0)
        scores, allowed, log_keep = stick_logs(
            queries, key_slice, offset_slice, begin_row, first_query
        )
        after = lax.cumsum(log_keep, axis=3, reverse=True) - log_keep
        weights = jnp.where(
            allowed, jnp.exp(jax.nn.log_sigmoid(scores) + after + log_carry), 0.0
        ).astype(jnp.bfloat16)
        output = output + jnp.einsum(
            "kgts,skd->kgtd", weights, value_slice, preferred_element_type=jnp.float32
        )
        log_carry = log_carry + jnp.sum(log_keep, axis=3, keepdims=True)
        return (output, log_carry)

    start_carry = jnp.zeros((kv_local, per_group, tok_rows, 1), jnp.float32)
    attended, final_carry = lax.fori_loop(0, own_group + 1, walk_back, (empty_output, start_carry))
    mean_square = jnp.mean(attended * attended, axis=3, keepdims=True)
    normed = attended * lax.rsqrt(mean_square + norm_eps)
    stick_mix = (
        jnp.transpose(normed, (2, 0, 1, 3)).reshape(tok_rows, query_cols) * stick_gain
    ).astype(jnp.bfloat16)
    return lax.psum_scatter(
        (
            jnp.dot(conv_mix, conv_output, preferred_element_type=jnp.float32)
            + jnp.dot(stick_mix, stick_output, preferred_element_type=jnp.float32)
        ).astype(jnp.bfloat16),
        "tp",
        scatter_dimension=0,
        tiled=True,
    )


def solution(mesh):
    return jax.shard_map(
        shards,
        mesh=mesh,
        in_specs=(
            P(("sp", "tp"), None),
            P(None, "tp"),
            P(None, "tp"),
            P(None, "tp"),
            P(None, "tp"),
            P(None, "tp"),
            P(None, "tp"),
            P("tp"),
            P("sp", "tp"),
            P("tp"),
            P("tp", None),
            P("tp", None),
        ),
        out_specs=P(("sp", "tp"), None),
        check_vma=False,
    )
```

profile of v0, /device:TPU:0, one launch (start us, length us, event | category | flops | bytes accessed | tf_op | source)
XLA Modules:
  0.0 152.0 jit_solution(14879834095888591023)
XLA Ops:
  6.5 9.0 %all_gather.12 = bf16[128,2048]{1,0:T(8,128)(2,1)S(1)} all-gather(bf16[32,2048]{1,0:T(8,128)(2,1)} %param.14), channel_id=1, replica_groups=mesh['sp'=8,'tp'=4] {'tp'}, dimensions={0}, use_global_device_ids=true | all-gather | bytes 655360 | tf_op jit(solution)/shard_map/all_gather | solution.py:59
  15.6 0.3 fusion.31
  15.8 0.8 copy-done.4
  16.6 0.3 fusion.30
  16.9 3.4 %collective-permute-start = (bf16[30,128]{1,0:T(8,128)(2,1)S(1)}, bf16[30,128]{1,0:T(8,128)(2,1)S(1)}, u32[]{:S(2)}, u32[]{:S(2)}) collective-permute-start(bf16[30,128]{1,0:T(8,128)(2,1)S(1)} %slice.260), channel_id=1, source_target_pairs={{0,4},{4,8},{8,12},{12,16},{16,20},{20,24},{24,28},{1,5},{5,9},{9,... | collective-permute-start | bytes 23048 | tf_op jit(solution)/shard_map/ppermute | solution.py:15
  20.4 18.8 %all_gather.14 = bf16[1024,2]{0,1:T(2,128)(2,1)S(1)} all-gather(bf16[128,2]{0,1:T(2,128)(2,1)S(1)} %copy-done.10), channel_id=1, replica_groups=mesh['sp'=8,'tp'=4] {'sp'}, dimensions={0}, use_global_device_ids=true | all-gather | bytes 4608 | tf_op jit(solution)/shard_map/all_gather | solution.py:104
  39.2 0.3 convolution_convert_fusion.1
  39.5 0.3 convolution_convert_fusion.2
  39.8 0.6 copy-done.1
  40.4 0.3 convolution_convert_fusion
  40.8 30.7 %all-gather = bf16[1024,128]{1,0:T(8,128)(2,1)S(1)} all-gather(bf16[128,128]{1,0:T(8,128)(2,1)S(1)} %convolution_convert_fusion.2), channel_id=2, replica_groups=mesh['sp'=8,'tp'=4] {'sp'}, dimensions={0}, use_global_device_ids=true | all-gather | bytes 294912 | tf_op jit(solution)/shard_map/all_gather | solution.py:103
  71.5 30.7 %all-gather.1 = bf16[1024,128]{1,0:T(8,128)(2,1)S(1)} all-gather(bf16[128,128]{1,0:T(8,128)(2,1)S(1)} %convolution_convert_fusion.1), channel_id=3, replica_groups=mesh['sp'=8,'tp'=4] {'sp'}, dimensions={0}, use_global_device_ids=true | all-gather | bytes 294912 | tf_op jit(solution)/shard_map/all_gather | solution.py:105
  102.3 3.6 %while.12 = (s32[]{:T(128)}, f32[1,2,128,128]{3,2,1,0:T(8,128)S(1)}, f32[1,2,128,1]{2,1,3,0:T(2,128)S(1)}, s32[]{:T(128)}, s32[]{:T(128)}, /*index=5*/s32[]{:T(1...) while((s32[]{:T(128)}, ...), condition=%wide.region_8.9_spmd, body=%wide.region_4.8_spmd.sunk | while | flops 44107400 | bytes 2945255 | solution.py:131
  102.5 0.4 fusion.94
  102.8 2.3 %fusion.95 = f32[1,2,128,2,128]{2,3,4,1,0:T(2,128)S(1)} fusion(f32[1,2,128,2,128]{2,4,3,1,0:T(8,128)S(1)} %bitcast.162), kind=kOutput, calls=%fused_computation.17.clone.1 | output fusion | flops 8323072 | bytes 524288 | tf_op jit(solution)/shard_map/reduce-window
  105.2 0.4 fusion.96
  106.1 0.6 copy-done.7
  106.8 0.6 copy-done.8
  107.5 0.3 fusion.70
  107.9 0.3 fusion.68
  108.2 5.7 %all-reduce = (f32[128]{0:T(128)S(1)}, f32[128]{0:T(128)S(1)}) all-reduce(f32[128]{0:T(128)S(1)} %get-tuple-element.80, f32[128]{0:T(128)S(1)} %get-tuple-element.79), channel_id=1, replica_groups=mesh['sp'=8,'tp'=4] {'tp'}, use_global_device_ids=true, to_apply=%region_3.0 | all-reduce | flops 256 | bytes 2048 | tf_op jit(solution)/shard_map/psum | solution.py:83
  113.9 0.7 copy-done.9
  114.5 1.1 fusion.23
  115.7 29.4 %reduce-scatter.2.cloned.1.call-done = bf16[32,2048]{1,0:T(8,128)(2,1)} async-done(((bf16[128,2048]{1,0:T(8,128)(2,1)}), bf16[32,2048]{1,0:T(8,128)(2,1)}) %reduce-scatter.2.cloned.1.call-update) | async-done | bytes 131088 | tf_op jit(solution)/shard_map/reduce_scatter | solution.py:137
  (44 shorter events, 0.9 us)
Async XLA Ops:
  6.5 101.0 %copy-start = (bf16[256,2048]{1,0:T(8,128)(2,1)S(1)}, bf16[256,2048]{1,0:T(8,128)(2,1)}, u32[]{:S(2)}) copy-start(bf16[256,2048]{1,0:T(8,128)(2,1)} %param.25) | copy-start | bytes 3145732
  6.5 9.0 %copy-start.3 = (bf16[2048,128]{1,0:T(8,128)(2,1)S(1)}, bf16[2048,128]{1,0:T(8,128)(2,1)}, u32[]{:S(2)}) copy-start(bf16[2048,128]{1,0:T(8,128)(2,1)} %param.15) | copy-start | bytes 1572868
  6.5 138.6 %reduce-scatter.2.cloned.1.call-start = ((), (), s32[]{:S(2)}) async-start(), calls=%async_computation.1 | async-start | bytes 655360 | tf_op jit(solution)/shard_map/reduce_scatter | solution.py:137
  15.5 1.0 copy-start.4
  16.6 3.8 %copy-start.10 = (bf16[128,2]{0,1:T(2,128)(2,1)S(1)}, bf16[128,2]{0,1:T(2,128)(2,1)}, u32[]{:S(2)}) copy-start(bf16[128,2]{0,1:T(2,128)(2,1)} %param.22) | copy-start | bytes 1540
  16.6 22.6 %copy-start.5 = (bf16[2048,128]{1,0:T(8,128)(2,1)S(1)}, bf16[2048,128]{1,0:T(8,128)(2,1)}, u32[]{:S(2)}) copy-start(bf16[2048,128]{1,0:T(8,128)(2,1)} %param.19) | copy-start | bytes 1572868
  16.9 91.0 %collective-permute-start = (bf16[30,128]{1,0:T(8,128)(2,1)S(1)}, bf16[30,128]{1,0:T(8,128)(2,1)S(1)}, u32[]{:S(2)}, u32[]{:S(2)}) collective-permute-start(bf16[30,128]{1,0:T(8,128)(2,1)S(1)} %slice.260), channel_id=1, source_target_pairs={{0,4},{4,8},{8,12},{12,16},{16,20},{20,24},{24,28},{1,5},{5,9},{9,... | collective-permute-start | bytes 23048 | tf_op jit(solution)/shard_map/ppermute | solution.py:15
  20.3 19.2 %copy-start.6 = (bf16[2048,128]{1,0:T(8,128)(2,1)S(1)}, bf16[2048,128]{1,0:T(8,128)(2,1)}, u32[]{:S(2)}) copy-start(bf16[2048,128]{1,0:T(8,128)(2,1)} %param.18) | copy-start | bytes 1572868
  39.2 1.2 copy-start.1
  106.0 0.7 copy-start.7
  106.7 0.7 copy-start.8
  107.9 6.0 %copy-start.2 = (bf16[128,2048]{1,0:T(8,128)(2,1)S(1)}, bf16[128,2048]{1,0:T(8,128)(2,1)}, u32[]{:S(2)}) copy-start(bf16[128,2048]{1,0:T(8,128)(2,1)} %param.24) | copy-start | bytes 1572868
  113.9 0.7 copy-start.9
Sparse Core Ops, SparseCore 0:
  115.8 29.2 reduce-scatter.1
where the time goes:
time: 152 us
  blocking collectives  95 us (62%)
  waiting for transfers between devices  29.4 us (19%)
  between operations  13.6 us (9%)
  matrix products  3.57 us (2%)
  local copies, waits for them, and re-layouts  3.52 us (2%)
  starting transfers between devices  3.4 us (2%)
  other arithmetic  3.39 us (2%)
    all_gather x1, blocking collectives, shards(): lax.all_gather(key_rows, 'sp', axis=0, tiled=True)  30.7 us
    all_gather x1, blocking collectives, shards(): lax.all_gather(value_rows, 'sp', axis=0, tiled=True)  30.7 us
    reduce_scatter x1, waiting for transfers between devices, shards(): lax.psum_scatter((jnp.dot(conv_mix, conv_output, preferred_element_type=j...  29.4 us
    all_gather x1, blocking collectives, shards(): lax.all_gather(key_offsets, 'sp', axis=0, tiled=True)  18.8 us
    all_gather x1, blocking collectives, shards(): row_piece = lax.all_gather(tokens, 'tp', axis=0, tiled=True)  9 us
    psum x1, blocking collectives, shards(): lax.psum((jnp.sum(conv_field, axis=1), jnp.sum(conv_field * conv_field, a...  5.66 us
    ppermute x1, starting transfers between devices, from_behind(): return lax.ppermute(value, axis, pairs)  3.39 us
    unnamed x22, local copies, waits for them, and re-layouts  3.33 us
  transfers between devices with their start and end apart: 2, of which 1 were waited for; matrix products, arithmetic and copies ran while one was open for 3% of the time, Pallas kernels for 0%

commit v1 on v0

v1 whole, which is shorter than its diff:
```python
import functools

import jax
import jax.numpy as jnp
from jax import lax
from jax.experimental import pallas as pl
from jax.experimental.pallas import tpu as pltpu
from jax.sharding import PartitionSpec as P

HEAD_DIM = 128
norm_eps = 1e-05
f32 = jnp.float32
bf16 = jnp.bfloat16


def swap(value, axis, by):
    count = lax.axis_size(axis)
    return lax.ppermute(value, axis, [(i, i ^ by) for i in range(count)])


def from_behind(value, axis, by):
    count = lax.axis_size(axis)
    pairs = [(i, i + by) for i in range(count) if 0 <= i + by < count]
    return lax.ppermute(value, axis, pairs)


def dot(a, b):
    return jnp.dot(a, b, preferred_element_type=f32)


def project_kernel(*refs, pieces):
    toks = refs[:pieces]
    w_in, w_gate, w_q, w_k, w_v, off, pay, qs, blend, tail, x_all = refs[pieces:]
    rows = toks[0].shape[0]
    me = lax.axis_index("tp")
    for k in range(pieces):
        x_all[pl.ds(pl.multiple_of((me ^ k) * rows, rows), rows), :] = toks[k][...]
    x = x_all[...]
    n = x.shape[0]
    kv = w_k.shape[1]
    pay[0:n, 0:kv] = dot(x, w_k[...]).astype(bf16)
    pay[0:n, kv : 2 * kv] = dot(x, w_v[...]).astype(bf16)
    pay[n:, 0:kv] = off[...]
    pay[n:, kv : 2 * kv] = jnp.zeros_like(off)
    q = dot(x, w_q[...]).astype(bf16)
    for h in range(q.shape[1] // HEAD_DIM):
        qs[h * n : (h + 1) * n, :] = q[:, h * HEAD_DIM : (h + 1) * HEAD_DIM]
    values = dot(x, w_in[...]).astype(bf16).astype(f32)
    gates = dot(x, w_gate[...]).astype(bf16).astype(f32)
    b = (values * jax.nn.sigmoid(gates)).astype(bf16)
    blend[...] = b
    tail[...] = b[n - tail.shape[0] :, :]


def conv_kernel(halo, blend, taps, field, stats, wide):
    n = blend.shape[0]
    h = halo.shape[0]
    reach = taps.shape[0] - 1
    wide[0:h, :] = halo[...].astype(f32)
    wide[h : h + n, :] = blend[...].astype(f32)
    base = h - reach
    f = taps[0:1, :] * wide[base : base + n, :]
    for t in range(1, reach + 1):
        f = f + taps[t : t + 1, :] * wide[base + t : base + t + n, :]
    field[...] = f
    ch = f.shape[1]
    mean = jnp.sum(f, axis=1, keepdims=True) / ch
    d = f - mean
    m2 = jnp.sum(d * d, axis=1, keepdims=True)
    stats[0:1, :] = jnp.transpose(jnp.broadcast_to(mean, (n, 128)))[0:1, :]
    stats[1:2, :] = jnp.transpose(jnp.broadcast_to(m2, (n, 128)))[0:1, :]


def block_part(q, pay, gap, n, per, tri):
    kv = HEAD_DIM
    keys = pay[0:n, 0:kv]
    vals = pay[0:n, kv : 2 * kv]
    off = pay[n : n + 8, 0:kv].astype(f32)
    s = lax.dot_general(q, keys, (((1,), (1,)), ((), ())), preferred_element_type=f32)
    s = s * (HEAD_DIM ** (-0.5))
    shift = jnp.concatenate(
        [jnp.broadcast_to(off[h : h + 1, :], (n, n)) for h in range(per)], axis=0
    )
    s = s + shift
    row = lax.broadcasted_iota(jnp.int32, s.shape, 0) & (n - 1)
    col = lax.broadcasted_iota(jnp.int32, s.shape, 1)
    allowed = col < row + gap
    soft = jnp.log1p(jnp.exp(-jnp.abs(s)))
    take = jnp.minimum(s, 0.0) - soft
    keep = jnp.where(allowed, jnp.minimum(-s, 0.0) - soft, 0.0)
    hi = keep.astype(bf16)
    lo = (keep - hi.astype(f32)).astype(bf16)
    sums = dot(hi, tri) + dot(lo, tri)
    w = jnp.where(allowed, jnp.exp(take + sums[:, 0:n]), 0.0).astype(bf16)
    return dot(w, vals), sums[:, n : 2 * n]


def tri_of(n):
    r = lax.broadcasted_iota(jnp.int32, (n, 2 * n), 0)
    c = lax.broadcasted_iota(jnp.int32, (n, 2 * n), 1)
    return jnp.where((r > c) | (c >= n), 1.0, 0.0).astype(bf16)


def finish(att, field, stats, c_gain, s_gain, w_c, w_s, mine, other, send, mix, n, per, members):
    ch = field.shape[1]
    mean = sum(st[0:1, :] for st in stats) / members
    m2 = sum(st[1:2, :] for st in stats)
    m2 = m2 + ch * sum((st[0:1, :] - mean) ** 2 for st in stats)
    rstd = lax.rsqrt(m2 / (ch * members) + norm_eps)
    mean_c = jnp.transpose(jnp.broadcast_to(mean, (ch, n)))
    rstd_c = jnp.transpose(jnp.broadcast_to(rstd, (ch, n)))
    z = (field[...] - mean_c) * rstd_c * c_gain[...]
    mix[:, 0:ch] = (z * jax.nn.sigmoid(z)).astype(bf16)
    ms = jnp.mean(att * att, axis=1, keepdims=True)
    normed = att * lax.rsqrt(ms + norm_eps)
    for h in range(per):
        part = normed[h * n : (h + 1) * n, :] * s_gain[h : h + 1, :]
        mix[:, ch + h * HEAD_DIM : ch + (h + 1) * HEAD_DIM] = part.astype(bf16)
    me = lax.axis_index("tp")
    rows = n // members
    lhs = jnp.concatenate(
        [mix[pl.ds(pl.multiple_of((me ^ k) * rows, rows), rows), :] for k in (0, 2, 1, 3)], axis=0
    )
    out = dot(lhs[:, 0:ch], w_c[...]) + dot(lhs[:, ch:], w_s[...])
    mine[...] = out[0:rows, :]
    other[...] = out[rows : 2 * rows, :]
    send[...] = out[2 * rows :, :].astype(bf16)


def attend_kernel(*refs, blocks, members, n, per):
    q_ref = refs[0]
    pays = refs[1 : 1 + blocks]
    field = refs[1 + blocks]
    stats = refs[2 + blocks : 2 + blocks + members]
    c_gain, s_gain, w_c, w_s, mine, other, send, mix, parts, totals = refs[2 + blocks + members :]
    me = lax.axis_index("sp")
    q = q_ref[...]
    tri = tri_of(n)
    for k in range(blocks):
        j = me ^ k
        part, total = block_part(q, pays[k], (me - j) * n, n, per, tri)
        parts[pl.ds(j, 1)] = part[None]
        totals[pl.ds(j, 1)] = total[None]
    att = parts[blocks - 1]
    carry = totals[blocks - 1]
    for j in range(blocks - 2, -1, -1):
        att = att + jnp.exp(carry) * parts[j]
        if j:
            carry = carry + totals[j]
    finish(att, field, stats, c_gain, s_gain, w_c, w_s, mine, other, send, mix, n, per, members)


def attend_loop_kernel(*refs, members, n, per):
    q_ref, pays, field = refs[:3]
    stats = refs[3 : 3 + members]
    c_gain, s_gain, w_c, w_s, mine, other, send, mix = refs[3 + members :]
    me = lax.axis_index("sp")
    q = q_ref[...]
    tri = tri_of(n)

    def step(turn, carried):
        att, carry = carried
        j = me - turn
        part, total = block_part(q, pays.at[j], turn * n, n, per, tri)
        return att + jnp.exp(carry) * part, carry + total

    zero = jnp.zeros((per * n, HEAD_DIM), f32)
    att, _ = lax.fori_loop(0, me + 1, step, (zero, zero))
    finish(att, field, stats, c_gain, s_gain, w_c, w_s, mine, other, send, mix, n, per, members)


def call(body, outs, *args, scratch=(), flops=0):
    spec = pl.BlockSpec(memory_space=pltpu.VMEM)
    return pl.pallas_call(
        body,
        out_shape=outs,
        in_specs=[spec] * len(args),
        out_specs=[spec] * len(outs),
        scratch_shapes=scratch,
        cost_estimate=pl.CostEstimate(flops=flops, transcendentals=0, bytes_accessed=0),
    )(*args)


def shards(
    tokens,
    conv_input,
    conv_gate,
    query_weight,
    key_weight,
    value_weight,
    conv_taps,
    conv_gain,
    key_offsets,
    stick_gain,
    conv_output,
    stick_output,
):
    members = lax.axis_size("tp")
    blocks = lax.axis_size("sp")
    rows, width = tokens.shape
    n = rows * members
    ch = conv_input.shape[1]
    kv = key_weight.shape[1]
    per = query_weight.shape[1] // kv
    off = jnp.pad(jnp.transpose(key_offsets), ((0, 8 - per), (0, 0)))
    by_core = swap(tokens, "tp", 1)
    by_chip = swap(tokens, "tp", 2)
    by_both = swap(by_chip, "tp", 1)
    pay, qs, blend, tail = call(
        functools.partial(project_kernel, pieces=4),
        [
            jax.ShapeDtypeStruct((n + 8, 2 * kv), bf16),
            jax.ShapeDtypeStruct((per * n, HEAD_DIM), bf16),
            jax.ShapeDtypeStruct((n, ch), bf16),
            jax.ShapeDtypeStruct((32, ch), bf16),
        ],
        tokens, by_core, by_chip, by_both,
        conv_input, conv_gate, query_weight, key_weight, value_weight, off,
        scratch=[pltpu.VMEM((n, width), bf16)],
        flops=2 * n * width * (2 * ch + 4 * kv),
    )
    halo = from_behind(tail, "sp", 1)
    if blocks == 8:
        z6 = swap(pay, "sp", 6)
        z4 = swap(pay, "sp", 4)
        z2 = swap(pay, "sp", 2)
        x1 = swap(pay, "sp", 1)
        pays = [pay, x1, z2, swap(z2, "sp", 1), z4, swap(z4, "sp", 1), z6, swap(z6, "sp", 1)]
    else:
        pays = [lax.all_gather(pay, "sp", axis=0)]
    field, stats = call(
        conv_kernel,
        [jax.ShapeDtypeStruct((n, ch), f32), jax.ShapeDtypeStruct((8, n), f32)],
        halo, blend, conv_taps,
        scratch=[pltpu.VMEM((n + 32, ch), f32)],
        flops=64 * n * ch,
    )
    stats_chip = swap(stats, "tp", 2)
    all_stats = [stats, swap(stats, "tp", 1), stats_chip, swap(stats_chip, "tp", 1)]
    scratch = [pltpu.VMEM((n, ch + per * HEAD_DIM), bf16)]
    if blocks == 8:
        body = functools.partial(attend_kernel, blocks=blocks, members=members, n=n, per=per)
        scratch += [pltpu.VMEM((blocks, per * n, HEAD_DIM), f32)] * 2
    else:
        body = functools.partial(attend_loop_kernel, members=members, n=n, per=per)
    mine, other, send = call(
        body,
        [
            jax.ShapeDtypeStruct((rows, width), f32),
            jax.ShapeDtypeStruct((rows, width), f32),
            jax.ShapeDtypeStruct((2 * rows, width), bf16),
        ],
        qs, *pays, field, *all_stats,
        conv_gain.reshape(1, ch), stick_gain.reshape(per, HEAD_DIM), conv_output, stick_output,
        scratch=scratch,
        flops=2 * n * width * (ch + per * HEAD_DIM),
    )
    got = swap(send, "tp", 1).astype(f32)
    chip = swap((other + got[rows:]).astype(bf16), "tp", 2)
    return (mine + got[:rows] + chip.astype(f32)).astype(bf16)


def solution(mesh):
    return jax.shard_map(
        shards,
        mesh=mesh,
        in_specs=(
            P(("sp", "tp"), None),
            P(None, "tp"),
            P(None, "tp"),
            P(None, "tp"),
            P(None, "tp"),
            P(None, "tp"),
            P(None, "tp"),
            P("tp"),
            P("sp", "tp"),
            P("tp"),
            P("tp", None),
            P("tp", None),
        ),
        out_specs=P(("sp", "tp"), None),
        check_vma=False,
    )
```

time: 152 us -> 54.4 us (0.36)
  blocking collectives: 95 us -> 0 us
  starting transfers between devices: 3.4 us -> 19.5 us
  between operations: 13.6 us -> 0.15 us
  Pallas kernels: 0 us -> 12.2 us
  waiting for transfers between devices: 29.4 us -> 19.1 us
  matrix products: 3.57 us -> 0 us
  other arithmetic: 3.39 us -> 0.76 us
    all_gather x4 -> x0, blocking collectives: 89.3 us -> none  [the longest x1 30.7 us: shards(): lax.all_gather(key_rows, 'sp', axis=0, tiled=True)]
    reduce_scatter x1 -> x0, waiting for transfers between devices: 29.4 us -> none  [shards(): lax.psum_scatter((jnp.dot(conv_mix, conv_output, preferred_element_type=j...]
    ppermute x0 -> x15, waiting for transfers between devices: none -> 17.5 us  [swap(): return lax.ppermute(value, axis, [(i, i ^ by) for i in range(count)])]
    ppermute x0 -> x15, starting transfers between devices: none -> 16.1 us  [swap(): return lax.ppermute(value, axis, [(i, i ^ by) for i in range(count)])]
    pallas_call x0 -> x3, Pallas kernels: none -> 12.2 us  [call(): pl.pallas_call(body, out_shape=outs, in_specs=[spec] * len(args), out_spe...]
    psum x1 -> x0, blocking collectives: 5.66 us -> none  [shards(): lax.psum((jnp.sum(conv_field, axis=1), jnp.sum(conv_field * conv_field, a...]
    dot_general x9 -> x0, matrix products: 3.57 us -> none  [the longest x5 1.48 us: shards(): jnp.dot(row_piece, matrix, preferred_element_type=jnp.float32)]
    another operation x2 -> x0, other arithmetic: 2.33 us -> none
  transfers between devices with their start and end apart: 2 -> 16, of which waited for: 1 -> 10; matrix products, arithmetic and copies ran while one was open for 3% -> 1% of each run, Pallas kernels for 0% -> 3%
where the time goes in v1:
time: 54.4 us; the launch traced here: 54.2 us
  starting transfers between devices  19.5 us (36%)
  waiting for transfers between devices  19.1 us (35%)
  Pallas kernels  12.2 us (22%)
  local copies, waits for them, and re-layouts  2.48 us (5%)
  other arithmetic  0.76 us (1%)
    ppermute x15, waiting for transfers between devices, swap(): return lax.ppermute(value, axis, [(i, i ^ by) for i in range(count)])  17.5 us
    ppermute x15, starting transfers between devices, swap(): return lax.ppermute(value, axis, [(i, i ^ by) for i in range(count)])  16.1 us
    pallas_call x3, Pallas kernels, call(): pl.pallas_call(body, out_shape=outs, in_specs=[spec] * len(args), out_spe...  12.2 us
    ppermute x1, starting transfers between devices, from_behind(): return lax.ppermute(value, axis, pairs)  3.38 us
    unnamed x34, local copies, waits for them, and re-layouts  1.87 us
    ppermute x1, waiting for transfers between devices, from_behind(): return lax.ppermute(value, axis, pairs)  1.56 us
  transfers between devices with their start and end apart: 16, of which 10 were waited for; matrix products, arithmetic and copies ran while one was open for 1% of the time, Pallas kernels for 3%

profile of v1, /device:TPU:0, one launch (start us, length us, event | category | flops | bytes accessed | tf_op | source)
XLA Modules:
  0.0 54.2 jit_solution(16297191222354707864)
XLA Ops:
  0.0 3.0 %collective-permute-start.1 = (bf16[32,2048]{1,0:T(8,128)(2,1)}, bf16[32,2048]{1,0:T(8,128)(2,1)S(1)}, u32[]{:S(2)}, u32[]{:S(2)}) collective-permute-start(bf16[32,2048]{1,0:T(8,128)(2,1)} %refs_0_.1), channel_id=1, source_target_pairs={{0,2},{1,3},{2,0},{3,1},{4,6},{5,7},{6,4},{7,5},{8,10},{9,11},{10,... | collective-permute-start | bytes 393224 | tf_op jit(solution)/shard_map/ppermute | solution.py:18
  3.0 3.7 %collective-permute-done.1.refs_2_ = bf16[32,2048]{1,0:T(8,128)(2,1)S(1)} collective-permute-done((bf16[32,2048]{1,0:T(8,128)(2,1)}, bf16[32,2048]{1,0:T(8,128)(2,1)S(1)}, u32[]{:S(2)}, u32[]{:S(2)}) %collective-permute-start.1) | collective-permute-done | bytes 131104 | tf_op jit(solution)/shard_map/ppermute | solution.py:18
  7.3 0.7 %collective-permute-done.2.refs_3_ = bf16[32,2048]{1,0:T(8,128)(2,1)S(1)} collective-permute-done((bf16[32,2048]{1,0:T(8,128)(2,1)S(1)}, bf16[32,2048]{1,0:T(8,128)(2,1)S(1)}, u32[]{:S(2)}, u32[]{:S(2)}) %collective-permute-start.2) | collective-permute-done | bytes 131104 | tf_op jit(solution)/shard_map/ppermute | solution.py:18
  8.1 0.6 %copy-done.4 = bf16[32,2048]{1,0:T(8,128)(2,1)} copy-done((bf16[32,2048]{1,0:T(8,128)(2,1)}, bf16[32,2048]{1,0:T(8,128)(2,1)S(1)}, u32[]{:S(2)}) %copy-start.4) | copy-done | bytes 131096
  8.7 3.5 %shard_map.118 = (bf16[136,256]{1,0:T(8,128)(2,1)}, bf16[256,128]{1,0:T(8,128)(2,1)}, bf16[128,128]{1,0:T(8,128)(2,1)}, bf16[32,128]{1,0:T(8,128)(2,1)}) custom-call(bf16[32,2048]{1,0:T(8,128)(2,1)} %refs_0_.1, bf16[32,2048]{1,0:T(8,128)(2,1)} %copy-done.3, bf16[32,2048]{1,0:T(8,128)(2,1)} %copy-done.2, bf16[32,2048]{1,0:T(8,128)(2,1)} %copy-done.4, ...), custom_call_target="tpu_custom_call" | custom-call | flops 402653184 | tf_op jit(solution)/shard_map/pallas_call | solution.py:174
  12.2 3.8 %collective-permute-start.8 = (bf16[136,256]{1,0:T(8,128)(2,1)}, bf16[136,256]{1,0:T(8,128)(2,1)S(1)}, u32[]{:S(2)}, u32[]{:S(2)}) collective-permute-start(bf16[136,256]{1,0:T(8,128)(2,1)} %get-tuple-element.15.refs_1_), channel_id=1, source_target_pairs={{0,24},{4,28},{8,16},{12,20},{16,8},{20,12},{24,0},{28,4},{1,25},{... | collective-permute-start | bytes 208904 | tf_op jit(solution)/shard_map/ppermute | solution.py:18
  16.1 0.6 %collective-permute-start.4 = (bf16[136,256]{1,0:T(8,128)(2,1)}, bf16[136,256]{1,0:T(8,128)(2,1)S(1)}, u32[]{:S(2)}, u32[]{:S(2)}) collective-permute-start(bf16[136,256]{1,0:T(8,128)(2,1)} %get-tuple-element.15.refs_1_), channel_id=1, source_target_pairs={{0,8},{4,12},{8,0},{12,4},{16,24},{20,28},{24,16},{28,20},{1,9},{5... | collective-permute-start | bytes 208904 | tf_op jit(solution)/shard_map/ppermute | solution.py:18
  16.7 1.7 %collective-permute-start.3 = (bf16[136,256]{1,0:T(8,128)(2,1)}, bf16[136,256]{1,0:T(8,128)(2,1)S(1)}, u32[]{:S(2)}, u32[]{:S(2)}) collective-permute-start(bf16[136,256]{1,0:T(8,128)(2,1)} %get-tuple-element.15.refs_1_), channel_id=1, source_target_pairs={{0,4},{4,0},{8,12},{12,8},{16,20},{20,16},{24,28},{28,24},{1,5},{5... | collective-permute-start | bytes 208904 | tf_op jit(solution)/shard_map/ppermute | solution.py:18
  18.4 1.0 %collective-permute-done.8.refs_7_ = bf16[136,256]{1,0:T(8,128)(2,1)S(1)} collective-permute-done((bf16[136,256]{1,0:T(8,128)(2,1)}, bf16[136,256]{1,0:T(8,128)(2,1)S(1)}, u32[]{:S(2)}, u32[]{:S(2)}) %collective-permute-start.8) | collective-permute-done | bytes 69664 | tf_op jit(solution)/shard_map/ppermute | solution.py:18
  19.3 1.5 %collective-permute-start.9 = (bf16[136,256]{1,0:T(8,128)(2,1)S(1)}, bf16[136,256]{1,0:T(8,128)(2,1)S(1)}, u32[]{:S(2)}, u32[]{:S(2)}) collective-permute-start(bf16[136,256]{1,0:T(8,128)(2,1)S(1)} %collective-permute-done.8.refs_7_), channel_id=1, source_target_pairs={{0,4},{4,0},{8,12},{12,8},{16,20},{20,16},{24,28},{28,24},{1,5},{5... | collective-permute-start | bytes 208904 | tf_op jit(solution)/shard_map/ppermute | solution.py:18
  20.8 1.9 %collective-permute-done.6.refs_5_ = bf16[136,256]{1,0:T(8,128)(2,1)S(1)} collective-permute-done((bf16[136,256]{1,0:T(8,128)(2,1)}, bf16[136,256]{1,0:T(8,128)(2,1)S(1)}, u32[]{:S(2)}, u32[]{:S(2)}) %collective-permute-start.6) | collective-permute-done | bytes 69664 | tf_op jit(solution)/shard_map/ppermute | solution.py:18
  22.7 1.5 %collective-permute-start.7 = (bf16[136,256]{1,0:T(8,128)(2,1)S(1)}, bf16[136,256]{1,0:T(8,128)(2,1)S(1)}, u32[]{:S(2)}, u32[]{:S(2)}) collective-permute-start(bf16[136,256]{1,0:T(8,128)(2,1)S(1)} %collective-permute-done.6.refs_5_), channel_id=1, source_target_pairs={{0,4},{4,0},{8,12},{12,8},{16,20},{20,16},{24,28},{28,24},{1,5},{5... | collective-permute-start | bytes 208904 | tf_op jit(solution)/shard_map/ppermute | solution.py:18
  24.7 3.4 %collective-permute-start.10 = (bf16[32,128]{1,0:T(8,128)(2,1)}, bf16[32,128]{1,0:T(8,128)(2,1)S(1)}, u32[]{:S(2)}, u32[]{:S(2)}) collective-permute-start(bf16[32,128]{1,0:T(8,128)(2,1)} %get-tuple-element.16), channel_id=1, source_target_pairs={{0,4},{4,8},{8,12},{12,16},{16,20},{20,24},{24,28},{1,5},{5,9},{9,... | collective-permute-start | bytes 24584 | tf_op jit(solution)/shard_map/ppermute | solution.py:24
  28.1 1.6 %collective-permute-done.10.halo = bf16[32,128]{1,0:T(8,128)(2,1)S(1)} collective-permute-done((bf16[32,128]{1,0:T(8,128)(2,1)}, bf16[32,128]{1,0:T(8,128)(2,1)S(1)}, u32[]{:S(2)}, u32[]{:S(2)}) %collective-permute-start.10) | collective-permute-done | bytes 8224 | tf_op jit(solution)/shard_map/ppermute | solution.py:24
  30.2 1.7 %shard_map.119 = (f32[128,128]{1,0:T(8,128)}, f32[8,128]{1,0:T(8,128)}) custom-call(bf16[32,128]{1,0:T(8,128)(2,1)} %copy-done.12, bf16[128,128]{1,0:T(8,128)(2,1)} %get-tuple-element.17.blend, f32[31,128]{1,0:T(8,128)} %taps.1), custom_call_target="tpu_custom_call" | custom-call | flops 1048576 | tf_op jit(solution)/shard_map/pallas_call | solution.py:174
  31.9 1.5 %collective-permute-start.12 = (f32[8,128]{1,0:T(8,128)}, f32[8,128]{1,0:T(8,128)S(1)}, u32[]{:S(2)}, u32[]{:S(2)}) collective-permute-start(f32[8,128]{1,0:T(8,128)} %get-tuple-element.19.refs_10_), channel_id=1, source_target_pairs={{0,2},{1,3},{2,0},{3,1},{4,6},{5,7},{6,4},{7,5},{8,10},{9,11},{10,... | collective-permute-start | bytes 12296 | tf_op jit(solution)/shard_map/ppermute | solution.py:18
  33.5 2.3 %collective-permute-done.12.refs_12_ = f32[8,128]{1,0:T(8,128)S(1)} collective-permute-done((f32[8,128]{1,0:T(8,128)}, f32[8,128]{1,0:T(8,128)S(1)}, u32[]{:S(2)}, u32[]{:S(2)}) %collective-permute-start.12) | collective-permute-done | bytes 4128 | tf_op jit(solution)/shard_map/ppermute | solution.py:18
  35.8 1.4 %collective-permute-done.11.refs_11_ = f32[8,128]{1,0:T(8,128)S(1)} collective-permute-done((f32[8,128]{1,0:T(8,128)}, f32[8,128]{1,0:T(8,128)S(1)}, u32[]{:S(2)}, u32[]{:S(2)}) %collective-permute-start.11) | collective-permute-done | bytes 4128 | tf_op jit(solution)/shard_map/ppermute | solution.py:18
  37.3 1.0 %collective-permute-done.13.refs_13_ = f32[8,128]{1,0:T(8,128)S(1)} collective-permute-done((f32[8,128]{1,0:T(8,128)S(1)}, f32[8,128]{1,0:T(8,128)S(1)}, u32[]{:S(2)}, u32[]{:S(2)}) %collective-permute-start.13) | collective-permute-done | bytes 4128 | tf_op jit(solution)/shard_map/ppermute | solution.py:18
  39.0 6.9 %shard_map.120 = (f32[32,2048]{1,0:T(8,128)}, f32[32,2048]{1,0:T(8,128)}, bf16[64,2048]{1,0:T(8,128)(2,1)}) custom-call(bf16[256,128]{1,0:T(8,128)(2,1)} %get-tuple-element.14.refs_0_, bf16[136,256]{1,0:T(8,128)(2,1)} %get-tuple-element.15.refs_1_, bf16[136,256]{1,0:T(8,128)(2,1)} %copy-done.8, bf16[136,256]{1,0:T(8,128)(2,1)} %copy-done.7, ...), custom_call_target="tpu_custom_call" | custom-call | flops 201326592 | tf_op jit(solution)/shard_map/pallas_call | solution.py:174
  46.2 1.6 %collective-permute-done.14 = bf16[64,2048]{1,0:T(8,128)(2,1)S(1)} collective-permute-done((bf16[64,2048]{1,0:T(8,128)(2,1)}, bf16[64,2048]{1,0:T(8,128)(2,1)S(1)}, u32[]{:S(2)}, u32[]{:S(2)}) %collective-permute-start.14) | collective-permute-done | bytes 262176 | tf_op jit(solution)/shard_map/ppermute | solution.py:18
  47.8 1.6 %collective-permute-start.15 = (bf16[32,2048]{1,0:T(8,128)(2,1)S(1)}, bf16[32,2048]{1,0:T(8,128)(2,1)S(1)}, u32[]{:S(2)}, u32[]{:S(2)}) collective-permute-start(bf16[32,2048]{1,0:T(8,128)(2,1)S(1)} %fusion), channel_id=1, source_target_pairs={{0,2},{1,3},{2,0},{3,1},{4,6},{5,7},{6,4},{7,5},{8,10},{9,11},{10,... | collective-permute-start | bytes 393224 | tf_op jit(solution)/shard_map/ppermute | solution.py:18
  49.4 4.0 %collective-permute-done.15 = bf16[32,2048]{1,0:T(8,128)(2,1)S(1)} collective-permute-done((bf16[32,2048]{1,0:T(8,128)(2,1)S(1)}, bf16[32,2048]{1,0:T(8,128)(2,1)S(1)}, u32[]{:S(2)}, u32[]{:S(2)}) %collective-permute-start.15) | collective-permute-done | bytes 131104 | tf_op jit(solution)/shard_map/ppermute | solution.py:18
  53.5 0.7 %fusion.2 = bf16[32,2048]{1,0:T(8,128)(2,1)} fusion(f32[32,2048]{1,0:T(8,128)S(1)} %copy-done, f32[64,2048]{1,0:T(8,128)S(1)} %convert_element_type.14, bf16[32,2048]{1,0:T(8,128)(2,1)S(1)} %collective-permute-done.15), kind=kLoop, calls=%fused_computation.4 | loop fusion | flops 262144 | bytes 786432 | tf_op jit(solution)/shard_map/convert_element_type | solution.py:260
  (49 shorter events, 2.9 us)
Async XLA Ops:
  0.0 6.7 %copy-start.16 = (bf16[128,2]{0,1:T(2,128)(2,1)S(1)}, bf16[128,2]{0,1:T(2,128)(2,1)}, u32[]{:S(2)}) copy-start(bf16[128,2]{0,1:T(2,128)(2,1)} %param.20) | copy-start | bytes 1540
  0.0 6.7 %collective-permute-start.1 = (bf16[32,2048]{1,0:T(8,128)(2,1)}, bf16[32,2048]{1,0:T(8,128)(2,1)S(1)}, u32[]{:S(2)}, u32[]{:S(2)}) collective-permute-start(bf16[32,2048]{1,0:T(8,128)(2,1)} %refs_0_.1), channel_id=1, source_target_pairs={{0,2},{1,3},{2,0},{3,1},{4,6},{5,7},{6,4},{7,5},{8,10},{9,11},{10,... | collective-permute-start | bytes 393224 | tf_op jit(solution)/shard_map/ppermute | solution.py:18
  3.0 4.3 %collective-permute-start = (bf16[32,2048]{1,0:T(8,128)(2,1)}, bf16[32,2048]{1,0:T(8,128)(2,1)S(1)}, u32[]{:S(2)}, u32[]{:S(2)}) collective-permute-start(bf16[32,2048]{1,0:T(8,128)(2,1)} %refs_0_.1), channel_id=1, source_target_pairs={{0,1},{1,0},{2,3},{3,2},{4,5},{5,4},{6,7},{7,6},{8,9},{9,8},{10,11... | collective-permute-start | bytes 393224 | tf_op jit(solution)/shard_map/ppermute | solution.py:18
  6.7 1.4 %copy-start.2 = (bf16[32,2048]{1,0:T(8,128)(2,1)}, bf16[32,2048]{1,0:T(8,128)(2,1)S(1)}, u32[]{:S(2)}) copy-start(bf16[32,2048]{1,0:T(8,128)(2,1)S(1)} %collective-permute-done.1.refs_2_) | copy-start | bytes 393220
  6.7 1.3 %collective-permute-start.2 = (bf16[32,2048]{1,0:T(8,128)(2,1)S(1)}, bf16[32,2048]{1,0:T(8,128)(2,1)S(1)}, u32[]{:S(2)}, u32[]{:S(2)}) collective-permute-start(bf16[32,2048]{1,0:T(8,128)(2,1)S(1)} %collective-permute-done.1.refs_2_), channel_id=1, source_target_pairs={{0,1},{1,0},{2,3},{3,2},{4,5},{5,4},{6,7},{7,6},{8,9},{9,8},{10,11... | collective-permute-start | bytes 393224 | tf_op jit(solution)/shard_map/ppermute | solution.py:18
  12.2 7.1 %collective-permute-start.8 = (bf16[136,256]{1,0:T(8,128)(2,1)}, bf16[136,256]{1,0:T(8,128)(2,1)S(1)}, u32[]{:S(2)}, u32[]{:S(2)}) collective-permute-start(bf16[136,256]{1,0:T(8,128)(2,1)} %get-tuple-element.15.refs_1_), channel_id=1, source_target_pairs={{0,24},{4,28},{8,16},{12,20},{16,8},{20,12},{24,0},{28,4},{1,25},{... | collective-permute-start | bytes 208904 | tf_op jit(solution)/shard_map/ppermute | solution.py:18
  16.1 6.6 %collective-permute-start.6 = (bf16[136,256]{1,0:T(8,128)(2,1)}, bf16[136,256]{1,0:T(8,128)(2,1)S(1)}, u32[]{:S(2)}, u32[]{:S(2)}) collective-permute-start(bf16[136,256]{1,0:T(8,128)(2,1)} %get-tuple-element.15.refs_1_), channel_id=1, source_target_pairs={{0,16},{4,20},{8,24},{12,28},{16,0},{20,4},{24,8},{28,12},{1,17},{... | collective-permute-start | bytes 208904 | tf_op jit(solution)/shard_map/ppermute | solution.py:18
  16.1 8.1 %collective-permute-start.4 = (bf16[136,256]{1,0:T(8,128)(2,1)}, bf16[136,256]{1,0:T(8,128)(2,1)S(1)}, u32[]{:S(2)}, u32[]{:S(2)}) collective-permute-start(bf16[136,256]{1,0:T(8,128)(2,1)} %get-tuple-element.15.refs_1_), channel_id=1, source_target_pairs={{0,8},{4,12},{8,0},{12,4},{16,24},{20,28},{24,16},{28,20},{1,9},{5... | collective-permute-start | bytes 208904 | tf_op jit(solution)/shard_map/ppermute | solution.py:18
  16.7 21.6 %collective-permute-start.3 = (bf16[136,256]{1,0:T(8,128)(2,1)}, bf16[136,256]{1,0:T(8,128)(2,1)S(1)}, u32[]{:S(2)}, u32[]{:S(2)}) collective-permute-start(bf16[136,256]{1,0:T(8,128)(2,1)} %get-tuple-element.15.refs_1_), channel_id=1, source_target_pairs={{0,4},{4,0},{8,12},{12,8},{16,20},{20,16},{24,28},{28,24},{1,5},{5... | collective-permute-start | bytes 208904 | tf_op jit(solution)/shard_map/ppermute | solution.py:18
  19.3 19.1 %copy-start.5 = (bf16[136,256]{1,0:T(8,128)(2,1)}, bf16[136,256]{1,0:T(8,128)(2,1)S(1)}, u32[]{:S(2)}) copy-start(bf16[136,256]{1,0:T(8,128)(2,1)S(1)} %collective-permute-done.8.refs_7_) | copy-start | bytes 208900
  19.3 19.0 %collective-permute-start.9 = (bf16[136,256]{1,0:T(8,128)(2,1)S(1)}, bf16[136,256]{1,0:T(8,128)(2,1)S(1)}, u32[]{:S(2)}, u32[]{:S(2)}) collective-permute-start(bf16[136,256]{1,0:T(8,128)(2,1)S(1)} %collective-permute-done.8.refs_7_), channel_id=1, source_target_pairs={{0,4},{4,0},{8,12},{12,8},{16,20},{20,16},{24,28},{28,24},{1,5},{5... | collective-permute-start | bytes 208904 | tf_op jit(solution)/shard_map/ppermute | solution.py:18
  22.7 15.7 %copy-start.6 = (bf16[136,256]{1,0:T(8,128)(2,1)}, bf16[136,256]{1,0:T(8,128)(2,1)S(1)}, u32[]{:S(2)}) copy-start(bf16[136,256]{1,0:T(8,128)(2,1)S(1)} %collective-permute-done.6.refs_5_) | copy-start | bytes 208900
  22.7 15.7 %collective-permute-start.7 = (bf16[136,256]{1,0:T(8,128)(2,1)S(1)}, bf16[136,256]{1,0:T(8,128)(2,1)S(1)}, u32[]{:S(2)}, u32[]{:S(2)}) collective-permute-start(bf16[136,256]{1,0:T(8,128)(2,1)S(1)} %collective-permute-done.6.refs_5_), channel_id=1, source_target_pairs={{0,4},{4,0},{8,12},{12,8},{16,20},{20,16},{24,28},{28,24},{1,5},{5... | collective-permute-start | bytes 208904 | tf_op jit(solution)/shard_map/ppermute | solution.py:18
  24.2 14.2 %copy-start.7 = (bf16[136,256]{1,0:T(8,128)(2,1)}, bf16[136,256]{1,0:T(8,128)(2,1)S(1)}, u32[]{:S(2)}) copy-start(bf16[136,256]{1,0:T(8,128)(2,1)S(1)} %collective-permute-done.4.refs_3_) | copy-start | bytes 208900
  24.2 14.2 %collective-permute-start.5 = (bf16[136,256]{1,0:T(8,128)(2,1)S(1)}, bf16[136,256]{1,0:T(8,128)(2,1)S(1)}, u32[]{:S(2)}, u32[]{:S(2)}) collective-permute-start(bf16[136,256]{1,0:T(8,128)(2,1)S(1)} %collective-permute-done.4.refs_3_), channel_id=1, source_target_pairs={{0,4},{4,0},{8,12},{12,8},{16,20},{20,16},{24,28},{28,24},{1,5},{5... | collective-permute-start | bytes 208904 | tf_op jit(solution)/shard_map/ppermute | solution.py:18
  24.7 5.0 %collective-permute-start.10 = (bf16[32,128]{1,0:T(8,128)(2,1)}, bf16[32,128]{1,0:T(8,128)(2,1)S(1)}, u32[]{:S(2)}, u32[]{:S(2)}) collective-permute-start(bf16[32,128]{1,0:T(8,128)(2,1)} %get-tuple-element.16), channel_id=1, source_target_pairs={{0,4},{4,8},{8,12},{12,16},{16,20},{20,24},{24,28},{1,5},{5,9},{9,... | collective-permute-start | bytes 24584 | tf_op jit(solution)/shard_map/ppermute | solution.py:24
  31.9 3.8 %collective-permute-start.12 = (f32[8,128]{1,0:T(8,128)}, f32[8,128]{1,0:T(8,128)S(1)}, u32[]{:S(2)}, u32[]{:S(2)}) collective-permute-start(f32[8,128]{1,0:T(8,128)} %get-tuple-element.19.refs_10_), channel_id=1, source_target_pairs={{0,2},{1,3},{2,0},{3,1},{4,6},{5,7},{6,4},{7,5},{8,10},{9,11},{10,... | collective-permute-start | bytes 12296 | tf_op jit(solution)/shard_map/ppermute | solution.py:18
  35.8 2.6 %copy-start.13 = (f32[8,128]{1,0:T(8,128)}, f32[8,128]{1,0:T(8,128)S(1)}, u32[]{:S(2)}) copy-start(f32[8,128]{1,0:T(8,128)S(1)} %collective-permute-done.12.refs_12_) | copy-start | bytes 12292
  35.8 1.4 %collective-permute-start.11 = (f32[8,128]{1,0:T(8,128)}, f32[8,128]{1,0:T(8,128)S(1)}, u32[]{:S(2)}, u32[]{:S(2)}) collective-permute-start(f32[8,128]{1,0:T(8,128)} %get-tuple-element.19.refs_10_), channel_id=1, source_target_pairs={{0,1},{1,0},{2,3},{3,2},{4,5},{5,4},{6,7},{7,6},{8,9},{9,8},{10,11... | collective-permute-start | bytes 12296 | tf_op jit(solution)/shard_map/ppermute | solution.py:18
  37.1 1.2 %collective-permute-start.13 = (f32[8,128]{1,0:T(8,128)S(1)}, f32[8,128]{1,0:T(8,128)S(1)}, u32[]{:S(2)}, u32[]{:S(2)}) collective-permute-start(f32[8,128]{1,0:T(8,128)S(1)} %collective-permute-done.12.refs_12_), channel_id=1, source_target_pairs={{0,1},{1,0},{2,3},{3,2},{4,5},{5,4},{6,7},{7,6},{8,9},{9,8},{10,11... | collective-permute-start | bytes 12296 | tf_op jit(solution)/shard_map/ppermute | solution.py:18
  45.9 1.9 %copy-start.1 = (f32[32,2048]{1,0:T(8,128)S(1)}, f32[32,2048]{1,0:T(8,128)}, u32[]{:S(2)}) copy-start(f32[32,2048]{1,0:T(8,128)} %get-tuple-element.22) | copy-start | bytes 786436
  45.9 1.8 %collective-permute-start.14 = (bf16[64,2048]{1,0:T(8,128)(2,1)}, bf16[64,2048]{1,0:T(8,128)(2,1)S(1)}, u32[]{:S(2)}, u32[]{:S(2)}) collective-permute-start(bf16[64,2048]{1,0:T(8,128)(2,1)} %get-tuple-element.21), channel_id=1, source_target_pairs={{0,1},{1,0},{2,3},{3,2},{4,5},{5,4},{6,7},{7,6},{8,9},{9,8},{10,11... | collective-permute-start | bytes 786440 | tf_op jit(solution)/shard_map/ppermute | solution.py:18
  47.8 5.7 %copy-start = (f32[32,2048]{1,0:T(8,128)S(1)}, f32[32,2048]{1,0:T(8,128)}, u32[]{:S(2)}) copy-start(f32[32,2048]{1,0:T(8,128)} %get-tuple-element.20) | copy-start | bytes 786436
  47.8 5.6 %collective-permute-start.15 = (bf16[32,2048]{1,0:T(8,128)(2,1)S(1)}, bf16[32,2048]{1,0:T(8,128)(2,1)S(1)}, u32[]{:S(2)}, u32[]{:S(2)}) collective-permute-start(bf16[32,2048]{1,0:T(8,128)(2,1)S(1)} %fusion), channel_id=1, source_target_pairs={{0,2},{1,3},{2,0},{3,1},{4,6},{5,7},{6,4},{7,5},{8,10},{9,11},{10,... | collective-permute-start | bytes 393224 | tf_op jit(solution)/shard_map/ppermute | solution.py:18
  (9 other events, 6.4 us)

commit v2 on v1

--- a/solution.py
+++ b/solution.py
@@ -28,37 +28,77 @@
     return jnp.dot(a, b, preferred_element_type=f32)
 
 
-def project_kernel(*refs, pieces):
-    toks = refs[:pieces]
-    w_in, w_gate, w_q, w_k, w_v, off, pay, qs, blend, tail, x_all = refs[pieces:]
-    rows = toks[0].shape[0]
+def load_kernel(*refs):
+    sources, sems = refs[:12], refs[-1]
+    tokens, w_in, w_gate, w_q, w_k, w_v, taps, c_gain, off, s_gain, w_c, w_s = sources
+    tok, conv_w, q_w, kv_w, taps_v, c_gain_v, off_v, s_gain_v, out_w = refs[12:-1]
+    ch = w_in.shape[1]
+    kv = w_k.shape[1]
+    pairs = [
+        (w_k, kv_w.at[:, 0:kv]),
+        (w_v, kv_w.at[:, kv:]),
+        (w_q, q_w),
+        (w_in, conv_w.at[:, 0:ch]),
+        (w_gate, conv_w.at[:, ch:]),
+        (tokens, tok),
+        (taps, taps_v),
+        (c_gain, c_gain_v),
+        (off, off_v),
+        (s_gain, s_gain_v),
+        (w_c, out_w.at[0:ch]),
+        (w_s, out_w.at[ch:]),
+    ]
+    copies = [pltpu.make_async_copy(a, b, sems.at[i]) for i, (a, b) in enumerate(pairs)]
+    for copy in copies:
+        copy.start()
+    for copy in copies:
+        copy.wait()
+
+
+def project_kernel(t0, t1, t2, t3, conv_w, q_w, kv_w, off, pay, qs, blend, x_all):
+    rows = t0.shape[0]
     me = lax.axis_index("tp")
-    for k in range(pieces):
-        x_all[pl.ds(pl.multiple_of((me ^ k) * rows, rows), rows), :] = toks[k][...]
+    for k, t in enumerate((t0, t1, t2, t3)):
+        x_all[pl.ds(pl.multiple_of((me ^ k) * rows, rows), rows), :] = t[...]
     x = x_all[...]
     n = x.shape[0]
-    kv = w_k.shape[1]
-    pay[0:n, 0:kv] = dot(x, w_k[...]).astype(bf16)
-    pay[0:n, kv : 2 * kv] = dot(x, w_v[...]).astype(bf16)
-    pay[n:, 0:kv] = off[...]
-    pay[n:, kv : 2 * kv] = jnp.zeros_like(off)
-    q = dot(x, w_q[...]).astype(bf16)
+    ch = conv_w.shape[1] // 2
+    kv = kv_w.shape[1] // 2
+    pay[0:n, :] = dot(x, kv_w[...]).astype(bf16)
+    q = dot(x, q_w[...]).astype(bf16)
     for h in range(q.shape[1] // HEAD_DIM):
         qs[h * n : (h + 1) * n, :] = q[:, h * HEAD_DIM : (h + 1) * HEAD_DIM]
-    values = dot(x, w_in[...]).astype(bf16).astype(f32)
-    gates = dot(x, w_gate[...]).astype(bf16).astype(f32)
-    b = (values * jax.nn.sigmoid(gates)).astype(bf16)
+    both = dot(x, conv_w[...]).astype(bf16).astype(f32)
+    b = (both[:, 0:ch] * jax.nn.sigmoid(both[:, ch:])).astype(bf16)
     blend[...] = b
-    tail[...] = b[n - tail.shape[0] :, :]
-
-
-def conv_kernel(halo, blend, taps, field, stats, wide):
+    row = lax.broadcasted_iota(jnp.int32, (16, kv), 0)
+    pay[n:, 0:kv] = jnp.where(row < 2, off[...], b[n - 32 : n - 16, :])
+    pay[n:, kv:] = b[n - 16 :, :]
+
+
+def conv_kernel(p1, p3, p7, blend, taps, field, stats, wide):
     n = blend.shape[0]
-    h = halo.shape[0]
+    half = p1.shape[1] // 2
     reach = taps.shape[0] - 1
-    wide[0:h, :] = halo[...].astype(f32)
-    wide[h : h + n, :] = blend[...].astype(f32)
-    base = h - reach
+    me = lax.axis_index("sp")
+    flip = me ^ (me - 1)
+    halo = jnp.where(flip == 1, p1[n:, :], jnp.where(flip == 3, p3[n:, :], p7[n:, :]))
+    halo = jnp.where(me > 0, halo.astype(f32), 0.0)
+    wide[0:16, :] = halo[:, 0:half]
+    wide[16:32, :] = halo[:, half:]
+    convolve(blend, taps, field, stats, wide)
+
+
+def conv_plain_kernel(halo, blend, taps, field, stats, wide):
+    wide[0:32, :] = halo[...].astype(f32)
+    convolve(blend, taps, field, stats, wide)
+
+
+def convolve(blend, taps, field, stats, wide):
+    n = blend.shape[0]
+    reach = taps.shape[0] - 1
+    wide[32 : 32 + n, :] = blend[...].astype(f32)
+    base = 32 - reach
     f = taps[0:1, :] * wide[base : base + n, :]
     for t in range(1, reach + 1):
         f = f + taps[t : t + 1, :] * wide[base + t : base + t + n, :]
@@ -75,7 +115,7 @@
     kv = HEAD_DIM
     keys = pay[0:n, 0:kv]
     vals = pay[0:n, kv : 2 * kv]
-    off = pay[n : n + 8, 0:kv].astype(f32)
+    off = pay[n : n + 16, 0:kv].astype(f32)
     s = lax.dot_general(q, keys, (((1,), (1,)), ((), ())), preferred_element_type=f32)
     s = s * (HEAD_DIM ** (-0.5))
     shift = jnp.concatenate(
@@ -101,7 +141,7 @@
     return jnp.where((r > c) | (c >= n), 1.0, 0.0).astype(bf16)
 
 
-def finish(att, field, stats, c_gain, s_gain, w_c, w_s, mine, other, send, mix, n, per, members):
+def finish(att, field, stats, c_gain, s_gain, out_w, mine, other, send, mix, n, per, members):
     ch = field.shape[1]
     mean = sum(st[0:1, :] for st in stats) / members
     m2 = sum(st[1:2, :] for st in stats)
@@ -121,7 +161,7 @@
     lhs = jnp.concatenate(
         [mix[pl.ds(pl.multiple_of((me ^ k) * rows, rows), rows), :] for k in (0, 2, 1, 3)], axis=0
     )
-    out = dot(lhs[:, 0:ch], w_c[...]) + dot(lhs[:, ch:], w_s[...])
+    out = dot(lhs, out_w[...])
     mine[...] = out[0:rows, :]
     other[...] = out[rows : 2 * rows, :]
     send[...] = out[2 * rows :, :].astype(bf16)
@@ -132,7 +172,7 @@
     pays = refs[1 : 1 + blocks]
     field = refs[1 + blocks]
     stats = refs[2 + blocks : 2 + blocks + members]
-    c_gain, s_gain, w_c, w_s, mine, other, send, mix, parts, totals = refs[2 + blocks + members :]
+    c_gain, s_gain, out_w, mine, other, send, mix, parts, totals = refs[2 + blocks + members :]
     me = lax.axis_index("sp")
     q = q_ref[...]
     tri = tri_of(n)
@@ -147,13 +187,13 @@
         att = att + jnp.exp(carry) * parts[j]
         if j:
             carry = carry + totals[j]
-    finish(att, field, stats, c_gain, s_gain, w_c, w_s, mine, other, send, mix, n, per, members)
+    finish(att, field, stats, c_gain, s_gain, out_w, mine, other, send, mix, n, per, members)
 
 
 def attend_loop_kernel(*refs, members, n, per):
     q_ref, pays, field = refs[:3]
     stats = refs[3 : 3 + members]
-    c_gain, s_gain, w_c, w_s, mine, other, send, mix = refs[3 + members :]
+    c_gain, s_gain, out_w, mine, other, send, mix = refs[3 + members :]
     me = lax.axis_index("sp")
     q = q_ref[...]
     tri = tri_of(n)
@@ -166,18 +206,25 @@
 
     zero = jnp.zeros((per * n, HEAD_DIM), f32)
     att, _ = lax.fori_loop(0, me + 1, step, (zero, zero))
-    finish(att, field, stats, c_gain, s_gain, w_c, w_s, mine, other, send, mix, n, per, members)
-
-
-def call(body, outs, *args, scratch=(), flops=0):
-    spec = pl.BlockSpec(memory_space=pltpu.VMEM)
+    finish(att, field, stats, c_gain, s_gain, out_w, mine, other, send, mix, n, per, members)
+
+
+def call(body, outs, args, scratch=(), flops=0, spaces=None, limit=2**23):
+    in_vmem = pl.BlockSpec(memory_space=pltpu.VMEM)
+    if spaces is None:
+        spaces = [True] * len(args)
+    args = [
+        pltpu.with_memory_space_constraint(arg, pltpu.VMEM) if held else arg
+        for arg, held in zip(args, spaces)
+    ]
     return pl.pallas_call(
         body,
-        out_shape=outs,
-        in_specs=[spec] * len(args),
-        out_specs=[spec] * len(outs),
+        out_shape=[pltpu.VMEM(shape, dtype) for shape, dtype in outs],
+        in_specs=[in_vmem] * len(args),
+        out_specs=[in_vmem] * len(outs),
         scratch_shapes=scratch,
         cost_estimate=pl.CostEstimate(flops=flops, transcendentals=0, bytes_accessed=0),
+        compiler_params=pltpu.CompilerParams(vmem_limit_bytes=limit),
     )(*args)
 
 
@@ -201,59 +248,81 @@
     n = rows * members
     ch = conv_input.shape[1]
     kv = key_weight.shape[1]
-    per = query_weight.shape[1] // kv
-    off = jnp.pad(jnp.transpose(key_offsets), ((0, 8 - per), (0, 0)))
+    query_cols = query_weight.shape[1]
+    per = query_cols // kv
+    off = jnp.pad(jnp.transpose(key_offsets), ((0, 16 - per), (0, 0)))
     by_core = swap(tokens, "tp", 1)
     by_chip = swap(tokens, "tp", 2)
     by_both = swap(by_chip, "tp", 1)
-    pay, qs, blend, tail = call(
-        functools.partial(project_kernel, pieces=4),
-        [
-            jax.ShapeDtypeStruct((n + 8, 2 * kv), bf16),
-            jax.ShapeDtypeStruct((per * n, HEAD_DIM), bf16),
-            jax.ShapeDtypeStruct((n, ch), bf16),
-            jax.ShapeDtypeStruct((32, ch), bf16),
+    in_vmem = pl.BlockSpec(memory_space=pltpu.VMEM)
+    tok, conv_w, q_w, kv_w, taps, c_gain, off, s_gain, out_w = pl.pallas_call(
+        load_kernel,
+        out_shape=[
+            pltpu.VMEM(shape, dtype)
+            for shape, dtype in (
+                ((rows, width), bf16),
+                ((width, 2 * ch), bf16),
+                ((width, query_cols), bf16),
+                ((width, 2 * kv), bf16),
+                (conv_taps.shape, f32),
+                ((1, ch), f32),
+                ((16, n), bf16),
+                ((per, HEAD_DIM), f32),
+                ((ch + query_cols, width), bf16),
+            )
         ],
-        tokens, by_core, by_chip, by_both,
-        conv_input, conv_gate, query_weight, key_weight, value_weight, off,
+        in_specs=[pl.BlockSpec(memory_space=pltpu.HBM)] * 12,
+        out_specs=[in_vmem] * 9,
+        scratch_shapes=[pltpu.SemaphoreType.DMA((12,))],
+        cost_estimate=pl.CostEstimate(flops=10**9, transcendentals=0, bytes_accessed=5 * 10**6),
+        compiler_params=pltpu.CompilerParams(vmem_limit_bytes=2**21),
+    )(
+        tokens, conv_input, conv_gate, query_weight, key_weight, value_weight, conv_taps,
+        conv_gain.reshape(1, ch), off, stick_gain.reshape(per, HEAD_DIM),
+        conv_output, stick_output,
+    )
+    pay, qs, blend = call(
+        project_kernel,
+        [((n + 16, 2 * kv), bf16), ((per * n, HEAD_DIM), bf16), ((n, ch), bf16)],
+        [tok, by_core, by_chip, by_both, conv_w, q_w, kv_w, off],
         scratch=[pltpu.VMEM((n, width), bf16)],
         flops=2 * n * width * (2 * ch + 4 * kv),
     )
-    halo = from_behind(tail, "sp", 1)
+    field_shapes = [((n, ch), f32), ((8, n), f32)]
+    wide = [pltpu.VMEM((n + 32, ch), f32)]
     if blocks == 8:
         z6 = swap(pay, "sp", 6)
+        z2 = swap(pay, "sp", 2)
         z4 = swap(pay, "sp", 4)
-        z2 = swap(pay, "sp", 2)
         x1 = swap(pay, "sp", 1)
-        pays = [pay, x1, z2, swap(z2, "sp", 1), z4, swap(z4, "sp", 1), z6, swap(z6, "sp", 1)]
+        x7 = swap(z6, "sp", 1)
+        x3 = swap(z2, "sp", 1)
+        x5 = swap(z4, "sp", 1)
+        pays = [pay, x1, z2, x3, z4, x5, z6, x7]
+        conv_args = [x1, x3, x7, blend, taps]
+        field, stats = call(conv_kernel, field_shapes, conv_args, wide, 64 * n * ch)
     else:
         pays = [lax.all_gather(pay, "sp", axis=0)]
-    field, stats = call(
-        conv_kernel,
-        [jax.ShapeDtypeStruct((n, ch), f32), jax.ShapeDtypeStruct((8, n), f32)],
-        halo, blend, conv_taps,
-        scratch=[pltpu.VMEM((n + 32, ch), f32)],
-        flops=64 * n * ch,
-    )
+        halo = from_behind(blend[n - 32 :], "sp", 1)
+        conv_args = [halo, blend, taps]
+        field, stats = call(conv_plain_kernel, field_shapes, conv_args, wide, 64 * n * ch)
     stats_chip = swap(stats, "tp", 2)
     all_stats = [stats, swap(stats, "tp", 1), stats_chip, swap(stats_chip, "tp", 1)]
-    scratch = [pltpu.VMEM((n, ch + per * HEAD_DIM), bf16)]
+    scratch = [pltpu.VMEM((n, ch + query_cols), bf16)]
     if blocks == 8:
         body = functools.partial(attend_kernel, blocks=blocks, members=members, n=n, per=per)
         scratch += [pltpu.VMEM((blocks, per * n, HEAD_DIM), f32)] * 2
     else:
         body = functools.partial(attend_loop_kernel, members=members, n=n, per=per)
+    args = [qs, *pays, field, *all_stats, c_gain, s_gain, out_w]
     mine, other, send = call(
         body,
-        [
-            jax.ShapeDtypeStruct((rows, width), f32),
-            jax.ShapeDtypeStruct((rows, width), f32),
-            jax.ShapeDtypeStruct((2 * rows, width), bf16),
-        ],
-        qs, *pays, field, *all_stats,
-        conv_gain.reshape(1, ch), stick_gain.reshape(per, HEAD_DIM), conv_output, stick_output,
+        [((rows, width), f32), ((rows, width), f32), ((2 * rows, width), bf16)],
+        args,
         scratch=scratch,
-        flops=2 * n * width * (ch + per * HEAD_DIM),
+        flops=2 * n * width * (ch + query_cols),
+        limit=2**23 if blocks == 8 else 2**25,
+        spaces=[True] + [blocks == 8] * len(pays) + [True] * (len(args) - 1 - len(pays)),
     )
     got = swap(send, "tp", 1).astype(f32)
     chip = swap((other + got[rows:]).astype(bf16), "tp", 2)

time: 54.4 us -> 52.4 us (0.963)
  local copies, waits for them, and re-layouts: 2.48 us -> 11.3 us
  Pallas kernels: 12.2 us -> 6.15 us
  starting transfers between devices: 19.5 us -> 16.8 us
  waiting for transfers between devices: 19.1 us -> 16.8 us
    unnamed x34 -> x22, local copies, waits for them, and re-layouts: 1.87 us -> 10.6 us
    pallas_call x3 -> x4, Pallas kernels: 12.2 us -> 6.15 us  [the longest x3 5.27 us: call(): pl.pallas_call(body, out_shape=[pltpu.VMEM(shape, dtype) for shape, dtype...]
    ppermute x1 -> x0, starting transfers between devices: 3.38 us -> none  [from_behind(): return lax.ppermute(value, axis, pairs)]
    ppermute x1 -> x0, waiting for transfers between devices: 1.56 us -> none  [from_behind(): return lax.ppermute(value, axis, pairs)]
    ppermute x15, waiting for transfers between devices: 17.5 us -> 16.8 us  [swap(): return lax.ppermute(value, axis, [(i, i ^ by) for i in range(count)])]
    ppermute x15, starting transfers between devices: 16.1 us -> 16.8 us  [swap(): return lax.ppermute(value, axis, [(i, i ^ by) for i in range(count)])]
  transfers between devices with their start and end apart: 16 -> 15, of which waited for: 10 -> 8; matrix products, arithmetic and copies ran while one was open for 1% -> 1% of each run, Pallas kernels for 3% -> 2%
where the time goes in v2:
time: 52.4 us; the launch traced here: 51.9 us
  starting transfers between devices  16.8 us (32%)
  waiting for transfers between devices  16.8 us (32%)
  local copies, waits for them, and re-layouts  11.3 us (22%)
  Pallas kernels  6.15 us (12%)
  other arithmetic  0.77 us (1%)
    ppermute x15, starting transfers between devices, swap(): return lax.ppermute(value, axis, [(i, i ^ by) for i in range(count)])  16.8 us
    ppermute x15, waiting for transfers between devices, swap(): return lax.ppermute(value, axis, [(i, i ^ by) for i in range(count)])  16.8 us
    unnamed x22, local copies, waits for them, and re-layouts  10.6 us
    pallas_call x3, Pallas kernels, call(): pl.pallas_call(body, out_shape=[pltpu.VMEM(shape, dtype) for shape, dtype...  5.27 us
  transfers between devices with their start and end apart: 15, of which 8 were waited for; matrix products, arithmetic and copies ran while one was open for 1% of the time, Pallas kernels for 2%

profile of v2, /device:TPU:0, one launch (start us, length us, event | category | flops | bytes accessed | tf_op | source)
XLA Modules:
  0.0 51.9 jit_solution(18152628977878451257)
XLA Ops:
  0.0 3.0 %collective-permute-start.1 = (bf16[32,2048]{1,0:T(8,128)(2,1)}, bf16[32,2048]{1,0:T(8,128)(2,1)S(1)}, u32[]{:S(2)}, u32[]{:S(2)}) collective-permute-start(bf16[32,2048]{1,0:T(8,128)(2,1)} %refs_0_.1), channel_id=1, source_target_pairs={{0,2},{1,3},{2,0},{3,1},{4,6},{5,7},{6,4},{7,5},{8,10},{9,11},{10,... | collective-permute-start | bytes 393224 | tf_op jit(solution)/shard_map/ppermute | solution.py:18
  3.0 3.7 %collective-permute-done.1.t2 = bf16[32,2048]{1,0:T(8,128)(2,1)S(1)} collective-permute-done((bf16[32,2048]{1,0:T(8,128)(2,1)}, bf16[32,2048]{1,0:T(8,128)(2,1)S(1)}, u32[]{:S(2)}, u32[]{:S(2)}) %collective-permute-start.1) | collective-permute-done | bytes 131104 | tf_op jit(solution)/shard_map/ppermute | solution.py:18
  7.4 1.2 %copy-done = bf16[2048,256]{1,0:T(8,128)(2,1)S(1)} copy-done((bf16[2048,256]{1,0:T(8,128)(2,1)S(1)}, bf16[2048,256]{1,0:T(8,128)(2,1)}, u32[]{:S(2)}) %copy-start) | copy-done | bytes 1048600
  8.6 1.2 %copy-done.1 = bf16[256,2048]{1,0:T(8,128)(2,1)S(1)} copy-done((bf16[256,2048]{1,0:T(8,128)(2,1)S(1)}, bf16[256,2048]{1,0:T(8,128)(2,1)}, u32[]{:S(2)}) %copy-start.1) | copy-done | bytes 1048600
  9.8 1.0 %copy-done.2 = bf16[2048,128]{1,0:T(8,128)(2,1)S(1)} copy-done((bf16[2048,128]{1,0:T(8,128)(2,1)S(1)}, bf16[2048,128]{1,0:T(8,128)(2,1)}, u32[]{:S(2)}) %copy-start.2) | copy-done | bytes 524312
  10.9 1.0 %copy-done.3 = bf16[2048,128]{1,0:T(8,128)(2,1)S(1)} copy-done((bf16[2048,128]{1,0:T(8,128)(2,1)S(1)}, bf16[2048,128]{1,0:T(8,128)(2,1)}, u32[]{:S(2)}) %copy-start.3) | copy-done | bytes 524312
  11.9 1.0 %copy-done.4 = bf16[2048,128]{1,0:T(8,128)(2,1)S(1)} copy-done((bf16[2048,128]{1,0:T(8,128)(2,1)S(1)}, bf16[2048,128]{1,0:T(8,128)(2,1)}, u32[]{:S(2)}) %copy-start.4) | copy-done | bytes 524312
  12.9 1.0 %copy-done.5 = bf16[2048,128]{1,0:T(8,128)(2,1)S(1)} copy-done((bf16[2048,128]{1,0:T(8,128)(2,1)S(1)}, bf16[2048,128]{1,0:T(8,128)(2,1)}, u32[]{:S(2)}) %copy-start.5) | copy-done | bytes 524312
  14.0 1.0 %copy-done.6 = bf16[128,2048]{1,0:T(8,128)(2,1)S(1)} copy-done((bf16[128,2048]{1,0:T(8,128)(2,1)S(1)}, bf16[128,2048]{1,0:T(8,128)(2,1)}, u32[]{:S(2)}) %copy-start.6) | copy-done | bytes 524312
  15.0 0.9 %copy-done.7 = bf16[32,2048]{1,0:T(8,128)(2,1)S(1)} copy-done((bf16[32,2048]{1,0:T(8,128)(2,1)S(1)}, bf16[32,2048]{1,0:T(8,128)(2,1)}, u32[]{:S(2)}) %copy-start.7) | copy-done | bytes 131096
  19.6 3.9 %collective-permute-start.8 = (bf16[144,256]{1,0:T(8,128)(2,1)S(1)}, bf16[144,256]{1,0:T(8,128)(2,1)S(1)}, u32[]{:S(2)}, u32[]{:S(2)}) collective-permute-start(bf16[144,256]{1,0:T(8,128)(2,1)S(1)} %get-tuple-element.28.refs_1_), channel_id=1, source_target_pairs={{0,24},{4,28},{8,16},{12,20},{16,8},{20,12},{24,0},{28,4},{1,25},{... | collective-permute-start | bytes 221192 | tf_op jit(solution)/shard_map/ppermute | solution.py:18
  24.1 1.6 %collective-permute-start.3 = (bf16[144,256]{1,0:T(8,128)(2,1)S(1)}, bf16[144,256]{1,0:T(8,128)(2,1)S(1)}, u32[]{:S(2)}, u32[]{:S(2)}) collective-permute-start(bf16[144,256]{1,0:T(8,128)(2,1)S(1)} %get-tuple-element.28.refs_1_), channel_id=1, source_target_pairs={{0,4},{4,0},{8,12},{12,8},{16,20},{20,16},{24,28},{28,24},{1,5},{5... | collective-permute-start | bytes 221192 | tf_op jit(solution)/shard_map/ppermute | solution.py:18
  25.7 0.9 %collective-permute-done.8.refs_7_ = bf16[144,256]{1,0:T(8,128)(2,1)S(1)} collective-permute-done((bf16[144,256]{1,0:T(8,128)(2,1)S(1)}, bf16[144,256]{1,0:T(8,128)(2,1)S(1)}, u32[]{:S(2)}, u32[]{:S(2)}) %collective-permute-start.8) | collective-permute-done | bytes 73760 | tf_op jit(solution)/shard_map/ppermute | solution.py:18
  26.6 1.7 %collective-permute-start.9 = (bf16[144,256]{1,0:T(8,128)(2,1)S(1)}, bf16[144,256]{1,0:T(8,128)(2,1)S(1)}, u32[]{:S(2)}, u32[]{:S(2)}) collective-permute-start(bf16[144,256]{1,0:T(8,128)(2,1)S(1)} %collective-permute-done.8.refs_7_), channel_id=1, source_target_pairs={{0,4},{4,0},{8,12},{12,8},{16,20},{20,16},{24,28},{28,24},{1,5},{5... | collective-permute-start | bytes 221192 | tf_op jit(solution)/shard_map/ppermute | solution.py:18
  28.3 1.0 %collective-permute-done.4.refs_3_ = bf16[144,256]{1,0:T(8,128)(2,1)S(1)} collective-permute-done((bf16[144,256]{1,0:T(8,128)(2,1)S(1)}, bf16[144,256]{1,0:T(8,128)(2,1)S(1)}, u32[]{:S(2)}, u32[]{:S(2)}) %collective-permute-start.4) | collective-permute-done | bytes 73760 | tf_op jit(solution)/shard_map/ppermute | solution.py:18
  29.3 1.7 %collective-permute-start.5 = (bf16[144,256]{1,0:T(8,128)(2,1)S(1)}, bf16[144,256]{1,0:T(8,128)(2,1)S(1)}, u32[]{:S(2)}, u32[]{:S(2)}) collective-permute-start(bf16[144,256]{1,0:T(8,128)(2,1)S(1)} %collective-permute-done.4.refs_3_), channel_id=1, source_target_pairs={{0,4},{4,0},{8,12},{12,8},{16,20},{20,16},{24,28},{28,24},{1,5},{5... | collective-permute-start | bytes 221192 | tf_op jit(solution)/shard_map/ppermute | solution.py:18
  31.9 2.5 %collective-permute-done.5.p3.refs_4_ = bf16[144,256]{1,0:T(8,128)(2,1)S(1)} collective-permute-done((bf16[144,256]{1,0:T(8,128)(2,1)S(1)}, bf16[144,256]{1,0:T(8,128)(2,1)S(1)}, u32[]{:S(2)}, u32[]{:S(2)}) %collective-permute-start.5) | collective-permute-done | bytes 73760 | tf_op jit(solution)/shard_map/ppermute | solution.py:18
  34.8 1.6 %collective-permute-start.11 = (f32[8,128]{1,0:T(8,128)S(1)}, f32[8,128]{1,0:T(8,128)S(1)}, u32[]{:S(2)}, u32[]{:S(2)}) collective-permute-start(f32[8,128]{1,0:T(8,128)S(1)} %get-tuple-element.32.refs_10_), channel_id=1, source_target_pairs={{0,2},{1,3},{2,0},{3,1},{4,6},{5,7},{6,4},{7,5},{8,10},{9,11},{10,... | collective-permute-start | bytes 12296 | tf_op jit(solution)/shard_map/ppermute | solution.py:18
  36.3 2.1 %collective-permute-done.11.refs_12_ = f32[8,128]{1,0:T(8,128)S(1)} collective-permute-done((f32[8,128]{1,0:T(8,128)S(1)}, f32[8,128]{1,0:T(8,128)S(1)}, u32[]{:S(2)}, u32[]{:S(2)}) %collective-permute-start.11) | collective-permute-done | bytes 4128 | tf_op jit(solution)/shard_map/ppermute | solution.py:18
  38.4 1.2 %collective-permute-done.12.refs_13_ = f32[8,128]{1,0:T(8,128)S(1)} collective-permute-done((f32[8,128]{1,0:T(8,128)S(1)}, f32[8,128]{1,0:T(8,128)S(1)}, u32[]{:S(2)}, u32[]{:S(2)}) %collective-permute-start.12) | collective-permute-done | bytes 4128 | tf_op jit(solution)/shard_map/ppermute | solution.py:18
  39.6 4.3 %shard_map.121 = (f32[32,2048]{1,0:T(8,128)S(1)}, f32[32,2048]{1,0:T(8,128)S(1)}, bf16[64,2048]{1,0:T(8,128)(2,1)S(1)}) custom-call(bf16[256,128]{1,0:T(8,128)(2,1)S(1)} %get-tuple-element.27.refs_0_, bf16[144,256]{1,0:T(8,128)(2,1)S(1)} %get-tuple-element.28.refs_1_, bf16[144,256]{1,0:T(8,128)(2,1)S(1)} %collective-permute-done.3.p1.refs_2_, ...), custom_call_target="tpu_custom_call" | custom-call | flops 201326592 | tf_op jit(solution)/shard_map/pallas_call | solution.py:220
  44.1 1.4 %collective-permute-done.13 = bf16[64,2048]{1,0:T(8,128)(2,1)S(1)} collective-permute-done((bf16[64,2048]{1,0:T(8,128)(2,1)S(1)}, bf16[64,2048]{1,0:T(8,128)(2,1)S(1)}, u32[]{:S(2)}, u32[]{:S(2)}) %collective-permute-start.13) | collective-permute-done | bytes 262176 | tf_op jit(solution)/shard_map/ppermute | solution.py:18
  45.5 1.6 %collective-permute-start.14 = (bf16[32,2048]{1,0:T(8,128)(2,1)S(1)}, bf16[32,2048]{1,0:T(8,128)(2,1)S(1)}, u32[]{:S(2)}, u32[]{:S(2)}) collective-permute-start(bf16[32,2048]{1,0:T(8,128)(2,1)S(1)} %fusion), channel_id=1, source_target_pairs={{0,2},{1,3},{2,0},{3,1},{4,6},{5,7},{6,4},{7,5},{8,10},{9,11},{10,... | collective-permute-start | bytes 393224 | tf_op jit(solution)/shard_map/ppermute | solution.py:18
  47.1 4.0 %collective-permute-done.14 = bf16[32,2048]{1,0:T(8,128)(2,1)S(1)} collective-permute-done((bf16[32,2048]{1,0:T(8,128)(2,1)S(1)}, bf16[32,2048]{1,0:T(8,128)(2,1)S(1)}, u32[]{:S(2)}, u32[]{:S(2)}) %collective-permute-start.14) | collective-permute-done | bytes 131104 | tf_op jit(solution)/shard_map/ppermute | solution.py:18
  (36 shorter events, 7.2 us)
Async XLA Ops:
  0.0 6.7 %collective-permute-start.1 = (bf16[32,2048]{1,0:T(8,128)(2,1)}, bf16[32,2048]{1,0:T(8,128)(2,1)S(1)}, u32[]{:S(2)}, u32[]{:S(2)}) collective-permute-start(bf16[32,2048]{1,0:T(8,128)(2,1)} %refs_0_.1), channel_id=1, source_target_pairs={{0,2},{1,3},{2,0},{3,1},{4,6},{5,7},{6,4},{7,5},{8,10},{9,11},{10,... | collective-permute-start | bytes 393224 | tf_op jit(solution)/shard_map/ppermute | solution.py:18
  3.0 15.9 %collective-permute-start = (bf16[32,2048]{1,0:T(8,128)(2,1)}, bf16[32,2048]{1,0:T(8,128)(2,1)S(1)}, u32[]{:S(2)}, u32[]{:S(2)}) collective-permute-start(bf16[32,2048]{1,0:T(8,128)(2,1)} %refs_0_.1), channel_id=1, source_target_pairs={{0,1},{1,0},{2,3},{3,2},{4,5},{5,4},{6,7},{7,6},{8,9},{9,8},{10,11... | collective-permute-start | bytes 393224 | tf_op jit(solution)/shard_map/ppermute | solution.py:18
  6.7 12.2 %collective-permute-start.2 = (bf16[32,2048]{1,0:T(8,128)(2,1)S(1)}, bf16[32,2048]{1,0:T(8,128)(2,1)S(1)}, u32[]{:S(2)}, u32[]{:S(2)}) collective-permute-start(bf16[32,2048]{1,0:T(8,128)(2,1)S(1)} %collective-permute-done.1.t2), channel_id=1, source_target_pairs={{0,1},{1,0},{2,3},{3,2},{4,5},{5,4},{6,7},{7,6},{8,9},{9,8},{10,11... | collective-permute-start | bytes 393224 | tf_op jit(solution)/shard_map/ppermute | solution.py:18
  7.4 1.2 %copy-start = (bf16[2048,256]{1,0:T(8,128)(2,1)S(1)}, bf16[2048,256]{1,0:T(8,128)(2,1)}, u32[]{:S(2)}) copy-start(bf16[2048,256]{1,0:T(8,128)(2,1)} %refs_3_.1) | copy-start | bytes 3145732
  8.6 1.2 %copy-start.1 = (bf16[256,2048]{1,0:T(8,128)(2,1)S(1)}, bf16[256,2048]{1,0:T(8,128)(2,1)}, u32[]{:S(2)}) copy-start(bf16[256,2048]{1,0:T(8,128)(2,1)} %refs_11_.1) | copy-start | bytes 3145732
  9.8 1.0 %copy-start.2 = (bf16[2048,128]{1,0:T(8,128)(2,1)S(1)}, bf16[2048,128]{1,0:T(8,128)(2,1)}, u32[]{:S(2)}) copy-start(bf16[2048,128]{1,0:T(8,128)(2,1)} %refs_1_.1) | copy-start | bytes 1572868
  10.9 1.0 %copy-start.3 = (bf16[2048,128]{1,0:T(8,128)(2,1)S(1)}, bf16[2048,128]{1,0:T(8,128)(2,1)}, u32[]{:S(2)}) copy-start(bf16[2048,128]{1,0:T(8,128)(2,1)} %refs_2_.1) | copy-start | bytes 1572868
  11.9 1.0 %copy-start.4 = (bf16[2048,128]{1,0:T(8,128)(2,1)S(1)}, bf16[2048,128]{1,0:T(8,128)(2,1)}, u32[]{:S(2)}) copy-start(bf16[2048,128]{1,0:T(8,128)(2,1)} %refs_4_.1) | copy-start | bytes 1572868
  12.9 1.0 %copy-start.5 = (bf16[2048,128]{1,0:T(8,128)(2,1)S(1)}, bf16[2048,128]{1,0:T(8,128)(2,1)}, u32[]{:S(2)}) copy-start(bf16[2048,128]{1,0:T(8,128)(2,1)} %refs_5_.1) | copy-start | bytes 1572868
  14.0 1.0 %copy-start.6 = (bf16[128,2048]{1,0:T(8,128)(2,1)S(1)}, bf16[128,2048]{1,0:T(8,128)(2,1)}, u32[]{:S(2)}) copy-start(bf16[128,2048]{1,0:T(8,128)(2,1)} %refs_10_.1) | copy-start | bytes 1572868
  15.0 0.9 %copy-start.7 = (bf16[32,2048]{1,0:T(8,128)(2,1)S(1)}, bf16[32,2048]{1,0:T(8,128)(2,1)}, u32[]{:S(2)}) copy-start(bf16[32,2048]{1,0:T(8,128)(2,1)} %refs_0_.1) | copy-start | bytes 393220
  15.9 0.7 %copy-start.8 = (f32[31,128]{1,0:T(8,128)S(1)}, f32[31,128]{1,0:T(8,128)}, u32[]{:S(2)}) copy-start(f32[31,128]{1,0:T(8,128)} %refs_6_.1) | copy-start | bytes 47620
  19.6 7.1 %collective-permute-start.8 = (bf16[144,256]{1,0:T(8,128)(2,1)S(1)}, bf16[144,256]{1,0:T(8,128)(2,1)S(1)}, u32[]{:S(2)}, u32[]{:S(2)}) collective-permute-start(bf16[144,256]{1,0:T(8,128)(2,1)S(1)} %get-tuple-element.28.refs_1_), channel_id=1, source_target_pairs={{0,24},{4,28},{8,16},{12,20},{16,8},{20,12},{24,0},{28,4},{1,25},{... | collective-permute-start | bytes 221192 | tf_op jit(solution)/shard_map/ppermute | solution.py:18
  23.4 5.9 %collective-permute-start.4 = (bf16[144,256]{1,0:T(8,128)(2,1)S(1)}, bf16[144,256]{1,0:T(8,128)(2,1)S(1)}, u32[]{:S(2)}, u32[]{:S(2)}) collective-permute-start(bf16[144,256]{1,0:T(8,128)(2,1)S(1)} %get-tuple-element.28.refs_1_), channel_id=1, source_target_pairs={{0,8},{4,12},{8,0},{12,4},{16,24},{20,28},{24,16},{28,20},{1,9},{5... | collective-permute-start | bytes 221192 | tf_op jit(solution)/shard_map/ppermute | solution.py:18
  23.4 7.5 %collective-permute-start.6 = (bf16[144,256]{1,0:T(8,128)(2,1)S(1)}, bf16[144,256]{1,0:T(8,128)(2,1)S(1)}, u32[]{:S(2)}, u32[]{:S(2)}) collective-permute-start(bf16[144,256]{1,0:T(8,128)(2,1)S(1)} %get-tuple-element.28.refs_1_), channel_id=1, source_target_pairs={{0,16},{4,20},{8,24},{12,28},{16,0},{20,4},{24,8},{28,12},{1,17},{... | collective-permute-start | bytes 221192 | tf_op jit(solution)/shard_map/ppermute | solution.py:18
  24.1 7.8 %collective-permute-start.3 = (bf16[144,256]{1,0:T(8,128)(2,1)S(1)}, bf16[144,256]{1,0:T(8,128)(2,1)S(1)}, u32[]{:S(2)}, u32[]{:S(2)}) collective-permute-start(bf16[144,256]{1,0:T(8,128)(2,1)S(1)} %get-tuple-element.28.refs_1_), channel_id=1, source_target_pairs={{0,4},{4,0},{8,12},{12,8},{16,20},{20,16},{24,28},{28,24},{1,5},{5... | collective-permute-start | bytes 221192 | tf_op jit(solution)/shard_map/ppermute | solution.py:18
  26.6 5.3 %collective-permute-start.9 = (bf16[144,256]{1,0:T(8,128)(2,1)S(1)}, bf16[144,256]{1,0:T(8,128)(2,1)S(1)}, u32[]{:S(2)}, u32[]{:S(2)}) collective-permute-start(bf16[144,256]{1,0:T(8,128)(2,1)S(1)} %collective-permute-done.8.refs_7_), channel_id=1, source_target_pairs={{0,4},{4,0},{8,12},{12,8},{16,20},{20,16},{24,28},{28,24},{1,5},{5... | collective-permute-start | bytes 221192 | tf_op jit(solution)/shard_map/ppermute | solution.py:18
  29.3 5.1 %collective-permute-start.5 = (bf16[144,256]{1,0:T(8,128)(2,1)S(1)}, bf16[144,256]{1,0:T(8,128)(2,1)S(1)}, u32[]{:S(2)}, u32[]{:S(2)}) collective-permute-start(bf16[144,256]{1,0:T(8,128)(2,1)S(1)} %collective-permute-done.4.refs_3_), channel_id=1, source_target_pairs={{0,4},{4,0},{8,12},{12,8},{16,20},{20,16},{24,28},{28,24},{1,5},{5... | collective-permute-start | bytes 221192 | tf_op jit(solution)/shard_map/ppermute | solution.py:18
  31.0 7.4 %collective-permute-start.7 = (bf16[144,256]{1,0:T(8,128)(2,1)S(1)}, bf16[144,256]{1,0:T(8,128)(2,1)S(1)}, u32[]{:S(2)}, u32[]{:S(2)}) collective-permute-start(bf16[144,256]{1,0:T(8,128)(2,1)S(1)} %collective-permute-done.6.refs_5_), channel_id=1, source_target_pairs={{0,4},{4,0},{8,12},{12,8},{16,20},{20,16},{24,28},{28,24},{1,5},{5... | collective-permute-start | bytes 221192 | tf_op jit(solution)/shard_map/ppermute | solution.py:18
  34.8 3.6 %collective-permute-start.11 = (f32[8,128]{1,0:T(8,128)S(1)}, f32[8,128]{1,0:T(8,128)S(1)}, u32[]{:S(2)}, u32[]{:S(2)}) collective-permute-start(f32[8,128]{1,0:T(8,128)S(1)} %get-tuple-element.32.refs_10_), channel_id=1, source_target_pairs={{0,2},{1,3},{2,0},{3,1},{4,6},{5,7},{6,4},{7,5},{8,10},{9,11},{10,... | collective-permute-start | bytes 12296 | tf_op jit(solution)/shard_map/ppermute | solution.py:18
  36.3 2.1 %collective-permute-start.10 = (f32[8,128]{1,0:T(8,128)S(1)}, f32[8,128]{1,0:T(8,128)S(1)}, u32[]{:S(2)}, u32[]{:S(2)}) collective-permute-start(f32[8,128]{1,0:T(8,128)S(1)} %get-tuple-element.32.refs_10_), channel_id=1, source_target_pairs={{0,1},{1,0},{2,3},{3,2},{4,5},{5,4},{6,7},{7,6},{8,9},{9,8},{10,11... | collective-permute-start | bytes 12296 | tf_op jit(solution)/shard_map/ppermute | solution.py:18
  38.4 1.2 %collective-permute-start.12 = (f32[8,128]{1,0:T(8,128)S(1)}, f32[8,128]{1,0:T(8,128)S(1)}, u32[]{:S(2)}, u32[]{:S(2)}) collective-permute-start(f32[8,128]{1,0:T(8,128)S(1)} %collective-permute-done.11.refs_12_), channel_id=1, source_target_pairs={{0,1},{1,0},{2,3},{3,2},{4,5},{5,4},{6,7},{7,6},{8,9},{9,8},{10,11... | collective-permute-start | bytes 12296 | tf_op jit(solution)/shard_map/ppermute | solution.py:18
  43.9 1.6 %collective-permute-start.13 = (bf16[64,2048]{1,0:T(8,128)(2,1)S(1)}, bf16[64,2048]{1,0:T(8,128)(2,1)S(1)}, u32[]{:S(2)}, u32[]{:S(2)}) collective-permute-start(bf16[64,2048]{1,0:T(8,128)(2,1)S(1)} %get-tuple-element.37), channel_id=1, source_target_pairs={{0,1},{1,0},{2,3},{3,2},{4,5},{5,4},{6,7},{7,6},{8,9},{9,8},{10,11... | collective-permute-start | bytes 786440 | tf_op jit(solution)/shard_map/ppermute | solution.py:18
  45.5 5.6 %collective-permute-start.14 = (bf16[32,2048]{1,0:T(8,128)(2,1)S(1)}, bf16[32,2048]{1,0:T(8,128)(2,1)S(1)}, u32[]{:S(2)}, u32[]{:S(2)}) collective-permute-start(bf16[32,2048]{1,0:T(8,128)(2,1)S(1)} %fusion), channel_id=1, source_target_pairs={{0,2},{1,3},{2,0},{3,1},{4,6},{5,7},{6,4},{7,5},{8,10},{9,11},{10,... | collective-permute-start | bytes 393224 | tf_op jit(solution)/shard_map/ppermute | solution.py:18
  (2 other events, 1.3 us)

commit v3 on v2

--- a/solution.py
+++ b/solution.py
@@ -253,8 +253,12 @@
     off = jnp.pad(jnp.transpose(key_offsets), ((0, 16 - per), (0, 0)))
     by_core = swap(tokens, "tp", 1)
     by_chip = swap(tokens, "tp", 2)
-    by_both = swap(by_chip, "tp", 1)
     in_vmem = pl.BlockSpec(memory_space=pltpu.VMEM)
+    sources = [
+        tokens, conv_input, conv_gate, query_weight, key_weight, value_weight, conv_taps,
+        conv_gain.reshape(1, ch), off, stick_gain.reshape(per, HEAD_DIM),
+        conv_output, stick_output,
+    ]
     tok, conv_w, q_w, kv_w, taps, c_gain, off, s_gain, out_w = pl.pallas_call(
         load_kernel,
         out_shape=[
@@ -276,11 +280,9 @@
         scratch_shapes=[pltpu.SemaphoreType.DMA((12,))],
         cost_estimate=pl.CostEstimate(flops=10**9, transcendentals=0, bytes_accessed=5 * 10**6),
         compiler_params=pltpu.CompilerParams(vmem_limit_bytes=2**21),
-    )(
-        tokens, conv_input, conv_gate, query_weight, key_weight, value_weight, conv_taps,
-        conv_gain.reshape(1, ch), off, stick_gain.reshape(per, HEAD_DIM),
-        conv_output, stick_output,
-    )
+    )(*[pltpu.with_memory_space_constraint(source, pltpu.HBM) for source in sources])
+    by_chip, tok = lax.optimization_barrier((by_chip, tok))
+    by_both = swap(by_chip, "tp", 1)
     pay, qs, blend = call(
         project_kernel,
         [((n + 16, 2 * kv), bf16), ((per * n, HEAD_DIM), bf16), ((n, ch), bf16)],
@@ -291,12 +293,12 @@
     field_shapes = [((n, ch), f32), ((8, n), f32)]
     wide = [pltpu.VMEM((n + 32, ch), f32)]
     if blocks == 8:
+        z2 = swap(pay, "sp", 2)
         z6 = swap(pay, "sp", 6)
-        z2 = swap(pay, "sp", 2)
         z4 = swap(pay, "sp", 4)
         x1 = swap(pay, "sp", 1)
+        x3 = swap(z2, "sp", 1)
         x7 = swap(z6, "sp", 1)
-        x3 = swap(z2, "sp", 1)
         x5 = swap(z4, "sp", 1)
         pays = [pay, x1, z2, x3, z4, x5, z6, x7]
         conv_args = [x1, x3, x7, blend, taps]

time: 52.4 us -> 41 us (0.78)
  local copies, waits for them, and re-layouts: 11.3 us -> 1.25 us
  Pallas kernels: 6.15 us -> 7.76 us
  waiting for transfers between devices: 16.8 us -> 15.2 us
  starting transfers between devices: 16.8 us -> 15.8 us
    unnamed x22 -> x0, local copies, waits for them, and re-layouts: 10.6 us -> none
    pallas_call x1, Pallas kernels: 0.89 us -> 2.52 us  [shards(): pl.pallas_call(load_kernel, out_shape=[pltpu.VMEM(shape, dtype) for shape...]
    ppermute x15, waiting for transfers between devices: 16.8 us -> 15.2 us  [swap(): return lax.ppermute(value, axis, [(i, i ^ by) for i in range(count)])]
    ppermute x15, starting transfers between devices: 16.8 us -> 15.8 us  [swap(): return lax.ppermute(value, axis, [(i, i ^ by) for i in range(count)])]
    pad x1, local copies, waits for them, and re-layouts: 0.66 us -> 1.25 us  [shards(): off = jnp.pad(jnp.transpose(key_offsets), ((0, 16 - per), (0, 0)))]
  transfers between devices with their start and end apart: 15 -> 15, of which waited for: 8 -> 8; matrix products, arithmetic and copies ran while one was open for 1% -> 3% of each run, Pallas kernels for 2% -> 7%
where the time goes in v3:
time: 41 us; the launch traced here: 40.8 us
  starting transfers between devices  15.8 us (39%)
  waiting for transfers between devices  15.2 us (37%)
  Pallas kernels  7.76 us (19%)
  local copies, waits for them, and re-layouts  1.25 us (3%)
  other arithmetic  0.77 us (2%)
    ppermute x15, starting transfers between devices, swap(): return lax.ppermute(value, axis, [(i, i ^ by) for i in range(count)])  15.8 us
    ppermute x15, waiting for transfers between devices, swap(): return lax.ppermute(value, axis, [(i, i ^ by) for i in range(count)])  15.2 us
    pallas_call x3, Pallas kernels, call(): pl.pallas_call(body, out_shape=[pltpu.VMEM(shape, dtype) for shape, dtype...  5.24 us
    pallas_call x1, Pallas kernels, shards(): pl.pallas_call(load_kernel, out_shape=[pltpu.VMEM(shape, dtype) for shape...  2.52 us
    pad x1, local copies, waits for them, and re-layouts, shards(): off = jnp.pad(jnp.transpose(key_offsets), ((0, 16 - per), (0, 0)))  1.25 us
  transfers between devices with their start and end apart: 15, of which 8 were waited for; matrix products, arithmetic and copies ran while one was open for 3% of the time, Pallas kernels for 7%

profile of v3, /device:TPU:0, one launch (start us, length us, event | category | flops | bytes accessed | tf_op | source)
XLA Modules:
  0.0 40.8 jit_solution(5111047482572302393)
XLA Ops:
  0.0 3.0 %collective-permute-start = (bf16[32,2048]{1,0:T(8,128)(2,1)}, bf16[32,2048]{1,0:T(8,128)(2,1)S(1)}, u32[]{:S(2)}, u32[]{:S(2)}) collective-permute-start(bf16[32,2048]{1,0:T(8,128)(2,1)} %refs_0_.1), channel_id=1, source_target_pairs={{0,2},{1,3},{2,0},{3,1},{4,6},{5,7},{6,4},{7,5},{8,10},{9,11},{10,... | collective-permute-start | bytes 393224 | tf_op jit(solution)/shard_map/ppermute | solution.py:18
  3.0 1.3 %pad.4.refs_8_ = bf16[16,128]{1,0:T(8,128)(2,1)} pad(bf16[2,128]{1,0:T(2,128)(2,1)} %bitcast.5, bf16[]{:T(256)} %constant.2.clone.1), padding=0_14x0_0 | pad | bytes 4610 | tf_op jit(solution)/shard_map/jit(_pad)/pad | solution.py:253
  4.3 2.5 %shard_map.118 = (bf16[32,2048]{1,0:T(8,128)(2,1)S(1)}, bf16[2048,256]{1,0:T(8,128)(2,1)S(1)}, bf16[2048,256]{1,0:T(8,128)(2,1)S(1)}, bf16[2048,256]{1,0:T(8,128...) custom-call(bf16[32,2048]{1,0:T(8,128)(2,1)} %refs_0_.1, ...), custom_call_target="tpu_custom_call" | custom-call | flops 1000000000 | bytes 5000000 | tf_op jit(solution)/shard_map/pallas_call | solution.py:262
  6.8 0.6 %collective-permute-start.2 = (bf16[32,2048]{1,0:T(8,128)(2,1)S(1)}, bf16[32,2048]{1,0:T(8,128)(2,1)S(1)}, u32[]{:S(2)}, u32[]{:S(2)}) collective-permute-start(bf16[32,2048]{1,0:T(8,128)(2,1)S(1)} %collective-permute-done.t2), channel_id=1, source_target_pairs={{0,1},{1,0},{2,3},{3,2},{4,5},{5,4},{6,7},{7,6},{8,9},{9,8},{10,11... | collective-permute-start | bytes 393224 | tf_op jit(solution)/shard_map/ppermute | solution.py:18
  7.4 1.0 %collective-permute-done.2.t3 = bf16[32,2048]{1,0:T(8,128)(2,1)S(1)} collective-permute-done((bf16[32,2048]{1,0:T(8,128)(2,1)S(1)}, bf16[32,2048]{1,0:T(8,128)(2,1)S(1)}, u32[]{:S(2)}, u32[]{:S(2)}) %collective-permute-start.2) | collective-permute-done | bytes 131104 | tf_op jit(solution)/shard_map/ppermute | solution.py:18
  8.3 0.6 %shard_map.119 = (bf16[144,256]{1,0:T(8,128)(2,1)S(1)}, bf16[256,128]{1,0:T(8,128)(2,1)S(1)}, bf16[128,128]{1,0:T(8,128)(2,1)S(1)}) custom-call(bf16[32,2048]{1,0:T(8,128)(2,1)S(1)} %get-tuple-element.25.t0, bf16[32,2048]{1,0:T(8,128)(2,1)S(1)} %collective-permute-done.1.t1, bf16[32,2048]{1,0:T(8,128)(2,1)S(1)} %collective-permute-done.t2, ...), custom_call_target="tpu_custom_call" | custom-call | flops 402653184 | tf_op jit(solution)/shard_map/pallas_call | solution.py:220
  9.0 3.7 %collective-permute-start.8 = (bf16[144,256]{1,0:T(8,128)(2,1)S(1)}, bf16[144,256]{1,0:T(8,128)(2,1)S(1)}, u32[]{:S(2)}, u32[]{:S(2)}) collective-permute-start(bf16[144,256]{1,0:T(8,128)(2,1)S(1)} %get-tuple-element.32.refs_1_), channel_id=1, source_target_pairs={{0,24},{4,28},{8,16},{12,20},{16,8},{20,12},{24,0},{28,4},{1,25},{... | collective-permute-start | bytes 221192 | tf_op jit(solution)/shard_map/ppermute | solution.py:18
  12.6 0.8 %collective-permute-start.6 = (bf16[144,256]{1,0:T(8,128)(2,1)S(1)}, bf16[144,256]{1,0:T(8,128)(2,1)S(1)}, u32[]{:S(2)}, u32[]{:S(2)}) collective-permute-start(bf16[144,256]{1,0:T(8,128)(2,1)S(1)} %get-tuple-element.32.refs_1_), channel_id=1, source_target_pairs={{0,16},{4,20},{8,24},{12,28},{16,0},{20,4},{24,8},{28,12},{1,17},{... | collective-permute-start | bytes 221192 | tf_op jit(solution)/shard_map/ppermute | solution.py:18
  13.4 1.5 %collective-permute-start.3 = (bf16[144,256]{1,0:T(8,128)(2,1)S(1)}, bf16[144,256]{1,0:T(8,128)(2,1)S(1)}, u32[]{:S(2)}, u32[]{:S(2)}) collective-permute-start(bf16[144,256]{1,0:T(8,128)(2,1)S(1)} %get-tuple-element.32.refs_1_), channel_id=1, source_target_pairs={{0,4},{4,0},{8,12},{12,8},{16,20},{20,16},{24,28},{28,24},{1,5},{5... | collective-permute-start | bytes 221192 | tf_op jit(solution)/shard_map/ppermute | solution.py:18
  14.9 1.1 %collective-permute-done.8.refs_7_ = bf16[144,256]{1,0:T(8,128)(2,1)S(1)} collective-permute-done((bf16[144,256]{1,0:T(8,128)(2,1)S(1)}, bf16[144,256]{1,0:T(8,128)(2,1)S(1)}, u32[]{:S(2)}, u32[]{:S(2)}) %collective-permute-start.8) | collective-permute-done | bytes 73760 | tf_op jit(solution)/shard_map/ppermute | solution.py:18
  16.0 1.5 %collective-permute-start.9 = (bf16[144,256]{1,0:T(8,128)(2,1)S(1)}, bf16[144,256]{1,0:T(8,128)(2,1)S(1)}, u32[]{:S(2)}, u32[]{:S(2)}) collective-permute-start(bf16[144,256]{1,0:T(8,128)(2,1)S(1)} %collective-permute-done.8.refs_7_), channel_id=1, source_target_pairs={{0,4},{4,0},{8,12},{12,8},{16,20},{20,16},{24,28},{28,24},{1,5},{5... | collective-permute-start | bytes 221192 | tf_op jit(solution)/shard_map/ppermute | solution.py:18
  17.5 1.2 %collective-permute-done.4.refs_3_ = bf16[144,256]{1,0:T(8,128)(2,1)S(1)} collective-permute-done((bf16[144,256]{1,0:T(8,128)(2,1)S(1)}, bf16[144,256]{1,0:T(8,128)(2,1)S(1)}, u32[]{:S(2)}, u32[]{:S(2)}) %collective-permute-start.4) | collective-permute-done | bytes 73760 | tf_op jit(solution)/shard_map/ppermute | solution.py:18
  18.7 1.5 %collective-permute-start.5 = (bf16[144,256]{1,0:T(8,128)(2,1)S(1)}, bf16[144,256]{1,0:T(8,128)(2,1)S(1)}, u32[]{:S(2)}, u32[]{:S(2)}) collective-permute-start(bf16[144,256]{1,0:T(8,128)(2,1)S(1)} %collective-permute-done.4.refs_3_), channel_id=1, source_target_pairs={{0,4},{4,0},{8,12},{12,8},{16,20},{20,16},{24,28},{28,24},{1,5},{5... | collective-permute-start | bytes 221192 | tf_op jit(solution)/shard_map/ppermute | solution.py:18
  20.2 0.8 %collective-permute-start.7 = (bf16[144,256]{1,0:T(8,128)(2,1)S(1)}, bf16[144,256]{1,0:T(8,128)(2,1)S(1)}, u32[]{:S(2)}, u32[]{:S(2)}) collective-permute-start(bf16[144,256]{1,0:T(8,128)(2,1)S(1)} %collective-permute-done.6.refs_5_), channel_id=1, source_target_pairs={{0,4},{4,0},{8,12},{12,8},{16,20},{20,16},{24,28},{28,24},{1,5},{5... | collective-permute-start | bytes 221192 | tf_op jit(solution)/shard_map/ppermute | solution.py:18
  21.0 2.4 %collective-permute-done.5.p3.refs_4_ = bf16[144,256]{1,0:T(8,128)(2,1)S(1)} collective-permute-done((bf16[144,256]{1,0:T(8,128)(2,1)S(1)}, bf16[144,256]{1,0:T(8,128)(2,1)S(1)}, u32[]{:S(2)}, u32[]{:S(2)}) %collective-permute-start.5) | collective-permute-done | bytes 73760 | tf_op jit(solution)/shard_map/ppermute | solution.py:18
  23.4 0.4 shard_map.120
  23.7 1.1 %collective-permute-start.11 = (f32[8,128]{1,0:T(8,128)S(1)}, f32[8,128]{1,0:T(8,128)S(1)}, u32[]{:S(2)}, u32[]{:S(2)}) collective-permute-start(f32[8,128]{1,0:T(8,128)S(1)} %get-tuple-element.36.refs_10_), channel_id=1, source_target_pairs={{0,2},{1,3},{2,0},{3,1},{4,6},{5,7},{6,4},{7,5},{8,10},{9,11},{10,... | collective-permute-start | bytes 12296 | tf_op jit(solution)/shard_map/ppermute | solution.py:18
  24.9 2.5 %collective-permute-done.11.refs_12_ = f32[8,128]{1,0:T(8,128)S(1)} collective-permute-done((f32[8,128]{1,0:T(8,128)S(1)}, f32[8,128]{1,0:T(8,128)S(1)}, u32[]{:S(2)}, u32[]{:S(2)}) %collective-permute-start.11) | collective-permute-done | bytes 4128 | tf_op jit(solution)/shard_map/ppermute | solution.py:18
  27.4 1.2 %collective-permute-done.12.refs_13_ = f32[8,128]{1,0:T(8,128)S(1)} collective-permute-done((f32[8,128]{1,0:T(8,128)S(1)}, f32[8,128]{1,0:T(8,128)S(1)}, u32[]{:S(2)}, u32[]{:S(2)}) %collective-permute-start.12) | collective-permute-done | bytes 4128 | tf_op jit(solution)/shard_map/ppermute | solution.py:18
  28.6 4.3 %shard_map.121 = (f32[32,2048]{1,0:T(8,128)S(1)}, f32[32,2048]{1,0:T(8,128)S(1)}, bf16[64,2048]{1,0:T(8,128)(2,1)S(1)}) custom-call(bf16[256,128]{1,0:T(8,128)(2,1)S(1)} %get-tuple-element.31.refs_0_, bf16[144,256]{1,0:T(8,128)(2,1)S(1)} %get-tuple-element.32.refs_1_, bf16[144,256]{1,0:T(8,128)(2,1)S(1)} %collective-permute-done.3.p1.refs_2_, ...), custom_call_target="tpu_custom_call" | custom-call | flops 201326592 | tf_op jit(solution)/shard_map/pallas_call | solution.py:220
  33.1 1.4 %collective-permute-done.13 = bf16[64,2048]{1,0:T(8,128)(2,1)S(1)} collective-permute-done((bf16[64,2048]{1,0:T(8,128)(2,1)S(1)}, bf16[64,2048]{1,0:T(8,128)(2,1)S(1)}, u32[]{:S(2)}, u32[]{:S(2)}) %collective-permute-start.13) | collective-permute-done | bytes 262176 | tf_op jit(solution)/shard_map/ppermute | solution.py:18
  34.5 1.2 %collective-permute-start.14 = (bf16[32,2048]{1,0:T(8,128)(2,1)S(1)}, bf16[32,2048]{1,0:T(8,128)(2,1)S(1)}, u32[]{:S(2)}, u32[]{:S(2)}) collective-permute-start(bf16[32,2048]{1,0:T(8,128)(2,1)S(1)} %fusion), channel_id=1, source_target_pairs={{0,2},{1,3},{2,0},{3,1},{4,6},{5,7},{6,4},{7,5},{8,10},{9,11},{10,... | collective-permute-start | bytes 393224 | tf_op jit(solution)/shard_map/ppermute | solution.py:18
  35.7 4.5 %collective-permute-done.14 = bf16[32,2048]{1,0:T(8,128)(2,1)S(1)} collective-permute-done((bf16[32,2048]{1,0:T(8,128)(2,1)S(1)}, bf16[32,2048]{1,0:T(8,128)(2,1)S(1)}, u32[]{:S(2)}, u32[]{:S(2)}) %collective-permute-start.14) | collective-permute-done | bytes 131104 | tf_op jit(solution)/shard_map/ppermute | solution.py:18
  40.1 0.7 %fusion.2 = bf16[32,2048]{1,0:T(8,128)(2,1)} fusion(f32[32,2048]{1,0:T(8,128)S(1)} %get-tuple-element.40, f32[64,2048]{1,0:T(8,128)S(1)} %convert_element_type.14, bf16[32,2048]{1,0:T(8,128)(2,1)S(1)} %collective-permute-done.14), kind=kLoop, calls=%fused_computation.4 | loop fusion | flops 262144 | bytes 786432 | tf_op jit(solution)/shard_map/convert_element_type | solution.py:331
  (14 shorter events, 0.3 us)
Async XLA Ops:
  0.0 6.8 %collective-permute-start = (bf16[32,2048]{1,0:T(8,128)(2,1)}, bf16[32,2048]{1,0:T(8,128)(2,1)S(1)}, u32[]{:S(2)}, u32[]{:S(2)}) collective-permute-start(bf16[32,2048]{1,0:T(8,128)(2,1)} %refs_0_.1), channel_id=1, source_target_pairs={{0,2},{1,3},{2,0},{3,1},{4,6},{5,7},{6,4},{7,5},{8,10},{9,11},{10,... | collective-permute-start | bytes 393224 | tf_op jit(solution)/shard_map/ppermute | solution.py:18
  3.0 4.4 %collective-permute-start.1 = (bf16[32,2048]{1,0:T(8,128)(2,1)}, bf16[32,2048]{1,0:T(8,128)(2,1)S(1)}, u32[]{:S(2)}, u32[]{:S(2)}) collective-permute-start(bf16[32,2048]{1,0:T(8,128)(2,1)} %refs_0_.1), channel_id=1, source_target_pairs={{0,1},{1,0},{2,3},{3,2},{4,5},{5,4},{6,7},{7,6},{8,9},{9,8},{10,11... | collective-permute-start | bytes 393224 | tf_op jit(solution)/shard_map/ppermute | solution.py:18
  6.8 1.6 %collective-permute-start.2 = (bf16[32,2048]{1,0:T(8,128)(2,1)S(1)}, bf16[32,2048]{1,0:T(8,128)(2,1)S(1)}, u32[]{:S(2)}, u32[]{:S(2)}) collective-permute-start(bf16[32,2048]{1,0:T(8,128)(2,1)S(1)} %collective-permute-done.t2), channel_id=1, source_target_pairs={{0,1},{1,0},{2,3},{3,2},{4,5},{5,4},{6,7},{7,6},{8,9},{9,8},{10,11... | collective-permute-start | bytes 393224 | tf_op jit(solution)/shard_map/ppermute | solution.py:18
  9.0 7.1 %collective-permute-start.8 = (bf16[144,256]{1,0:T(8,128)(2,1)S(1)}, bf16[144,256]{1,0:T(8,128)(2,1)S(1)}, u32[]{:S(2)}, u32[]{:S(2)}) collective-permute-start(bf16[144,256]{1,0:T(8,128)(2,1)S(1)} %get-tuple-element.32.refs_1_), channel_id=1, source_target_pairs={{0,24},{4,28},{8,16},{12,20},{16,8},{20,12},{24,0},{28,4},{1,25},{... | collective-permute-start | bytes 221192 | tf_op jit(solution)/shard_map/ppermute | solution.py:18
  12.6 6.1 %collective-permute-start.4 = (bf16[144,256]{1,0:T(8,128)(2,1)S(1)}, bf16[144,256]{1,0:T(8,128)(2,1)S(1)}, u32[]{:S(2)}, u32[]{:S(2)}) collective-permute-start(bf16[144,256]{1,0:T(8,128)(2,1)S(1)} %get-tuple-element.32.refs_1_), channel_id=1, source_target_pairs={{0,8},{4,12},{8,0},{12,4},{16,24},{20,28},{24,16},{28,20},{1,9},{5... | collective-permute-start | bytes 221192 | tf_op jit(solution)/shard_map/ppermute | solution.py:18
  12.6 7.6 %collective-permute-start.6 = (bf16[144,256]{1,0:T(8,128)(2,1)S(1)}, bf16[144,256]{1,0:T(8,128)(2,1)S(1)}, u32[]{:S(2)}, u32[]{:S(2)}) collective-permute-start(bf16[144,256]{1,0:T(8,128)(2,1)S(1)} %get-tuple-element.32.refs_1_), channel_id=1, source_target_pairs={{0,16},{4,20},{8,24},{12,28},{16,0},{20,4},{24,8},{28,12},{1,17},{... | collective-permute-start | bytes 221192 | tf_op jit(solution)/shard_map/ppermute | solution.py:18
  13.4 7.5 %collective-permute-start.3 = (bf16[144,256]{1,0:T(8,128)(2,1)S(1)}, bf16[144,256]{1,0:T(8,128)(2,1)S(1)}, u32[]{:S(2)}, u32[]{:S(2)}) collective-permute-start(bf16[144,256]{1,0:T(8,128)(2,1)S(1)} %get-tuple-element.32.refs_1_), channel_id=1, source_target_pairs={{0,4},{4,0},{8,12},{12,8},{16,20},{20,16},{24,28},{28,24},{1,5},{5... | collective-permute-start | bytes 221192 | tf_op jit(solution)/shard_map/ppermute | solution.py:18
  16.0 4.9 %collective-permute-start.9 = (bf16[144,256]{1,0:T(8,128)(2,1)S(1)}, bf16[144,256]{1,0:T(8,128)(2,1)S(1)}, u32[]{:S(2)}, u32[]{:S(2)}) collective-permute-start(bf16[144,256]{1,0:T(8,128)(2,1)S(1)} %collective-permute-done.8.refs_7_), channel_id=1, source_target_pairs={{0,4},{4,0},{8,12},{12,8},{16,20},{20,16},{24,28},{28,24},{1,5},{5... | collective-permute-start | bytes 221192 | tf_op jit(solution)/shard_map/ppermute | solution.py:18
  18.7 4.7 %collective-permute-start.5 = (bf16[144,256]{1,0:T(8,128)(2,1)S(1)}, bf16[144,256]{1,0:T(8,128)(2,1)S(1)}, u32[]{:S(2)}, u32[]{:S(2)}) collective-permute-start(bf16[144,256]{1,0:T(8,128)(2,1)S(1)} %collective-permute-done.4.refs_3_), channel_id=1, source_target_pairs={{0,4},{4,0},{8,12},{12,8},{16,20},{20,16},{24,28},{28,24},{1,5},{5... | collective-permute-start | bytes 221192 | tf_op jit(solution)/shard_map/ppermute | solution.py:18
  20.2 7.2 %collective-permute-start.7 = (bf16[144,256]{1,0:T(8,128)(2,1)S(1)}, bf16[144,256]{1,0:T(8,128)(2,1)S(1)}, u32[]{:S(2)}, u32[]{:S(2)}) collective-permute-start(bf16[144,256]{1,0:T(8,128)(2,1)S(1)} %collective-permute-done.6.refs_5_), channel_id=1, source_target_pairs={{0,4},{4,0},{8,12},{12,8},{16,20},{20,16},{24,28},{28,24},{1,5},{5... | collective-permute-start | bytes 221192 | tf_op jit(solution)/shard_map/ppermute | solution.py:18
  23.7 3.6 %collective-permute-start.11 = (f32[8,128]{1,0:T(8,128)S(1)}, f32[8,128]{1,0:T(8,128)S(1)}, u32[]{:S(2)}, u32[]{:S(2)}) collective-permute-start(f32[8,128]{1,0:T(8,128)S(1)} %get-tuple-element.36.refs_10_), channel_id=1, source_target_pairs={{0,2},{1,3},{2,0},{3,1},{4,6},{5,7},{6,4},{7,5},{8,10},{9,11},{10,... | collective-permute-start | bytes 12296 | tf_op jit(solution)/shard_map/ppermute | solution.py:18
  24.9 2.5 %collective-permute-start.10 = (f32[8,128]{1,0:T(8,128)S(1)}, f32[8,128]{1,0:T(8,128)S(1)}, u32[]{:S(2)}, u32[]{:S(2)}) collective-permute-start(f32[8,128]{1,0:T(8,128)S(1)} %get-tuple-element.36.refs_10_), channel_id=1, source_target_pairs={{0,1},{1,0},{2,3},{3,2},{4,5},{5,4},{6,7},{7,6},{8,9},{9,8},{10,11... | collective-permute-start | bytes 12296 | tf_op jit(solution)/shard_map/ppermute | solution.py:18
  27.4 1.2 %collective-permute-start.12 = (f32[8,128]{1,0:T(8,128)S(1)}, f32[8,128]{1,0:T(8,128)S(1)}, u32[]{:S(2)}, u32[]{:S(2)}) collective-permute-start(f32[8,128]{1,0:T(8,128)S(1)} %collective-permute-done.11.refs_12_), channel_id=1, source_target_pairs={{0,1},{1,0},{2,3},{3,2},{4,5},{5,4},{6,7},{7,6},{8,9},{9,8},{10,11... | collective-permute-start | bytes 12296 | tf_op jit(solution)/shard_map/ppermute | solution.py:18
  32.8 1.6 %collective-permute-start.13 = (bf16[64,2048]{1,0:T(8,128)(2,1)S(1)}, bf16[64,2048]{1,0:T(8,128)(2,1)S(1)}, u32[]{:S(2)}, u32[]{:S(2)}) collective-permute-start(bf16[64,2048]{1,0:T(8,128)(2,1)S(1)} %get-tuple-element.41), channel_id=1, source_target_pairs={{0,1},{1,0},{2,3},{3,2},{4,5},{5,4},{6,7},{7,6},{8,9},{9,8},{10,11... | collective-permute-start | bytes 786440 | tf_op jit(solution)/shard_map/ppermute | solution.py:18
  34.5 5.6 %collective-permute-start.14 = (bf16[32,2048]{1,0:T(8,128)(2,1)S(1)}, bf16[32,2048]{1,0:T(8,128)(2,1)S(1)}, u32[]{:S(2)}, u32[]{:S(2)}) collective-permute-start(bf16[32,2048]{1,0:T(8,128)(2,1)S(1)} %fusion), channel_id=1, source_target_pairs={{0,2},{1,3},{2,0},{3,1},{4,6},{5,7},{6,4},{7,5},{8,10},{9,11},{10,... | collective-permute-start | bytes 393224 | tf_op jit(solution)/shard_map/ppermute | solution.py:18

commit v4 on v3

--- a/solution.py
+++ b/solution.py
@@ -141,8 +141,71 @@
     return jnp.where((r > c) | (c >= n), 1.0, 0.0).astype(bf16)
 
 
-def finish(att, field, stats, c_gain, s_gain, out_w, mine, other, send, mix, n, per, members):
-    ch = field.shape[1]
+def normed_heads(att, s_gain, mix, n, per):
+    ms = jnp.mean(att * att, axis=1, keepdims=True)
+    normed = att * lax.rsqrt(ms + norm_eps)
+    for h in range(per):
+        part = normed[h * n : (h + 1) * n, :] * s_gain[h : h + 1, :]
+        mix[:, h * HEAD_DIM : (h + 1) * HEAD_DIM] = part.astype(bf16)
+
+
+def by_slot(mix, n, members):
+    me = lax.axis_index("tp")
+    rows = n // members
+    picks = [mix[pl.ds(pl.multiple_of((me ^ k) * rows, rows), rows), :] for k in (0, 2, 1, 3)]
+    return jnp.concatenate(picks, axis=0)
+
+
+def parts_kernel(*refs, slots, blocks, n, per):
+    q_ref = refs[0]
+    pays = refs[1 : 1 + len(slots)]
+    sums = refs[-1]
+    me = lax.axis_index("sp")
+    q = q_ref[...]
+    tri = tri_of(n)
+    for k, pay in zip(slots, pays):
+        j = me ^ k
+        part, total = block_part(q, pay, (me - j) * n, n, per, tri)
+        sums[pl.ds(j, 1)] = part[None]
+        sums[pl.ds(blocks + j, 1)] = total[None]
+
+
+def stick_kernel(q_ref, pay, sums_in, s_gain, out_w, stick, mix, *, slot, blocks, members, n, per):
+    me = lax.axis_index("sp")
+    last = me ^ slot
+    part, total = block_part(q_ref[...], pay, (me - last) * n, n, per, tri_of(n))
+    att = jnp.zeros_like(part)
+    carry = jnp.zeros_like(total)
+    for j in range(blocks - 1, -1, -1):
+        here = last == j
+        att = att + jnp.exp(carry) * jnp.where(here, part, sums_in[j])
+        if j:
+            carry = carry + jnp.where(here, total, sums_in[blocks + j])
+    normed_heads(att, s_gain, mix, n, per)
+    ch = out_w.shape[0] - per * HEAD_DIM
+    stick[...] = dot(by_slot(mix, n, members), out_w[ch:, :])
+
+
+def stick_loop_kernel(q_ref, pays, s_gain, out_w, stick, mix, *, members, n, per):
+    me = lax.axis_index("sp")
+    q = q_ref[...]
+    tri = tri_of(n)
+
+    def step(turn, carried):
+        att, carry = carried
+        part, total = block_part(q, pays.at[me - turn], turn * n, n, per, tri)
+        return att + jnp.exp(carry) * part, carry + total
+
+    zero = jnp.zeros((per * n, HEAD_DIM), f32)
+    att, _ = lax.fori_loop(0, me + 1, step, (zero, zero))
+    normed_heads(att, s_gain, mix, n, per)
+    ch = out_w.shape[0] - per * HEAD_DIM
+    stick[...] = dot(by_slot(mix, n, members), out_w[ch:, :])
+
+
+def finish_kernel(field, s0, s1, s2, s3, c_gain, out_w, stick, mine, other, send, mix, *, members):
+    n, ch = field.shape
+    stats = (s0, s1, s2, s3)
     mean = sum(st[0:1, :] for st in stats) / members
     m2 = sum(st[1:2, :] for st in stats)
     m2 = m2 + ch * sum((st[0:1, :] - mean) ** 2 for st in stats)
@@ -150,66 +213,15 @@
     mean_c = jnp.transpose(jnp.broadcast_to(mean, (ch, n)))
     rstd_c = jnp.transpose(jnp.broadcast_to(rstd, (ch, n)))
     z = (field[...] - mean_c) * rstd_c * c_gain[...]
-    mix[:, 0:ch] = (z * jax.nn.sigmoid(z)).astype(bf16)
-    ms = jnp.mean(att * att, axis=1, keepdims=True)
-    normed = att * lax.rsqrt(ms + norm_eps)
-    for h in range(per):
-        part = normed[h * n : (h + 1) * n, :] * s_gain[h : h + 1, :]
-        mix[:, ch + h * HEAD_DIM : ch + (h + 1) * HEAD_DIM] = part.astype(bf16)
-    me = lax.axis_index("tp")
+    mix[...] = (z * jax.nn.sigmoid(z)).astype(bf16)
+    out = dot(by_slot(mix, n, members), out_w[0:ch, :]) + stick[...]
     rows = n // members
-    lhs = jnp.concatenate(
-        [mix[pl.ds(pl.multiple_of((me ^ k) * rows, rows), rows), :] for k in (0, 2, 1, 3)], axis=0
-    )
-    out = dot(lhs, out_w[...])
     mine[...] = out[0:rows, :]
     other[...] = out[rows : 2 * rows, :]
     send[...] = out[2 * rows :, :].astype(bf16)
 
 
-def attend_kernel(*refs, blocks, members, n, per):
-    q_ref = refs[0]
-    pays = refs[1 : 1 + blocks]
-    field = refs[1 + blocks]
-    stats = refs[2 + blocks : 2 + blocks + members]
-    c_gain, s_gain, out_w, mine, other, send, mix, parts, totals = refs[2 + blocks + members :]
-    me = lax.axis_index("sp")
-    q = q_ref[...]
-    tri = tri_of(n)
-    for k in range(blocks):
-        j = me ^ k
-        part, total = block_part(q, pays[k], (me - j) * n, n, per, tri)
-        parts[pl.ds(j, 1)] = part[None]
-        totals[pl.ds(j, 1)] = total[None]
-    att = parts[blocks - 1]
-    carry = totals[blocks - 1]
-    for j in range(blocks - 2, -1, -1):
-        att = att + jnp.exp(carry) * parts[j]
-        if j:
-            carry = carry + totals[j]
-    finish(att, field, stats, c_gain, s_gain, out_w, mine, other, send, mix, n, per, members)
-
-
-def attend_loop_kernel(*refs, members, n, per):
-    q_ref, pays, field = refs[:3]
-    stats = refs[3 : 3 + members]
-    c_gain, s_gain, out_w, mine, other, send, mix = refs[3 + members :]
-    me = lax.axis_index("sp")
-    q = q_ref[...]
-    tri = tri_of(n)
-
-    def step(turn, carried):
-        att, carry = carried
-        j = me - turn
-        part, total = block_part(q, pays.at[j], turn * n, n, per, tri)
-        return att + jnp.exp(carry) * part, carry + total
-
-    zero = jnp.zeros((per * n, HEAD_DIM), f32)
-    att, _ = lax.fori_loop(0, me + 1, step, (zero, zero))
-    finish(att, field, stats, c_gain, s_gain, out_w, mine, other, send, mix, n, per, members)
-
-
-def call(body, outs, args, scratch=(), flops=0, spaces=None, limit=2**23):
+def call(body, outs, args, scratch=(), flops=0, spaces=None, limit=2**22, aliases={}):
     in_vmem = pl.BlockSpec(memory_space=pltpu.VMEM)
     if spaces is None:
         spaces = [True] * len(args)
@@ -223,6 +235,8 @@
         in_specs=[in_vmem] * len(args),
         out_specs=[in_vmem] * len(outs),
         scratch_shapes=scratch,
+        input_output_aliases=aliases,
+        name=getattr(body, "func", body).__name__,
         cost_estimate=pl.CostEstimate(flops=flops, transcendentals=0, bytes_accessed=0),
         compiler_params=pltpu.CompilerParams(vmem_limit_bytes=limit),
     )(*args)
@@ -292,39 +306,65 @@
     )
     field_shapes = [((n, ch), f32), ((8, n), f32)]
     wide = [pltpu.VMEM((n + 32, ch), f32)]
+    sizes = dict(n=n, per=per)
+    heads = per * n
+    mixed = [pltpu.VMEM((n, query_cols), bf16)]
+    block_flops = 2 * heads * n * HEAD_DIM * 8
     if blocks == 8:
         z2 = swap(pay, "sp", 2)
         z6 = swap(pay, "sp", 6)
         z4 = swap(pay, "sp", 4)
         x1 = swap(pay, "sp", 1)
+        x7 = swap(z6, "sp", 1)
         x3 = swap(z2, "sp", 1)
-        x7 = swap(z6, "sp", 1)
         x5 = swap(z4, "sp", 1)
-        pays = [pay, x1, z2, x3, z4, x5, z6, x7]
+
+        def parts(slots, pays, sums):
+            args = [qs, *pays] + ([] if sums is None else [sums])
+            (out,) = call(
+                functools.partial(parts_kernel, slots=slots, blocks=blocks, **sizes),
+                [((2 * blocks, heads, HEAD_DIM), f32)],
+                args,
+                flops=len(slots) * block_flops,
+                aliases={} if sums is None else {len(args) - 1: 0},
+            )
+            return out
+
+        sums = parts((0,), (pay,), None)
+        sums = parts((2, 6, 1), (z2, z6, x1), sums)
+        sums = parts((4,), (z4,), sums)
         conv_args = [x1, x3, x7, blend, taps]
         field, stats = call(conv_kernel, field_shapes, conv_args, wide, 64 * n * ch)
+        all_stats = [stats] + [swap(stats, "tp", k) for k in (2, 3, 1)]
+        sums = parts((7, 3), (x7, x3), sums)
+        body = functools.partial(stick_kernel, slot=5, blocks=blocks, members=members, **sizes)
+        stick_args = [qs, x5, sums, s_gain, out_w]
+        spaces = None
     else:
-        pays = [lax.all_gather(pay, "sp", axis=0)]
+        pays = lax.all_gather(pay, "sp", axis=0)
         halo = from_behind(blend[n - 32 :], "sp", 1)
-        conv_args = [halo, blend, taps]
-        field, stats = call(conv_plain_kernel, field_shapes, conv_args, wide, 64 * n * ch)
-    stats_chip = swap(stats, "tp", 2)
-    all_stats = [stats, swap(stats, "tp", 1), stats_chip, swap(stats_chip, "tp", 1)]
-    scratch = [pltpu.VMEM((n, ch + query_cols), bf16)]
-    if blocks == 8:
-        body = functools.partial(attend_kernel, blocks=blocks, members=members, n=n, per=per)
-        scratch += [pltpu.VMEM((blocks, per * n, HEAD_DIM), f32)] * 2
-    else:
-        body = functools.partial(attend_loop_kernel, members=members, n=n, per=per)
-    args = [qs, *pays, field, *all_stats, c_gain, s_gain, out_w]
+        field, stats = call(
+            conv_plain_kernel, field_shapes, [halo, blend, taps], wide, 64 * n * ch
+        )
+        all_stats = [stats] + [swap(stats, "tp", k) for k in (2, 3, 1)]
+        body = functools.partial(stick_loop_kernel, members=members, **sizes)
+        stick_args = [qs, pays, s_gain, out_w]
+        spaces = [True, False, True, True]
+    (stick,) = call(
+        body,
+        [((n, width), f32)],
+        stick_args,
+        scratch=mixed,
+        flops=block_flops + 2 * n * width * query_cols,
+        spaces=spaces,
+        limit=2**22 if blocks == 8 else 2**25,
+    )
     mine, other, send = call(
-        body,
+        functools.partial(finish_kernel, members=members),
         [((rows, width), f32), ((rows, width), f32), ((2 * rows, width), bf16)],
-        args,
-        scratch=scratch,
-        flops=2 * n * width * (ch + query_cols),
-        limit=2**23 if blocks == 8 else 2**25,
-        spaces=[True] + [blocks == 8] * len(pays) + [True] * (len(args) - 1 - len(pays)),
+        [field, *all_stats, c_gain, out_w, stick],
+        scratch=[pltpu.VMEM((n, ch), bf16)],
+        flops=2 * n * width * ch,
     )
     got = swap(send, "tp", 1).astype(f32)
     chip = swap((other + got[rows:]).astype(bf16), "tp", 2)

time: 41 us -> 37.9 us (0.924)
  waiting for transfers between devices: 15.2 us -> 11.3 us
  Pallas kernels: 7.76 us -> 8.51 us
    ppermute x15, waiting for transfers between devices: 15.2 us -> 11.3 us  [swap(): return lax.ppermute(value, axis, [(i, i ^ by) for i in range(count)])]
    pallas_call x3 -> x8, Pallas kernels: 5.24 us -> 5.99 us  [call(): pl.pallas_call(body, out_shape=[pltpu.VMEM(shape, dtype) for shape, dtype...]
  transfers between devices with their start and end apart: 15 -> 15, of which waited for: 8 -> 6; matrix products, arithmetic and copies ran while one was open for 3% -> 3% of each run, Pallas kernels for 7% -> 20%
where the time goes in v4:
time: 37.9 us; the launch traced here: 37.7 us
  starting transfers between devices  15.8 us (42%)
  waiting for transfers between devices  11.3 us (30%)
  Pallas kernels  8.51 us (22%)
  local copies, waits for them, and re-layouts  1.25 us (3%)
  other arithmetic  0.76 us (2%)
    ppermute x15, starting transfers between devices, swap(): return lax.ppermute(value, axis, [(i, i ^ by) for i in range(count)])  15.8 us
    ppermute x15, waiting for transfers between devices, swap(): return lax.ppermute(value, axis, [(i, i ^ by) for i in range(count)])  11.3 us
    pallas_call x8, Pallas kernels, call(): pl.pallas_call(body, out_shape=[pltpu.VMEM(shape, dtype) for shape, dtype...  5.99 us
    pallas_call x1, Pallas kernels, shards(): pl.pallas_call(load_kernel, out_shape=[pltpu.VMEM(shape, dtype) for shape...  2.52 us
    pad x1, local copies, waits for them, and re-layouts, shards(): off = jnp.pad(jnp.transpose(key_offsets), ((0, 16 - per), (0, 0)))  1.25 us
  transfers between devices with their start and end apart: 15, of which 6 were waited for; matrix products, arithmetic and copies ran while one was open for 3% of the time, Pallas kernels for 20%

profile of v4, /device:TPU:0, one launch (start us, length us, event | category | flops | bytes accessed | tf_op | source)
XLA Modules:
  0.0 37.7 jit_solution(7210872607690961808)
XLA Ops:
  0.0 3.0 %collective-permute-start = (bf16[32,2048]{1,0:T(8,128)(2,1)}, bf16[32,2048]{1,0:T(8,128)(2,1)S(1)}, u32[]{:S(2)}, u32[]{:S(2)}) collective-permute-start(bf16[32,2048]{1,0:T(8,128)(2,1)} %refs_0_.1), channel_id=1, source_target_pairs={{0,2},{1,3},{2,0},{3,1},{4,6},{5,7},{6,4},{7,5},{8,10},{9,11},{10,... | collective-permute-start | bytes 393224 | tf_op jit(solution)/shard_map/ppermute | solution.py:18
  3.0 1.3 %pad.4.refs_8_ = bf16[16,128]{1,0:T(8,128)(2,1)} pad(bf16[2,128]{1,0:T(2,128)(2,1)} %bitcast.5, bf16[]{:T(256)} %constant.2.clone.1), padding=0_14x0_0 | pad | bytes 4610 | tf_op jit(solution)/shard_map/jit(_pad)/pad | solution.py:267
  4.3 2.5 %shard_map.118 = (bf16[32,2048]{1,0:T(8,128)(2,1)S(1)}, bf16[2048,256]{1,0:T(8,128)(2,1)S(1)}, bf16[2048,256]{1,0:T(8,128)(2,1)S(1)}, bf16[2048,256]{1,0:T(8,128...) custom-call(bf16[32,2048]{1,0:T(8,128)(2,1)} %refs_0_.1, ...), custom_call_target="tpu_custom_call" | custom-call | flops 1000000000 | bytes 5000000 | tf_op jit(solution)/shard_map/pallas_call | solution.py:276
  6.8 0.6 %collective-permute-start.2 = (bf16[32,2048]{1,0:T(8,128)(2,1)S(1)}, bf16[32,2048]{1,0:T(8,128)(2,1)S(1)}, u32[]{:S(2)}, u32[]{:S(2)}) collective-permute-start(bf16[32,2048]{1,0:T(8,128)(2,1)S(1)} %collective-permute-done.t2), channel_id=1, source_target_pairs={{0,1},{1,0},{2,3},{3,2},{4,5},{5,4},{6,7},{7,6},{8,9},{9,8},{10,11... | collective-permute-start | bytes 393224 | tf_op jit(solution)/shard_map/ppermute | solution.py:18
  7.4 1.0 %collective-permute-done.2.t3 = bf16[32,2048]{1,0:T(8,128)(2,1)S(1)} collective-permute-done((bf16[32,2048]{1,0:T(8,128)(2,1)S(1)}, bf16[32,2048]{1,0:T(8,128)(2,1)S(1)}, u32[]{:S(2)}, u32[]{:S(2)}) %collective-permute-start.2) | collective-permute-done | bytes 131104 | tf_op jit(solution)/shard_map/ppermute | solution.py:18
  8.3 0.6 %project_kernel.1 = (bf16[144,256]{1,0:T(8,128)(2,1)S(1)}, bf16[256,128]{1,0:T(8,128)(2,1)S(1)}, bf16[128,128]{1,0:T(8,128)(2,1)S(1)}) custom-call(bf16[32,2048]{1,0:T(8,128)(2,1)S(1)} %get-tuple-element.25.t0, bf16[32,2048]{1,0:T(8,128)(2,1)S(1)} %collective-permute-done.1.t1, bf16[32,2048]{1,0:T(8,128)(2,1)S(1)} %collective-permute-done.t2, ...), custom_call_target="tpu_custom_call" | custom-call | flops 402653184 | tf_op jit(solution)/shard_map/project_kernel/pallas_call | solution.py:232
  9.0 1.6 %collective-permute-start.4 = (bf16[144,256]{1,0:T(8,128)(2,1)S(1)}, bf16[144,256]{1,0:T(8,128)(2,1)S(1)}, u32[]{:S(2)}, u32[]{:S(2)}) collective-permute-start(bf16[144,256]{1,0:T(8,128)(2,1)S(1)} %get-tuple-element.31.refs_1_), channel_id=1, source_target_pairs={{0,8},{4,12},{8,0},{12,4},{16,24},{20,28},{24,16},{28,20},{1,9},{5... | collective-permute-start | bytes 221192 | tf_op jit(solution)/shard_map/ppermute | solution.py:18
  10.6 2.5 %collective-permute-start.6 = (bf16[144,256]{1,0:T(8,128)(2,1)S(1)}, bf16[144,256]{1,0:T(8,128)(2,1)S(1)}, u32[]{:S(2)}, u32[]{:S(2)}) collective-permute-start(bf16[144,256]{1,0:T(8,128)(2,1)S(1)} %get-tuple-element.31.refs_1_), channel_id=1, source_target_pairs={{0,24},{4,28},{8,16},{12,20},{16,8},{20,12},{24,0},{28,4},{1,25},{... | collective-permute-start | bytes 221192 | tf_op jit(solution)/shard_map/ppermute | solution.py:18
  13.2 1.5 %collective-permute-start.3 = (bf16[144,256]{1,0:T(8,128)(2,1)S(1)}, bf16[144,256]{1,0:T(8,128)(2,1)S(1)}, u32[]{:S(2)}, u32[]{:S(2)}) collective-permute-start(bf16[144,256]{1,0:T(8,128)(2,1)S(1)} %get-tuple-element.31.refs_1_), channel_id=1, source_target_pairs={{0,4},{4,0},{8,12},{12,8},{16,20},{20,16},{24,28},{28,24},{1,5},{5... | collective-permute-start | bytes 221192 | tf_op jit(solution)/shard_map/ppermute | solution.py:18
  14.7 0.5 %collective-permute-start.5 = (bf16[144,256]{1,0:T(8,128)(2,1)S(1)}, bf16[144,256]{1,0:T(8,128)(2,1)S(1)}, u32[]{:S(2)}, u32[]{:S(2)}) collective-permute-start(bf16[144,256]{1,0:T(8,128)(2,1)S(1)} %collective-permute-done.4.refs_1_), channel_id=1, source_target_pairs={{0,4},{4,0},{8,12},{12,8},{16,20},{20,16},{24,28},{28,24},{1,5},{5... | collective-permute-start | bytes 221192 | tf_op jit(solution)/shard_map/ppermute | solution.py:18
  15.3 2.5 %collective-permute-done.6.refs_2_ = bf16[144,256]{1,0:T(8,128)(2,1)S(1)} collective-permute-done((bf16[144,256]{1,0:T(8,128)(2,1)S(1)}, bf16[144,256]{1,0:T(8,128)(2,1)S(1)}, u32[]{:S(2)}, u32[]{:S(2)}) %collective-permute-start.6) | collective-permute-done | bytes 73760 | tf_op jit(solution)/shard_map/ppermute | solution.py:18
  17.8 1.5 %collective-permute-start.7 = (bf16[144,256]{1,0:T(8,128)(2,1)S(1)}, bf16[144,256]{1,0:T(8,128)(2,1)S(1)}, u32[]{:S(2)}, u32[]{:S(2)}) collective-permute-start(bf16[144,256]{1,0:T(8,128)(2,1)S(1)} %collective-permute-done.6.refs_2_), channel_id=1, source_target_pairs={{0,4},{4,0},{8,12},{12,8},{16,20},{20,16},{24,28},{28,24},{1,5},{5... | collective-permute-start | bytes 221192 | tf_op jit(solution)/shard_map/ppermute | solution.py:18
  19.3 1.2 %collective-permute-done.11.refs_1_ = bf16[144,256]{1,0:T(8,128)(2,1)S(1)} collective-permute-done((bf16[144,256]{1,0:T(8,128)(2,1)S(1)}, bf16[144,256]{1,0:T(8,128)(2,1)S(1)}, u32[]{:S(2)}, u32[]{:S(2)}) %collective-permute-start.11) | collective-permute-done | bytes 73760 | tf_op jit(solution)/shard_map/ppermute | solution.py:18
  20.5 1.5 %collective-permute-start.12 = (bf16[144,256]{1,0:T(8,128)(2,1)S(1)}, bf16[144,256]{1,0:T(8,128)(2,1)S(1)}, u32[]{:S(2)}, u32[]{:S(2)}) collective-permute-start(bf16[144,256]{1,0:T(8,128)(2,1)S(1)} %collective-permute-done.11.refs_1_), channel_id=1, source_target_pairs={{0,4},{4,0},{8,12},{12,8},{16,20},{20,16},{24,28},{28,24},{1,5},{5... | collective-permute-start | bytes 221192 | tf_op jit(solution)/shard_map/ppermute | solution.py:18
  22.0 0.6 %parts_kernel.4.refs_4_ = f32[16,256,128]{2,1,0:T(8,128)S(1)} custom-call(bf16[256,128]{1,0:T(8,128)(2,1)S(1)} %get-tuple-element.38.refs_0_.q_ref, bf16[144,256]{1,0:T(8,128)(2,1)S(1)} %get-tuple-element.31.refs_1_), custom_call_target="tpu_custom_call" | custom-call | flops 67108864 | tf_op jit(solution)/shard_map/parts_kernel/pallas_call | solution.py:232
  22.5 1.4 %parts_kernel.5.refs_2_ = f32[16,256,128]{2,1,0:T(8,128)S(1)} custom-call(bf16[256,128]{1,0:T(8,128)(2,1)S(1)} %get-tuple-element.38.refs_0_.q_ref, bf16[144,256]{1,0:T(8,128)(2,1)S(1)} %collective-permute-done.4.refs_1_, bf16[144,256]{1,0:T(8,128)(2,1)S(1)} %collective-permute-done.6.refs_2_, ...), custom_call_target="tpu_custom_call", output_to_operand_aliasing={{}: (4, {})} | custom-call | flops 201326592 | tf_op jit(solution)/shard_map/parts_kernel/pallas_call | solution.py:232
  24.0 0.6 %parts_kernel.6.refs_3_ = f32[16,256,128]{2,1,0:T(8,128)S(1)} custom-call(bf16[256,128]{1,0:T(8,128)(2,1)S(1)} %get-tuple-element.38.refs_0_.q_ref, bf16[144,256]{1,0:T(8,128)(2,1)S(1)} %collective-permute-done.11.refs_1_, f32[16,256,128]{2,1,0:T(8,128)S(1)} %parts_kernel.5.refs_2_), custom_call_target="tpu_custom_call", output_to_operand_aliasing={{}: (2, {})} | custom-call | flops 67108864 | tf_op jit(solution)/shard_map/parts_kernel/pallas_call | solution.py:232
  25.0 1.3 %collective-permute-start.8 = (f32[8,128]{1,0:T(8,128)S(1)}, f32[8,128]{1,0:T(8,128)S(1)}, u32[]{:S(2)}, u32[]{:S(2)}) collective-permute-start(f32[8,128]{1,0:T(8,128)S(1)} %get-tuple-element.35.s0), channel_id=1, source_target_pairs={{0,2},{1,3},{2,0},{3,1},{4,6},{5,7},{6,4},{7,5},{8,10},{9,11},{10,... | collective-permute-start | bytes 12296 | tf_op jit(solution)/shard_map/ppermute | solution.py:18
  26.8 0.9 %parts_kernel.7.sums_in = f32[16,256,128]{2,1,0:T(8,128)S(1)} custom-call(bf16[256,128]{1,0:T(8,128)(2,1)S(1)} %get-tuple-element.38.refs_0_.q_ref, bf16[144,256]{1,0:T(8,128)(2,1)S(1)} %collective-permute-done.7.p7.refs_1_, bf16[144,256]{1,0:T(8,128)(2,1)S(1)} %collective-permute-done.5.p3.refs_2_, ...), custom_call_target="tpu_custom_call", output_to_operand_aliasing={{}: (3, {})} | custom-call | flops 134217728 | tf_op jit(solution)/shard_map/parts_kernel/pallas_call | solution.py:232
  27.8 1.1 %stick_kernel.1.stick = f32[128,2048]{1,0:T(8,128)S(1)} custom-call(bf16[256,128]{1,0:T(8,128)(2,1)S(1)} %get-tuple-element.38.refs_0_.q_ref, bf16[144,256]{1,0:T(8,128)(2,1)S(1)} %collective-permute-done.12.pay, f32[16,256,128]{2,1,0:T(8,128)S(1)} %parts_kernel.7.sums_in, f32[2,128]{1,0:T(2,128)S(1)} %get-tuple-element.39.s_gain, ...), custom_call_target="tpu_custom_call" | custom-call | flops 201326592 | tf_op jit(solution)/shard_map/stick_kernel/pallas_call | solution.py:232
  30.0 1.4 %collective-permute-done.13 = bf16[64,2048]{1,0:T(8,128)(2,1)S(1)} collective-permute-done((bf16[64,2048]{1,0:T(8,128)(2,1)S(1)}, bf16[64,2048]{1,0:T(8,128)(2,1)S(1)}, u32[]{:S(2)}, u32[]{:S(2)}) %collective-permute-start.13) | collective-permute-done | bytes 262176 | tf_op jit(solution)/shard_map/ppermute | solution.py:18
  31.4 0.9 %collective-permute-start.14 = (bf16[32,2048]{1,0:T(8,128)(2,1)S(1)}, bf16[32,2048]{1,0:T(8,128)(2,1)S(1)}, u32[]{:S(2)}, u32[]{:S(2)}) collective-permute-start(bf16[32,2048]{1,0:T(8,128)(2,1)S(1)} %fusion), channel_id=1, source_target_pairs={{0,2},{1,3},{2,0},{3,1},{4,6},{5,7},{6,4},{7,5},{8,10},{9,11},{10,... | collective-permute-start | bytes 393224 | tf_op jit(solution)/shard_map/ppermute | solution.py:18
  32.3 4.7 %collective-permute-done.14 = bf16[32,2048]{1,0:T(8,128)(2,1)S(1)} collective-permute-done((bf16[32,2048]{1,0:T(8,128)(2,1)S(1)}, bf16[32,2048]{1,0:T(8,128)(2,1)S(1)}, u32[]{:S(2)}, u32[]{:S(2)}) %collective-permute-start.14) | collective-permute-done | bytes 131104 | tf_op jit(solution)/shard_map/ppermute | solution.py:18
  37.0 0.7 %fusion.2 = bf16[32,2048]{1,0:T(8,128)(2,1)} fusion(f32[32,2048]{1,0:T(8,128)S(1)} %get-tuple-element.40, f32[64,2048]{1,0:T(8,128)S(1)} %convert_element_type.14, bf16[32,2048]{1,0:T(8,128)(2,1)S(1)} %collective-permute-done.14), kind=kLoop, calls=%fused_computation.4 | loop fusion | flops 262144 | bytes 786432 | tf_op jit(solution)/shard_map/convert_element_type | solution.py:371
  (19 shorter events, 2.2 us)
Async XLA Ops:
  0.0 6.8 %collective-permute-start = (bf16[32,2048]{1,0:T(8,128)(2,1)}, bf16[32,2048]{1,0:T(8,128)(2,1)S(1)}, u32[]{:S(2)}, u32[]{:S(2)}) collective-permute-start(bf16[32,2048]{1,0:T(8,128)(2,1)} %refs_0_.1), channel_id=1, source_target_pairs={{0,2},{1,3},{2,0},{3,1},{4,6},{5,7},{6,4},{7,5},{8,10},{9,11},{10,... | collective-permute-start | bytes 393224 | tf_op jit(solution)/shard_map/ppermute | solution.py:18
  3.0 4.4 %collective-permute-start.1 = (bf16[32,2048]{1,0:T(8,128)(2,1)}, bf16[32,2048]{1,0:T(8,128)(2,1)S(1)}, u32[]{:S(2)}, u32[]{:S(2)}) collective-permute-start(bf16[32,2048]{1,0:T(8,128)(2,1)} %refs_0_.1), channel_id=1, source_target_pairs={{0,1},{1,0},{2,3},{3,2},{4,5},{5,4},{6,7},{7,6},{8,9},{9,8},{10,11... | collective-permute-start | bytes 393224 | tf_op jit(solution)/shard_map/ppermute | solution.py:18
  6.8 1.6 %collective-permute-start.2 = (bf16[32,2048]{1,0:T(8,128)(2,1)S(1)}, bf16[32,2048]{1,0:T(8,128)(2,1)S(1)}, u32[]{:S(2)}, u32[]{:S(2)}) collective-permute-start(bf16[32,2048]{1,0:T(8,128)(2,1)S(1)} %collective-permute-done.t2), channel_id=1, source_target_pairs={{0,1},{1,0},{2,3},{3,2},{4,5},{5,4},{6,7},{7,6},{8,9},{9,8},{10,11... | collective-permute-start | bytes 393224 | tf_op jit(solution)/shard_map/ppermute | solution.py:18
  9.0 5.7 %collective-permute-start.4 = (bf16[144,256]{1,0:T(8,128)(2,1)S(1)}, bf16[144,256]{1,0:T(8,128)(2,1)S(1)}, u32[]{:S(2)}, u32[]{:S(2)}) collective-permute-start(bf16[144,256]{1,0:T(8,128)(2,1)S(1)} %get-tuple-element.31.refs_1_), channel_id=1, source_target_pairs={{0,8},{4,12},{8,0},{12,4},{16,24},{20,28},{24,16},{28,20},{1,9},{5... | collective-permute-start | bytes 221192 | tf_op jit(solution)/shard_map/ppermute | solution.py:18
  10.6 7.2 %collective-permute-start.6 = (bf16[144,256]{1,0:T(8,128)(2,1)S(1)}, bf16[144,256]{1,0:T(8,128)(2,1)S(1)}, u32[]{:S(2)}, u32[]{:S(2)}) collective-permute-start(bf16[144,256]{1,0:T(8,128)(2,1)S(1)} %get-tuple-element.31.refs_1_), channel_id=1, source_target_pairs={{0,24},{4,28},{8,16},{12,20},{16,8},{20,12},{24,0},{28,4},{1,25},{... | collective-permute-start | bytes 221192 | tf_op jit(solution)/shard_map/ppermute | solution.py:18
  13.1 7.4 %collective-permute-start.11 = (bf16[144,256]{1,0:T(8,128)(2,1)S(1)}, bf16[144,256]{1,0:T(8,128)(2,1)S(1)}, u32[]{:S(2)}, u32[]{:S(2)}) collective-permute-start(bf16[144,256]{1,0:T(8,128)(2,1)S(1)} %get-tuple-element.31.refs_1_), channel_id=1, source_target_pairs={{0,16},{4,20},{8,24},{12,28},{16,0},{20,4},{24,8},{28,12},{1,17},{... | collective-permute-start | bytes 221192 | tf_op jit(solution)/shard_map/ppermute | solution.py:18
  13.2 9.3 %collective-permute-start.3 = (bf16[144,256]{1,0:T(8,128)(2,1)S(1)}, bf16[144,256]{1,0:T(8,128)(2,1)S(1)}, u32[]{:S(2)}, u32[]{:S(2)}) collective-permute-start(bf16[144,256]{1,0:T(8,128)(2,1)S(1)} %get-tuple-element.31.refs_1_), channel_id=1, source_target_pairs={{0,4},{4,0},{8,12},{12,8},{16,20},{20,16},{24,28},{28,24},{1,5},{5... | collective-permute-start | bytes 221192 | tf_op jit(solution)/shard_map/ppermute | solution.py:18
  14.7 9.8 %collective-permute-start.5 = (bf16[144,256]{1,0:T(8,128)(2,1)S(1)}, bf16[144,256]{1,0:T(8,128)(2,1)S(1)}, u32[]{:S(2)}, u32[]{:S(2)}) collective-permute-start(bf16[144,256]{1,0:T(8,128)(2,1)S(1)} %collective-permute-done.4.refs_1_), channel_id=1, source_target_pairs={{0,4},{4,0},{8,12},{12,8},{16,20},{20,16},{24,28},{28,24},{1,5},{5... | collective-permute-start | bytes 221192 | tf_op jit(solution)/shard_map/ppermute | solution.py:18
  17.8 6.7 %collective-permute-start.7 = (bf16[144,256]{1,0:T(8,128)(2,1)S(1)}, bf16[144,256]{1,0:T(8,128)(2,1)S(1)}, u32[]{:S(2)}, u32[]{:S(2)}) collective-permute-start(bf16[144,256]{1,0:T(8,128)(2,1)S(1)} %collective-permute-done.6.refs_2_), channel_id=1, source_target_pairs={{0,4},{4,0},{8,12},{12,8},{16,20},{20,16},{24,28},{28,24},{1,5},{5... | collective-permute-start | bytes 221192 | tf_op jit(solution)/shard_map/ppermute | solution.py:18
  20.5 7.3 %collective-permute-start.12 = (bf16[144,256]{1,0:T(8,128)(2,1)S(1)}, bf16[144,256]{1,0:T(8,128)(2,1)S(1)}, u32[]{:S(2)}, u32[]{:S(2)}) collective-permute-start(bf16[144,256]{1,0:T(8,128)(2,1)S(1)} %collective-permute-done.11.refs_1_), channel_id=1, source_target_pairs={{0,4},{4,0},{8,12},{12,8},{16,20},{20,16},{24,28},{28,24},{1,5},{5... | collective-permute-start | bytes 221192 | tf_op jit(solution)/shard_map/ppermute | solution.py:18
  24.9 3.9 %collective-permute-start.10 = (f32[8,128]{1,0:T(8,128)S(1)}, f32[8,128]{1,0:T(8,128)S(1)}, u32[]{:S(2)}, u32[]{:S(2)}) collective-permute-start(f32[8,128]{1,0:T(8,128)S(1)} %get-tuple-element.35.s0), channel_id=1, source_target_pairs={{0,1},{1,0},{2,3},{3,2},{4,5},{5,4},{6,7},{7,6},{8,9},{9,8},{10,11... | collective-permute-start | bytes 12296 | tf_op jit(solution)/shard_map/ppermute | solution.py:18
  25.0 3.9 %collective-permute-start.8 = (f32[8,128]{1,0:T(8,128)S(1)}, f32[8,128]{1,0:T(8,128)S(1)}, u32[]{:S(2)}, u32[]{:S(2)}) collective-permute-start(f32[8,128]{1,0:T(8,128)S(1)} %get-tuple-element.35.s0), channel_id=1, source_target_pairs={{0,2},{1,3},{2,0},{3,1},{4,6},{5,7},{6,4},{7,5},{8,10},{9,11},{10,... | collective-permute-start | bytes 12296 | tf_op jit(solution)/shard_map/ppermute | solution.py:18
  26.3 3.0 %collective-permute-start.9 = (f32[8,128]{1,0:T(8,128)S(1)}, f32[8,128]{1,0:T(8,128)S(1)}, u32[]{:S(2)}, u32[]{:S(2)}) collective-permute-start(f32[8,128]{1,0:T(8,128)S(1)} %get-tuple-element.35.s0), channel_id=1, source_target_pairs={{0,3},{1,2},{2,1},{3,0},{4,7},{5,6},{6,5},{7,4},{8,11},{9,10},{10,... | collective-permute-start | bytes 12296 | tf_op jit(solution)/shard_map/ppermute | solution.py:18
  29.7 1.6 %collective-permute-start.13 = (bf16[64,2048]{1,0:T(8,128)(2,1)S(1)}, bf16[64,2048]{1,0:T(8,128)(2,1)S(1)}, u32[]{:S(2)}, u32[]{:S(2)}) collective-permute-start(bf16[64,2048]{1,0:T(8,128)(2,1)S(1)} %get-tuple-element.41), channel_id=1, source_target_pairs={{0,1},{1,0},{2,3},{3,2},{4,5},{5,4},{6,7},{7,6},{8,9},{9,8},{10,11... | collective-permute-start | bytes 786440 | tf_op jit(solution)/shard_map/ppermute | solution.py:18
  31.4 5.6 %collective-permute-start.14 = (bf16[32,2048]{1,0:T(8,128)(2,1)S(1)}, bf16[32,2048]{1,0:T(8,128)(2,1)S(1)}, u32[]{:S(2)}, u32[]{:S(2)}) collective-permute-start(bf16[32,2048]{1,0:T(8,128)(2,1)S(1)} %fusion), channel_id=1, source_target_pairs={{0,2},{1,3},{2,0},{3,1},{4,6},{5,7},{6,4},{7,5},{8,10},{9,11},{10,... | collective-permute-start | bytes 393224 | tf_op jit(solution)/shard_map/ppermute | solution.py:18

commit v5 on v4

--- a/solution.py
+++ b/solution.py
@@ -8,6 +8,7 @@
 from jax.sharding import PartitionSpec as P
 
 HEAD_DIM = 128
+LOG2E = 1.4426950408889634
 norm_eps = 1e-05
 f32 = jnp.float32
 bf16 = jnp.bfloat16
@@ -71,8 +72,12 @@
     both = dot(x, conv_w[...]).astype(bf16).astype(f32)
     b = (both[:, 0:ch] * jax.nn.sigmoid(both[:, ch:])).astype(bf16)
     blend[...] = b
-    row = lax.broadcasted_iota(jnp.int32, (16, kv), 0)
-    pay[n:, 0:kv] = jnp.where(row < 2, off[...], b[n - 32 : n - 16, :])
+    head = b[n - 32 : n - 16, :].astype(f32)
+    row = lax.broadcasted_iota(jnp.int32, head.shape, 0)
+    offs = off[...].astype(f32)
+    for h in range(off.shape[0]):
+        head = jnp.where(row == h, offs[h : h + 1, :], head)
+    pay[n:, 0:kv] = head.astype(bf16)
     pay[n:, kv:] = b[n - 16 :, :]
 
 
@@ -111,33 +116,45 @@
     stats[1:2, :] = jnp.transpose(jnp.broadcast_to(m2, (n, 128)))[0:1, :]
 
 
-def block_part(q, pay, gap, n, per, tri):
-    kv = HEAD_DIM
-    keys = pay[0:n, 0:kv]
-    vals = pay[0:n, kv : 2 * kv]
-    off = pay[n : n + 16, 0:kv].astype(f32)
-    s = lax.dot_general(q, keys, (((1,), (1,)), ((), ())), preferred_element_type=f32)
-    s = s * (HEAD_DIM ** (-0.5))
-    shift = jnp.concatenate(
-        [jnp.broadcast_to(off[h : h + 1, :], (n, n)) for h in range(per)], axis=0
-    )
-    s = s + shift
-    row = lax.broadcasted_iota(jnp.int32, s.shape, 0) & (n - 1)
-    col = lax.broadcasted_iota(jnp.int32, s.shape, 1)
-    allowed = col < row + gap
-    soft = jnp.log1p(jnp.exp(-jnp.abs(s)))
-    take = jnp.minimum(s, 0.0) - soft
-    keep = jnp.where(allowed, jnp.minimum(-s, 0.0) - soft, 0.0)
-    hi = keep.astype(bf16)
-    lo = (keep - hi.astype(f32)).astype(bf16)
-    sums = dot(hi, tri) + dot(lo, tri)
-    w = jnp.where(allowed, jnp.exp(take + sums[:, 0:n]), 0.0).astype(bf16)
-    return dot(w, vals), sums[:, n : 2 * n]
+def shares(q, pays, own, n, per, tri):
+    scale = LOG2E * HEAD_DIM ** (-0.5)
+    takes, splits, outs = [], [], []
+    for pay, mine in zip(pays, own):
+        s = lax.dot_general(
+            q, pay[0:n, 0:HEAD_DIM], (((1,), (1,)), ((), ())), preferred_element_type=f32
+        )
+        off = pay[n : n + 16, 0:HEAD_DIM].astype(f32) * LOG2E
+        shift = [jnp.broadcast_to(off[h : h + 1, :], (n, n)) for h in range(per)]
+        u = s * scale + jnp.concatenate(shift, axis=0)
+        soft = jnp.log2(1.0 + jnp.exp2(-jnp.abs(u)))
+        take = jnp.minimum(u, 0.0) - soft
+        keep = take - u
+        if mine:
+            keep = jnp.where(before(u.shape, n), keep, 0.0)
+        hi = keep.astype(bf16)
+        lo = (keep - hi.astype(f32)).astype(bf16)
+        takes.append(take)
+        splits.append(jnp.concatenate([hi, lo], axis=1))
+    for pay, mine, take, split in zip(pays, own, takes, splits):
+        sums = dot(split, tri)
+        w = jnp.exp2(take + sums[:, 0:n])
+        if mine:
+            w = jnp.where(before(w.shape, n), w, 0.0)
+        outs.append((w.astype(bf16), sums[:, n : 2 * n]))
+    return [
+        (dot(w, pay[0:n, HEAD_DIM : 2 * HEAD_DIM]), total)
+        for pay, (w, total) in zip(pays, outs)
+    ]
+
+
+def before(shape, n):
+    row = lax.broadcasted_iota(jnp.int32, shape, 0) & (n - 1)
+    return lax.broadcasted_iota(jnp.int32, shape, 1) < row
 
 
 def tri_of(n):
-    r = lax.broadcasted_iota(jnp.int32, (n, 2 * n), 0)
-    c = lax.broadcasted_iota(jnp.int32, (n, 2 * n), 1)
+    r = lax.broadcasted_iota(jnp.int32, (2 * n, 2 * n), 0) & (n - 1)
+    c = lax.broadcasted_iota(jnp.int32, (2 * n, 2 * n), 1)
     return jnp.where((r > c) | (c >= n), 1.0, 0.0).astype(bf16)
 
 
@@ -161,26 +178,31 @@
     pays = refs[1 : 1 + len(slots)]
     sums = refs[-1]
     me = lax.axis_index("sp")
-    q = q_ref[...]
-    tri = tri_of(n)
-    for k, pay in zip(slots, pays):
+    found = shares(q_ref[...], pays, [k == 0 for k in slots], n, per, tri_of(n))
+    for k, (part, total) in zip(slots, found):
         j = me ^ k
-        part, total = block_part(q, pay, (me - j) * n, n, per, tri)
+        if k:
+            part = jnp.where(j < me, part, 0.0)
+            total = jnp.where(j < me, total, 0.0)
         sums[pl.ds(j, 1)] = part[None]
         sums[pl.ds(blocks + j, 1)] = total[None]
 
 
-def stick_kernel(q_ref, pay, sums_in, s_gain, out_w, stick, mix, *, slot, blocks, members, n, per):
+def stick_kernel(q_ref, *refs, slots, blocks, members, n, per):
+    pays = refs[: len(slots)]
+    s_gain, out_w, _, stick, sums, mix = refs[len(slots) :]
     me = lax.axis_index("sp")
-    last = me ^ slot
-    part, total = block_part(q_ref[...], pay, (me - last) * n, n, per, tri_of(n))
-    att = jnp.zeros_like(part)
-    carry = jnp.zeros_like(total)
-    for j in range(blocks - 1, -1, -1):
-        here = last == j
-        att = att + jnp.exp(carry) * jnp.where(here, part, sums_in[j])
+    late = shares(q_ref[...], pays, [False] * len(slots), n, per, tri_of(n))
+    for k, (part, total) in zip(slots, late):
+        j = me ^ k
+        sums[pl.ds(j, 1)] = jnp.where(j < me, part, 0.0)[None]
+        sums[pl.ds(blocks + j, 1)] = jnp.where(j < me, total, 0.0)[None]
+    att = sums[blocks - 1]
+    carry = sums[2 * blocks - 1]
+    for j in range(blocks - 2, -1, -1):
+        att = att + jnp.exp2(carry) * sums[j]
         if j:
-            carry = carry + jnp.where(here, total, sums_in[blocks + j])
+            carry = carry + sums[blocks + j]
     normed_heads(att, s_gain, mix, n, per)
     ch = out_w.shape[0] - per * HEAD_DIM
     stick[...] = dot(by_slot(mix, n, members), out_w[ch:, :])
@@ -193,11 +215,11 @@
 
     def step(turn, carried):
         att, carry = carried
-        part, total = block_part(q, pays.at[me - turn], turn * n, n, per, tri)
-        return att + jnp.exp(carry) * part, carry + total
-
-    zero = jnp.zeros((per * n, HEAD_DIM), f32)
-    att, _ = lax.fori_loop(0, me + 1, step, (zero, zero))
+        ((part, total),) = shares(q, [pays.at[me - turn]], [False], n, per, tri)
+        return att + jnp.exp2(carry) * part, carry + total
+
+    (start,) = shares(q, [pays.at[me]], [True], n, per, tri)
+    att, _ = lax.fori_loop(1, me + 1, step, start)
     normed_heads(att, s_gain, mix, n, per)
     ch = out_w.shape[0] - per * HEAD_DIM
     stick[...] = dot(by_slot(mix, n, members), out_w[ch:, :])
@@ -264,7 +286,7 @@
     kv = key_weight.shape[1]
     query_cols = query_weight.shape[1]
     per = query_cols // kv
-    off = jnp.pad(jnp.transpose(key_offsets), ((0, 16 - per), (0, 0)))
+    off = jnp.transpose(key_offsets)
     by_core = swap(tokens, "tp", 1)
     by_chip = swap(tokens, "tp", 2)
     in_vmem = pl.BlockSpec(memory_space=pltpu.VMEM)
@@ -284,7 +306,7 @@
                 ((width, 2 * kv), bf16),
                 (conv_taps.shape, f32),
                 ((1, ch), f32),
-                ((16, n), bf16),
+                ((per, n), bf16),
                 ((per, HEAD_DIM), f32),
                 ((ch + query_cols, width), bf16),
             )
@@ -330,15 +352,16 @@
             )
             return out
 
-        sums = parts((0,), (pay,), None)
-        sums = parts((2, 6, 1), (z2, z6, x1), sums)
-        sums = parts((4,), (z4,), sums)
+        sums = parts((0, 2, 6, 1, 4), (pay, z2, z6, x1, z4), None)
         conv_args = [x1, x3, x7, blend, taps]
         field, stats = call(conv_kernel, field_shapes, conv_args, wide, 64 * n * ch)
         all_stats = [stats] + [swap(stats, "tp", k) for k in (2, 3, 1)]
-        sums = parts((7, 3), (x7, x3), sums)
-        body = functools.partial(stick_kernel, slot=5, blocks=blocks, members=members, **sizes)
-        stick_args = [qs, x5, sums, s_gain, out_w]
+        body = functools.partial(
+            stick_kernel, slots=(3, 7, 5), blocks=blocks, members=members, **sizes
+        )
+        stick_args = [qs, x3, x7, x5, s_gain, out_w, sums]
+        stick_outs = [((2 * blocks, heads, HEAD_DIM), f32)]
+        aliases = {6: 1}
         spaces = None
     else:
         pays = lax.all_gather(pay, "sp", axis=0)
@@ -349,14 +372,17 @@
         all_stats = [stats] + [swap(stats, "tp", k) for k in (2, 3, 1)]
         body = functools.partial(stick_loop_kernel, members=members, **sizes)
         stick_args = [qs, pays, s_gain, out_w]
+        stick_outs = []
+        aliases = {}
         spaces = [True, False, True, True]
-    (stick,) = call(
+    stick, *_ = call(
         body,
-        [((n, width), f32)],
+        [((n, width), f32)] + stick_outs,
         stick_args,
         scratch=mixed,
         flops=block_flops + 2 * n * width * query_cols,
         spaces=spaces,
+        aliases=aliases,
         limit=2**22 if blocks == 8 else 2**25,
     )
     mine, other, send = call(

time: 37.9 us -> 37.1 us (0.979)
  Pallas kernels: 8.51 us -> 5.83 us
  waiting for transfers between devices: 11.3 us -> 13.7 us
  local copies, waits for them, and re-layouts: 1.25 us -> 0 us
  starting transfers between devices: 15.8 us -> 16.6 us
    pallas_call x8 -> x5, Pallas kernels: 5.99 us -> 3.31 us  [call(): pl.pallas_call(body, out_shape=[pltpu.VMEM(shape, dtype) for shape, dtype...]
    ppermute x15, waiting for transfers between devices: 11.3 us -> 13.7 us  [swap(): return lax.ppermute(value, axis, [(i, i ^ by) for i in range(count)])]
    pad x1 -> x0, local copies, waits for them, and re-layouts: 1.25 us -> none  [shards(): off = jnp.pad(jnp.transpose(key_offsets), ((0, 16 - per), (0, 0)))]
    ppermute x15, starting transfers between devices: 15.8 us -> 16.6 us  [swap(): return lax.ppermute(value, axis, [(i, i ^ by) for i in range(count)])]
  transfers between devices with their start and end apart: 15 -> 15, of which waited for: 6 -> 8; matrix products, arithmetic and copies ran while one was open for 3% -> 0% of each run, Pallas kernels for 20% -> 13%
where the time goes in v5:
time: 37.1 us; the launch traced here: 37 us
  starting transfers between devices  16.6 us (45%)
  waiting for transfers between devices  13.7 us (37%)
  Pallas kernels  5.83 us (16%)
  other arithmetic  0.76 us (2%)
    ppermute x15, starting transfers between devices, swap(): return lax.ppermute(value, axis, [(i, i ^ by) for i in range(count)])  16.6 us
    ppermute x15, waiting for transfers between devices, swap(): return lax.ppermute(value, axis, [(i, i ^ by) for i in range(count)])  13.7 us
    pallas_call x5, Pallas kernels, call(): pl.pallas_call(body, out_shape=[pltpu.VMEM(shape, dtype) for shape, dtype...  3.31 us
    pallas_call x1, Pallas kernels, shards(): pl.pallas_call(load_kernel, out_shape=[pltpu.VMEM(shape, dtype) for shape...  2.52 us
  transfers between devices with their start and end apart: 15, of which 8 were waited for; matrix products, arithmetic and copies ran while one was open for 0% of the time, Pallas kernels for 13%

profile of v5, /device:TPU:0, one launch (start us, length us, event | category | flops | bytes accessed | tf_op | source)
XLA Modules:
  0.0 37.0 jit_solution(6404757561892762499)
XLA Ops:
  0.0 3.0 %collective-permute-start = (bf16[32,2048]{1,0:T(8,128)(2,1)}, bf16[32,2048]{1,0:T(8,128)(2,1)S(1)}, u32[]{:S(2)}, u32[]{:S(2)}) collective-permute-start(bf16[32,2048]{1,0:T(8,128)(2,1)} %refs_0_.1), channel_id=1, source_target_pairs={{0,2},{1,3},{2,0},{3,1},{4,6},{5,7},{6,4},{7,5},{8,10},{9,11},{10,... | collective-permute-start | bytes 393224 | tf_op jit(solution)/shard_map/ppermute | solution.py:19
  3.0 2.5 %shard_map.118 = (bf16[32,2048]{1,0:T(8,128)(2,1)S(1)}, bf16[2048,256]{1,0:T(8,128)(2,1)S(1)}, bf16[2048,256]{1,0:T(8,128)(2,1)S(1)}, bf16[2048,256]{1,0:T(8,128...) custom-call(bf16[32,2048]{1,0:T(8,128)(2,1)} %refs_0_.1, ...), custom_call_target="tpu_custom_call" | custom-call | flops 1000000000 | bytes 5000000 | tf_op jit(solution)/shard_map/pallas_call | solution.py:298
  5.5 1.2 %collective-permute-done.t2 = bf16[32,2048]{1,0:T(8,128)(2,1)S(1)} collective-permute-done((bf16[32,2048]{1,0:T(8,128)(2,1)}, bf16[32,2048]{1,0:T(8,128)(2,1)S(1)}, u32[]{:S(2)}, u32[]{:S(2)}) %collective-permute-start) | collective-permute-done | bytes 131104 | tf_op jit(solution)/shard_map/ppermute | solution.py:19
  6.7 1.3 %collective-permute-done.2.t3 = bf16[32,2048]{1,0:T(8,128)(2,1)S(1)} collective-permute-done((bf16[32,2048]{1,0:T(8,128)(2,1)S(1)}, bf16[32,2048]{1,0:T(8,128)(2,1)S(1)}, u32[]{:S(2)}, u32[]{:S(2)}) %collective-permute-start.2) | collective-permute-done | bytes 131104 | tf_op jit(solution)/shard_map/ppermute | solution.py:19
  8.0 0.6 %project_kernel.1 = (bf16[144,256]{1,0:T(8,128)(2,1)S(1)}, bf16[256,128]{1,0:T(8,128)(2,1)S(1)}, bf16[128,128]{1,0:T(8,128)(2,1)S(1)}) custom-call(bf16[32,2048]{1,0:T(8,128)(2,1)S(1)} %get-tuple-element.26.t0, bf16[32,2048]{1,0:T(8,128)(2,1)S(1)} %collective-permute-done.1.t1, bf16[32,2048]{1,0:T(8,128)(2,1)S(1)} %collective-permute-done.t2, ...), custom_call_target="tpu_custom_call" | custom-call | flops 402653184 | tf_op jit(solution)/shard_map/project_kernel/pallas_call | solution.py:254
  8.7 3.9 %collective-permute-start.6 = (bf16[144,256]{1,0:T(8,128)(2,1)S(1)}, bf16[144,256]{1,0:T(8,128)(2,1)S(1)}, u32[]{:S(2)}, u32[]{:S(2)}) collective-permute-start(bf16[144,256]{1,0:T(8,128)(2,1)S(1)} %get-tuple-element.32.refs_1_), channel_id=1, source_target_pairs={{0,24},{4,28},{8,16},{12,20},{16,8},{20,12},{24,0},{28,4},{1,25},{... | collective-permute-start | bytes 221192 | tf_op jit(solution)/shard_map/ppermute | solution.py:19
  12.6 0.6 %collective-permute-start.11 = (bf16[144,256]{1,0:T(8,128)(2,1)S(1)}, bf16[144,256]{1,0:T(8,128)(2,1)S(1)}, u32[]{:S(2)}, u32[]{:S(2)}) collective-permute-start(bf16[144,256]{1,0:T(8,128)(2,1)S(1)} %get-tuple-element.32.refs_1_), channel_id=1, source_target_pairs={{0,16},{4,20},{8,24},{12,28},{16,0},{20,4},{24,8},{28,12},{1,17},{... | collective-permute-start | bytes 221192 | tf_op jit(solution)/shard_map/ppermute | solution.py:19
  13.2 1.6 %collective-permute-start.3 = (bf16[144,256]{1,0:T(8,128)(2,1)S(1)}, bf16[144,256]{1,0:T(8,128)(2,1)S(1)}, u32[]{:S(2)}, u32[]{:S(2)}) collective-permute-start(bf16[144,256]{1,0:T(8,128)(2,1)S(1)} %get-tuple-element.32.refs_1_), channel_id=1, source_target_pairs={{0,4},{4,0},{8,12},{12,8},{16,20},{20,16},{24,28},{28,24},{1,5},{5... | collective-permute-start | bytes 221192 | tf_op jit(solution)/shard_map/ppermute | solution.py:19
  14.9 0.9 %collective-permute-done.6.refs_3_ = bf16[144,256]{1,0:T(8,128)(2,1)S(1)} collective-permute-done((bf16[144,256]{1,0:T(8,128)(2,1)S(1)}, bf16[144,256]{1,0:T(8,128)(2,1)S(1)}, u32[]{:S(2)}, u32[]{:S(2)}) %collective-permute-start.6) | collective-permute-done | bytes 73760 | tf_op jit(solution)/shard_map/ppermute | solution.py:19
  15.7 1.7 %collective-permute-start.7 = (bf16[144,256]{1,0:T(8,128)(2,1)S(1)}, bf16[144,256]{1,0:T(8,128)(2,1)S(1)}, u32[]{:S(2)}, u32[]{:S(2)}) collective-permute-start(bf16[144,256]{1,0:T(8,128)(2,1)S(1)} %collective-permute-done.6.refs_3_), channel_id=1, source_target_pairs={{0,4},{4,0},{8,12},{12,8},{16,20},{20,16},{24,28},{28,24},{1,5},{5... | collective-permute-start | bytes 221192 | tf_op jit(solution)/shard_map/ppermute | solution.py:19
  17.4 0.5 %collective-permute-done.4.refs_2_ = bf16[144,256]{1,0:T(8,128)(2,1)S(1)} collective-permute-done((bf16[144,256]{1,0:T(8,128)(2,1)S(1)}, bf16[144,256]{1,0:T(8,128)(2,1)S(1)}, u32[]{:S(2)}, u32[]{:S(2)}) %collective-permute-start.4) | collective-permute-done | bytes 73760 | tf_op jit(solution)/shard_map/ppermute | solution.py:19
  17.9 1.6 %collective-permute-start.5 = (bf16[144,256]{1,0:T(8,128)(2,1)S(1)}, bf16[144,256]{1,0:T(8,128)(2,1)S(1)}, u32[]{:S(2)}, u32[]{:S(2)}) collective-permute-start(bf16[144,256]{1,0:T(8,128)(2,1)S(1)} %collective-permute-done.4.refs_2_), channel_id=1, source_target_pairs={{0,4},{4,0},{8,12},{12,8},{16,20},{20,16},{24,28},{28,24},{1,5},{5... | collective-permute-start | bytes 221192 | tf_op jit(solution)/shard_map/ppermute | solution.py:19
  19.5 1.4 %collective-permute-start.12 = (bf16[144,256]{1,0:T(8,128)(2,1)S(1)}, bf16[144,256]{1,0:T(8,128)(2,1)S(1)}, u32[]{:S(2)}, u32[]{:S(2)}) collective-permute-start(bf16[144,256]{1,0:T(8,128)(2,1)S(1)} %collective-permute-done.11.refs_5_), channel_id=1, source_target_pairs={{0,4},{4,0},{8,12},{12,8},{16,20},{20,16},{24,28},{28,24},{1,5},{5... | collective-permute-start | bytes 221192 | tf_op jit(solution)/shard_map/ppermute | solution.py:19
  20.9 0.8 %parts_kernel.1.refs_5_ = f32[16,256,128]{2,1,0:T(8,128)S(1)} custom-call(bf16[256,128]{1,0:T(8,128)(2,1)S(1)} %get-tuple-element.39.refs_0_.q_ref, bf16[144,256]{1,0:T(8,128)(2,1)S(1)} %get-tuple-element.32.refs_1_, bf16[144,256]{1,0:T(8,128)(2,1)S(1)} %collective-permute-done.4.refs_2_, bf16[144,256]{1,0:T(8,128)(2,1)S(1)} %collective-permute-done.6.refs_3_, ...), custom_call_target="tpu_custom_call" | custom-call | flops 335544320 | tf_op jit(solution)/shard_map/parts_kernel/pallas_call | solution.py:254
  21.7 1.3 %collective-permute-done.5.p3.refs_0_ = bf16[144,256]{1,0:T(8,128)(2,1)S(1)} collective-permute-done((bf16[144,256]{1,0:T(8,128)(2,1)S(1)}, bf16[144,256]{1,0:T(8,128)(2,1)S(1)}, u32[]{:S(2)}, u32[]{:S(2)}) %collective-permute-start.5) | collective-permute-done | bytes 73760 | tf_op jit(solution)/shard_map/ppermute | solution.py:19
  23.4 1.6 %collective-permute-start.9 = (f32[8,128]{1,0:T(8,128)S(1)}, f32[8,128]{1,0:T(8,128)S(1)}, u32[]{:S(2)}, u32[]{:S(2)}) collective-permute-start(f32[8,128]{1,0:T(8,128)S(1)} %get-tuple-element.36.s0), channel_id=1, source_target_pairs={{0,3},{1,2},{2,1},{3,0},{4,7},{5,6},{6,5},{7,4},{8,11},{9,10},{10,... | collective-permute-start | bytes 12296 | tf_op jit(solution)/shard_map/ppermute | solution.py:19
  25.0 0.5 %collective-permute-start.8 = (f32[8,128]{1,0:T(8,128)S(1)}, f32[8,128]{1,0:T(8,128)S(1)}, u32[]{:S(2)}, u32[]{:S(2)}) collective-permute-start(f32[8,128]{1,0:T(8,128)S(1)} %get-tuple-element.36.s0), channel_id=1, source_target_pairs={{0,2},{1,3},{2,0},{3,1},{4,6},{5,7},{6,4},{7,5},{8,10},{9,11},{10,... | collective-permute-start | bytes 12296 | tf_op jit(solution)/shard_map/ppermute | solution.py:19
  25.5 1.1 %stick_kernel.1 = (f32[128,2048]{1,0:T(8,128)S(1)}, f32[16,256,128]{2,1,0:T(8,128)S(1)}) custom-call(bf16[256,128]{1,0:T(8,128)(2,1)S(1)} %get-tuple-element.39.refs_0_.q_ref, bf16[144,256]{1,0:T(8,128)(2,1)S(1)} %collective-permute-done.5.p3.refs_0_, bf16[144,256]{1,0:T(8,128)(2,1)S(1)} %collective-permute-done.7.p7.refs_1_, ...), custom_call_target="tpu_custom_call", output_to_operand_aliasing={{1}: (6, {})} | custom-call | flops 201326592 | tf_op jit(solution)/shard_map/stick_kernel/pallas_call | solution.py:254
  26.7 1.9 %collective-permute-done.8.s1 = f32[8,128]{1,0:T(8,128)S(1)} collective-permute-done((f32[8,128]{1,0:T(8,128)S(1)}, f32[8,128]{1,0:T(8,128)S(1)}, u32[]{:S(2)}, u32[]{:S(2)}) %collective-permute-start.8) | collective-permute-done | bytes 4128 | tf_op jit(solution)/shard_map/ppermute | solution.py:19
  28.6 0.4 %finish_kernel.1 = (f32[32,2048]{1,0:T(8,128)S(1)}, f32[32,2048]{1,0:T(8,128)S(1)}, bf16[64,2048]{1,0:T(8,128)(2,1)S(1)}) custom-call(f32[128,128]{1,0:T(8,128)S(1)} %get-tuple-element.35.field, f32[8,128]{1,0:T(8,128)S(1)} %get-tuple-element.36.s0, f32[8,128]{1,0:T(8,128)S(1)} %collective-permute-done.8.s1, f32[8,128]{1,0:T(8,128)S(1)} %collective-permute-done.9.s2, ...), custom_call_target="tpu_custom_call" | custom-call | flops 67108864 | tf_op jit(solution)/shard_map/finish_kernel/pallas_call | solution.py:254
  29.1 1.5 %collective-permute-done.13 = bf16[64,2048]{1,0:T(8,128)(2,1)S(1)} collective-permute-done((bf16[64,2048]{1,0:T(8,128)(2,1)S(1)}, bf16[64,2048]{1,0:T(8,128)(2,1)S(1)}, u32[]{:S(2)}, u32[]{:S(2)}) %collective-permute-start.13) | collective-permute-done | bytes 262176 | tf_op jit(solution)/shard_map/ppermute | solution.py:19
  30.7 0.6 %collective-permute-start.14 = (bf16[32,2048]{1,0:T(8,128)(2,1)S(1)}, bf16[32,2048]{1,0:T(8,128)(2,1)S(1)}, u32[]{:S(2)}, u32[]{:S(2)}) collective-permute-start(bf16[32,2048]{1,0:T(8,128)(2,1)S(1)} %fusion), channel_id=1, source_target_pairs={{0,2},{1,3},{2,0},{3,1},{4,6},{5,7},{6,4},{7,5},{8,10},{9,11},{10,... | collective-permute-start | bytes 393224 | tf_op jit(solution)/shard_map/ppermute | solution.py:19
  31.3 5.0 %collective-permute-done.14 = bf16[32,2048]{1,0:T(8,128)(2,1)S(1)} collective-permute-done((bf16[32,2048]{1,0:T(8,128)(2,1)S(1)}, bf16[32,2048]{1,0:T(8,128)(2,1)S(1)}, u32[]{:S(2)}, u32[]{:S(2)}) %collective-permute-start.14) | collective-permute-done | bytes 131104 | tf_op jit(solution)/shard_map/ppermute | solution.py:19
  36.3 0.7 %fusion.2 = bf16[32,2048]{1,0:T(8,128)(2,1)} fusion(f32[32,2048]{1,0:T(8,128)S(1)} %get-tuple-element.42, f32[64,2048]{1,0:T(8,128)S(1)} %convert_element_type.12, bf16[32,2048]{1,0:T(8,128)(2,1)S(1)} %collective-permute-done.14), kind=kLoop, calls=%fused_computation.4 | loop fusion | flops 262144 | bytes 786432 | tf_op jit(solution)/shard_map/convert_element_type | solution.py:397
  (15 shorter events, 0.6 us)
Async XLA Ops:
  0.0 6.7 %collective-permute-start = (bf16[32,2048]{1,0:T(8,128)(2,1)}, bf16[32,2048]{1,0:T(8,128)(2,1)S(1)}, u32[]{:S(2)}, u32[]{:S(2)}) collective-permute-start(bf16[32,2048]{1,0:T(8,128)(2,1)} %refs_0_.1), channel_id=1, source_target_pairs={{0,2},{1,3},{2,0},{3,1},{4,6},{5,7},{6,4},{7,5},{8,10},{9,11},{10,... | collective-permute-start | bytes 393224 | tf_op jit(solution)/shard_map/ppermute | solution.py:19
  3.0 3.7 %collective-permute-start.1 = (bf16[32,2048]{1,0:T(8,128)(2,1)}, bf16[32,2048]{1,0:T(8,128)(2,1)S(1)}, u32[]{:S(2)}, u32[]{:S(2)}) collective-permute-start(bf16[32,2048]{1,0:T(8,128)(2,1)} %refs_0_.1), channel_id=1, source_target_pairs={{0,1},{1,0},{2,3},{3,2},{4,5},{5,4},{6,7},{7,6},{8,9},{9,8},{10,11... | collective-permute-start | bytes 393224 | tf_op jit(solution)/shard_map/ppermute | solution.py:19
  6.7 1.3 %collective-permute-start.2 = (bf16[32,2048]{1,0:T(8,128)(2,1)S(1)}, bf16[32,2048]{1,0:T(8,128)(2,1)S(1)}, u32[]{:S(2)}, u32[]{:S(2)}) collective-permute-start(bf16[32,2048]{1,0:T(8,128)(2,1)S(1)} %collective-permute-done.t2), channel_id=1, source_target_pairs={{0,1},{1,0},{2,3},{3,2},{4,5},{5,4},{6,7},{7,6},{8,9},{9,8},{10,11... | collective-permute-start | bytes 393224 | tf_op jit(solution)/shard_map/ppermute | solution.py:19
  8.7 7.1 %collective-permute-start.6 = (bf16[144,256]{1,0:T(8,128)(2,1)S(1)}, bf16[144,256]{1,0:T(8,128)(2,1)S(1)}, u32[]{:S(2)}, u32[]{:S(2)}) collective-permute-start(bf16[144,256]{1,0:T(8,128)(2,1)S(1)} %get-tuple-element.32.refs_1_), channel_id=1, source_target_pairs={{0,24},{4,28},{8,16},{12,20},{16,8},{20,12},{24,0},{28,4},{1,25},{... | collective-permute-start | bytes 221192 | tf_op jit(solution)/shard_map/ppermute | solution.py:19
  12.6 5.4 %collective-permute-start.4 = (bf16[144,256]{1,0:T(8,128)(2,1)S(1)}, bf16[144,256]{1,0:T(8,128)(2,1)S(1)}, u32[]{:S(2)}, u32[]{:S(2)}) collective-permute-start(bf16[144,256]{1,0:T(8,128)(2,1)S(1)} %get-tuple-element.32.refs_1_), channel_id=1, source_target_pairs={{0,8},{4,12},{8,0},{12,4},{16,24},{20,28},{24,16},{28,20},{1,9},{5... | collective-permute-start | bytes 221192 | tf_op jit(solution)/shard_map/ppermute | solution.py:19
  12.6 7.0 %collective-permute-start.11 = (bf16[144,256]{1,0:T(8,128)(2,1)S(1)}, bf16[144,256]{1,0:T(8,128)(2,1)S(1)}, u32[]{:S(2)}, u32[]{:S(2)}) collective-permute-start(bf16[144,256]{1,0:T(8,128)(2,1)S(1)} %get-tuple-element.32.refs_1_), channel_id=1, source_target_pairs={{0,16},{4,20},{8,24},{12,28},{16,0},{20,4},{24,8},{28,12},{1,17},{... | collective-permute-start | bytes 221192 | tf_op jit(solution)/shard_map/ppermute | solution.py:19
  13.2 7.7 %collective-permute-start.3 = (bf16[144,256]{1,0:T(8,128)(2,1)S(1)}, bf16[144,256]{1,0:T(8,128)(2,1)S(1)}, u32[]{:S(2)}, u32[]{:S(2)}) collective-permute-start(bf16[144,256]{1,0:T(8,128)(2,1)S(1)} %get-tuple-element.32.refs_1_), channel_id=1, source_target_pairs={{0,4},{4,0},{8,12},{12,8},{16,20},{20,16},{24,28},{28,24},{1,5},{5... | collective-permute-start | bytes 221192 | tf_op jit(solution)/shard_map/ppermute | solution.py:19
  15.7 6.0 %collective-permute-start.7 = (bf16[144,256]{1,0:T(8,128)(2,1)S(1)}, bf16[144,256]{1,0:T(8,128)(2,1)S(1)}, u32[]{:S(2)}, u32[]{:S(2)}) collective-permute-start(bf16[144,256]{1,0:T(8,128)(2,1)S(1)} %collective-permute-done.6.refs_3_), channel_id=1, source_target_pairs={{0,4},{4,0},{8,12},{12,8},{16,20},{20,16},{24,28},{28,24},{1,5},{5... | collective-permute-start | bytes 221192 | tf_op jit(solution)/shard_map/ppermute | solution.py:19
  17.9 5.0 %collective-permute-start.5 = (bf16[144,256]{1,0:T(8,128)(2,1)S(1)}, bf16[144,256]{1,0:T(8,128)(2,1)S(1)}, u32[]{:S(2)}, u32[]{:S(2)}) collective-permute-start(bf16[144,256]{1,0:T(8,128)(2,1)S(1)} %collective-permute-done.4.refs_2_), channel_id=1, source_target_pairs={{0,4},{4,0},{8,12},{12,8},{16,20},{20,16},{24,28},{28,24},{1,5},{5... | collective-permute-start | bytes 221192 | tf_op jit(solution)/shard_map/ppermute | solution.py:19
  19.5 6.0 %collective-permute-start.12 = (bf16[144,256]{1,0:T(8,128)(2,1)S(1)}, bf16[144,256]{1,0:T(8,128)(2,1)S(1)}, u32[]{:S(2)}, u32[]{:S(2)}) collective-permute-start(bf16[144,256]{1,0:T(8,128)(2,1)S(1)} %collective-permute-done.11.refs_5_), channel_id=1, source_target_pairs={{0,4},{4,0},{8,12},{12,8},{16,20},{20,16},{24,28},{28,24},{1,5},{5... | collective-permute-start | bytes 221192 | tf_op jit(solution)/shard_map/ppermute | solution.py:19
  23.3 3.3 %collective-permute-start.10 = (f32[8,128]{1,0:T(8,128)S(1)}, f32[8,128]{1,0:T(8,128)S(1)}, u32[]{:S(2)}, u32[]{:S(2)}) collective-permute-start(f32[8,128]{1,0:T(8,128)S(1)} %get-tuple-element.36.s0), channel_id=1, source_target_pairs={{0,1},{1,0},{2,3},{3,2},{4,5},{5,4},{6,7},{7,6},{8,9},{9,8},{10,11... | collective-permute-start | bytes 12296 | tf_op jit(solution)/shard_map/ppermute | solution.py:19
  23.4 3.3 %collective-permute-start.9 = (f32[8,128]{1,0:T(8,128)S(1)}, f32[8,128]{1,0:T(8,128)S(1)}, u32[]{:S(2)}, u32[]{:S(2)}) collective-permute-start(f32[8,128]{1,0:T(8,128)S(1)} %get-tuple-element.36.s0), channel_id=1, source_target_pairs={{0,3},{1,2},{2,1},{3,0},{4,7},{5,6},{6,5},{7,4},{8,11},{9,10},{10,... | collective-permute-start | bytes 12296 | tf_op jit(solution)/shard_map/ppermute | solution.py:19
  25.0 3.6 %collective-permute-start.8 = (f32[8,128]{1,0:T(8,128)S(1)}, f32[8,128]{1,0:T(8,128)S(1)}, u32[]{:S(2)}, u32[]{:S(2)}) collective-permute-start(f32[8,128]{1,0:T(8,128)S(1)} %get-tuple-element.36.s0), channel_id=1, source_target_pairs={{0,2},{1,3},{2,0},{3,1},{4,6},{5,7},{6,4},{7,5},{8,10},{9,11},{10,... | collective-permute-start | bytes 12296 | tf_op jit(solution)/shard_map/ppermute | solution.py:19
  29.0 1.6 %collective-permute-start.13 = (bf16[64,2048]{1,0:T(8,128)(2,1)S(1)}, bf16[64,2048]{1,0:T(8,128)(2,1)S(1)}, u32[]{:S(2)}, u32[]{:S(2)}) collective-permute-start(bf16[64,2048]{1,0:T(8,128)(2,1)S(1)} %get-tuple-element.43), channel_id=1, source_target_pairs={{0,1},{1,0},{2,3},{3,2},{4,5},{5,4},{6,7},{7,6},{8,9},{9,8},{10,11... | collective-permute-start | bytes 786440 | tf_op jit(solution)/shard_map/ppermute | solution.py:19
  30.7 5.6 %collective-permute-start.14 = (bf16[32,2048]{1,0:T(8,128)(2,1)S(1)}, bf16[32,2048]{1,0:T(8,128)(2,1)S(1)}, u32[]{:S(2)}, u32[]{:S(2)}) collective-permute-start(bf16[32,2048]{1,0:T(8,128)(2,1)S(1)} %fusion), channel_id=1, source_target_pairs={{0,2},{1,3},{2,0},{3,1},{4,6},{5,7},{6,4},{7,5},{8,10},{9,11},{10,... | collective-permute-start | bytes 393224 | tf_op jit(solution)/shard_map/ppermute | solution.py:19

commit v6 on v5

--- a/solution.py
+++ b/solution.py
@@ -6,6 +6,7 @@
 from jax.experimental import pallas as pl
 from jax.experimental.pallas import tpu as pltpu
 from jax.sharding import PartitionSpec as P
+
 
 HEAD_DIM = 128
 LOG2E = 1.4426950408889634
@@ -56,7 +57,7 @@
         copy.wait()
 
 
-def project_kernel(t0, t1, t2, t3, conv_w, q_w, kv_w, off, pay, qs, blend, x_all):
+def project_kernel(t0, t1, t2, t3, conv_w, q_w, kv_w, off, pay, pay_x, qs, blend, tail, x_all):
     rows = t0.shape[0]
     me = lax.axis_index("tp")
     for k, t in enumerate((t0, t1, t2, t3)):
@@ -65,32 +66,37 @@
     n = x.shape[0]
     ch = conv_w.shape[1] // 2
     kv = kv_w.shape[1] // 2
-    pay[0:n, :] = dot(x, kv_w[...]).astype(bf16)
+    rows_kv = dot(x, kv_w[...]).astype(bf16)
+    pay[0:n, :] = rows_kv
+    pay_x[0:n, :] = rows_kv
     q = dot(x, q_w[...]).astype(bf16)
     for h in range(q.shape[1] // HEAD_DIM):
         qs[h * n : (h + 1) * n, :] = q[:, h * HEAD_DIM : (h + 1) * HEAD_DIM]
     both = dot(x, conv_w[...]).astype(bf16).astype(f32)
     b = (both[:, 0:ch] * jax.nn.sigmoid(both[:, ch:])).astype(bf16)
     blend[...] = b
-    head = b[n - 32 : n - 16, :].astype(f32)
-    row = lax.broadcasted_iota(jnp.int32, head.shape, 0)
+    tail[...] = b[n - tail.shape[0] :, :]
+    row = lax.broadcasted_iota(jnp.int32, (8, kv), 0)
     offs = off[...].astype(f32)
+    head = jnp.zeros((8, kv), f32)
     for h in range(off.shape[0]):
         head = jnp.where(row == h, offs[h : h + 1, :], head)
-    pay[n:, 0:kv] = head.astype(bf16)
-    pay[n:, kv:] = b[n - 16 :, :]
-
-
-def conv_kernel(p1, p3, p7, blend, taps, field, stats, wide):
+    for out in (pay, pay_x):
+        out[n : n + 8, 0:kv] = head.astype(bf16)
+        out[n : n + 8, kv:] = jnp.zeros((8, kv), bf16)
+    pay_x[n + 8 :, 0:kv] = b[n - 32 : n - 16, :]
+    pay_x[n + 8 :, kv:] = b[n - 16 :, :]
+
+
+def conv_kernel(even, odd, blend, taps, field, stats, wide):
     n = blend.shape[0]
-    half = p1.shape[1] // 2
-    reach = taps.shape[0] - 1
+    kv = odd.shape[1] // 2
     me = lax.axis_index("sp")
-    flip = me ^ (me - 1)
-    halo = jnp.where(flip == 1, p1[n:, :], jnp.where(flip == 3, p3[n:, :], p7[n:, :]))
-    halo = jnp.where(me > 0, halo.astype(f32), 0.0)
-    wide[0:16, :] = halo[:, 0:half]
-    wide[16:32, :] = halo[:, half:]
+    right = me & 1 == 1
+    for half in (0, 1):
+        fill = odd[n + 8 :, half * kv : (half + 1) * kv].astype(f32)
+        rest = jnp.where(me > 0, even[16 * half : 16 * half + 16, :].astype(f32), 0.0)
+        wide[16 * half : 16 * half + 16, :] = jnp.where(right, fill, rest)
     convolve(blend, taps, field, stats, wide)
 
 
@@ -116,6 +122,20 @@
     stats[1:2, :] = jnp.transpose(jnp.broadcast_to(m2, (n, 128)))[0:1, :]
 
 
+def both_stats(a, b, count):
+    gap = a[0:1, :] - b[0:1, :]
+    return (a[0:1, :] + b[0:1, :]) / 2, a[1:2, :] + b[1:2, :] + gap * gap * (count / 2)
+
+
+def pair_kernel(stats, peer, out, *, ch):
+    out[0:1, :], out[1:2, :] = both_stats(stats, peer, ch)
+
+
+def join_kernel(za, zb, joined):
+    joined[0] = za[...]
+    joined[1] = zb[...]
+
+
 def shares(q, pays, own, n, per, tri):
     scale = LOG2E * HEAD_DIM ** (-0.5)
     takes, splits, outs = [], [], []
@@ -123,7 +143,7 @@
         s = lax.dot_general(
             q, pay[0:n, 0:HEAD_DIM], (((1,), (1,)), ((), ())), preferred_element_type=f32
         )
-        off = pay[n : n + 16, 0:HEAD_DIM].astype(f32) * LOG2E
+        off = pay[n : n + 8, 0:HEAD_DIM].astype(f32) * LOG2E
         shift = [jnp.broadcast_to(off[h : h + 1, :], (n, n)) for h in range(per)]
         u = s * scale + jnp.concatenate(shift, axis=0)
         soft = jnp.log2(1.0 + jnp.exp2(-jnp.abs(u)))
@@ -175,7 +195,7 @@
 
 def parts_kernel(*refs, slots, blocks, n, per):
     q_ref = refs[0]
-    pays = refs[1 : 1 + len(slots)]
+    pays = views(refs[1:-1])
     sums = refs[-1]
     me = lax.axis_index("sp")
     found = shares(q_ref[...], pays, [k == 0 for k in slots], n, per, tri_of(n))
@@ -188,9 +208,16 @@
         sums[pl.ds(blocks + j, 1)] = total[None]
 
 
+def views(refs):
+    flat = []
+    for ref in refs:
+        flat += [ref] if len(ref.shape) == 2 else [ref.at[i] for i in range(ref.shape[0])]
+    return flat
+
+
 def stick_kernel(q_ref, *refs, slots, blocks, members, n, per):
-    pays = refs[: len(slots)]
-    s_gain, out_w, _, stick, sums, mix = refs[len(slots) :]
+    s_gain, out_w, _, stick, sums, mix = refs[-6:]
+    pays = views(refs[:-6])
     me = lax.axis_index("sp")
     late = shares(q_ref[...], pays, [False] * len(slots), n, per, tri_of(n))
     for k, (part, total) in zip(slots, late):
@@ -225,12 +252,9 @@
     stick[...] = dot(by_slot(mix, n, members), out_w[ch:, :])
 
 
-def finish_kernel(field, s0, s1, s2, s3, c_gain, out_w, stick, mine, other, send, mix, *, members):
+def finish_kernel(field, near, far, c_gain, out_w, stick, mine, other, send, mix, *, members):
     n, ch = field.shape
-    stats = (s0, s1, s2, s3)
-    mean = sum(st[0:1, :] for st in stats) / members
-    m2 = sum(st[1:2, :] for st in stats)
-    m2 = m2 + ch * sum((st[0:1, :] - mean) ** 2 for st in stats)
+    mean, m2 = both_stats(near, far, ch * members // 2)
     rstd = lax.rsqrt(m2 / (ch * members) + norm_eps)
     mean_c = jnp.transpose(jnp.broadcast_to(mean, (ch, n)))
     rstd_c = jnp.transpose(jnp.broadcast_to(rstd, (ch, n)))
@@ -258,7 +282,6 @@
         out_specs=[in_vmem] * len(outs),
         scratch_shapes=scratch,
         input_output_aliases=aliases,
-        name=getattr(body, "func", body).__name__,
         cost_estimate=pl.CostEstimate(flops=flops, transcendentals=0, bytes_accessed=0),
         compiler_params=pltpu.CompilerParams(vmem_limit_bytes=limit),
     )(*args)
@@ -319,62 +342,72 @@
     )(*[pltpu.with_memory_space_constraint(source, pltpu.HBM) for source in sources])
     by_chip, tok = lax.optimization_barrier((by_chip, tok))
     by_both = swap(by_chip, "tp", 1)
-    pay, qs, blend = call(
+    pay, pay_x, qs, blend, tail = call(
         project_kernel,
-        [((n + 16, 2 * kv), bf16), ((per * n, HEAD_DIM), bf16), ((n, ch), bf16)],
+        [
+            ((n + 8, 2 * kv), bf16),
+            ((n + 24, 2 * kv), bf16),
+            ((per * n, HEAD_DIM), bf16),
+            ((n, ch), bf16),
+            ((32, ch), bf16),
+        ],
         [tok, by_core, by_chip, by_both, conv_w, q_w, kv_w, off],
         scratch=[pltpu.VMEM((n, width), bf16)],
         flops=2 * n * width * (2 * ch + 4 * kv),
     )
-    field_shapes = [((n, ch), f32), ((8, n), f32)]
-    wide = [pltpu.VMEM((n + 32, ch), f32)]
     sizes = dict(n=n, per=per)
     heads = per * n
     mixed = [pltpu.VMEM((n, query_cols), bf16)]
     block_flops = 2 * heads * n * HEAD_DIM * 8
+    stat = ((8, n), f32)
     if blocks == 8:
         z2 = swap(pay, "sp", 2)
         z6 = swap(pay, "sp", 6)
         z4 = swap(pay, "sp", 4)
-        x1 = swap(pay, "sp", 1)
-        x7 = swap(z6, "sp", 1)
+        x1 = swap(pay_x, "sp", 1)
         x3 = swap(z2, "sp", 1)
-        x5 = swap(z4, "sp", 1)
-
-        def parts(slots, pays, sums):
-            args = [qs, *pays] + ([] if sums is None else [sums])
-            (out,) = call(
-                functools.partial(parts_kernel, slots=slots, blocks=blocks, **sizes),
-                [((2 * blocks, heads, HEAD_DIM), f32)],
-                args,
-                flops=len(slots) * block_flops,
-                aliases={} if sums is None else {len(args) - 1: 0},
-            )
-            return out
-
-        sums = parts((0, 2, 6, 1, 4), (pay, z2, z6, x1, z4), None)
-        conv_args = [x1, x3, x7, blend, taps]
-        field, stats = call(conv_kernel, field_shapes, conv_args, wide, 64 * n * ch)
-        all_stats = [stats] + [swap(stats, "tp", k) for k in (2, 3, 1)]
+        pairs = []
+        for i in range(1, blocks - 1, 2):
+            pairs += [(i, i + 1), (i + 1, i)]
+        even = lax.ppermute(tail, "sp", pairs)
+        conv_body = conv_kernel
+        conv_args = [even, x1, blend, taps]
+    else:
+        pays = lax.all_gather(pay, "sp", axis=0)
+        conv_body = conv_plain_kernel
+        conv_args = [from_behind(tail, "sp", 1), blend, taps]
+    field, stats = call(
+        conv_body,
+        [((n, ch), f32), stat],
+        conv_args,
+        [pltpu.VMEM((n + 32, ch), f32)],
+        64 * n * ch,
+    )
+    peer = swap(stats, "tp", 1)
+    (near,) = call(functools.partial(pair_kernel, ch=ch), [stat], [stats, peer])
+    if blocks == 8:
+        (z46,) = call(join_kernel, [((2, n + 8, 2 * kv), bf16)], [z4, z6])
+        x57 = swap(z46, "sp", 1)
+        (sums,) = call(
+            functools.partial(parts_kernel, slots=(0, 2, 1, 4, 6), blocks=blocks, **sizes),
+            [((2 * blocks, heads, HEAD_DIM), f32)],
+            [qs, pay, z2, x1, z46],
+            flops=5 * block_flops,
+        )
         body = functools.partial(
-            stick_kernel, slots=(3, 7, 5), blocks=blocks, members=members, **sizes
+            stick_kernel, slots=(3, 5, 7), blocks=blocks, members=members, **sizes
         )
-        stick_args = [qs, x3, x7, x5, s_gain, out_w, sums]
+        stick_args = [qs, x3, x57, s_gain, out_w, sums]
         stick_outs = [((2 * blocks, heads, HEAD_DIM), f32)]
-        aliases = {6: 1}
+        aliases = {5: 1}
         spaces = None
     else:
-        pays = lax.all_gather(pay, "sp", axis=0)
-        halo = from_behind(blend[n - 32 :], "sp", 1)
-        field, stats = call(
-            conv_plain_kernel, field_shapes, [halo, blend, taps], wide, 64 * n * ch
-        )
-        all_stats = [stats] + [swap(stats, "tp", k) for k in (2, 3, 1)]
         body = functools.partial(stick_loop_kernel, members=members, **sizes)
         stick_args = [qs, pays, s_gain, out_w]
         stick_outs = []
         aliases = {}
         spaces = [True, False, True, True]
+    far = swap(near, "tp", 2)
     stick, *_ = call(
         body,
         [((n, width), f32)] + stick_outs,
@@ -388,7 +421,7 @@
     mine, other, send = call(
         functools.partial(finish_kernel, members=members),
         [((rows, width), f32), ((rows, width), f32), ((2 * rows, width), bf16)],
-        [field, *all_stats, c_gain, out_w, stick],
+        [field, near, far, c_gain, out_w, stick],
         scratch=[pltpu.VMEM((n, ch), bf16)],
         flops=2 * n * width * ch,
     )

time: 37.1 us -> 40.1 us (1.081)
  waiting for transfers between devices: 13.7 us -> 18.2 us
  starting transfers between devices: 16.6 us -> 15 us
    ppermute x15 -> x13, waiting for transfers between devices: 13.7 us -> 18.2 us  [swap(): return lax.ppermute(value, axis, [(i, i ^ by) for i in range(count)])]
    ppermute x15 -> x13, starting transfers between devices: 16.6 us -> 14.4 us  [swap(): return lax.ppermute(value, axis, [(i, i ^ by) for i in range(count)])]
    ppermute x0 -> x1, starting transfers between devices: none -> 0.65 us  [shards(): even = lax.ppermute(tail, 'sp', pairs)]
    pallas_call x5 -> x7, Pallas kernels: 3.31 us -> 3.31 us  [call(): pl.pallas_call(body, out_shape=[pltpu.VMEM(shape, dtype) for shape, dtype...]
  transfers between devices with their start and end apart: 15 -> 14, of which waited for: 8 -> 9; matrix products, arithmetic and copies ran while one was open for 0% -> 0% of each run, Pallas kernels for 13% -> 12%
where the time goes in v6:
time: 40.1 us; the launch traced here: 39.9 us
  waiting for transfers between devices  18.2 us (45%)
  starting transfers between devices  15 us (37%)
  Pallas kernels  5.83 us (15%)
  other arithmetic  0.76 us (2%)
    ppermute x13, waiting for transfers between devices, swap(): return lax.ppermute(value, axis, [(i, i ^ by) for i in range(count)])  18.2 us
    ppermute x13, starting transfers between devices, swap(): return lax.ppermute(value, axis, [(i, i ^ by) for i in range(count)])  14.4 us
    pallas_call x7, Pallas kernels, call(): pl.pallas_call(body, out_shape=[pltpu.VMEM(shape, dtype) for shape, dtype...  3.31 us
    pallas_call x1, Pallas kernels, shards(): pl.pallas_call(load_kernel, out_shape=[pltpu.VMEM(shape, dtype) for shape...  2.52 us
  transfers between devices with their start and end apart: 14, of which 9 were waited for; matrix products, arithmetic and copies ran while one was open for 0% of the time, Pallas kernels for 12%

profile of v6, /device:TPU:0, one launch (start us, length us, event | category | flops | bytes accessed | tf_op | source)
XLA Modules:
  0.0 39.9 jit_solution(11094740022658964586)
XLA Ops:
  0.0 3.0 %collective-permute-start = (bf16[32,2048]{1,0:T(8,128)(2,1)}, bf16[32,2048]{1,0:T(8,128)(2,1)S(1)}, u32[]{:S(2)}, u32[]{:S(2)}) collective-permute-start(bf16[32,2048]{1,0:T(8,128)(2,1)} %refs_0_.1), channel_id=1, source_target_pairs={{0,2},{1,3},{2,0},{3,1},{4,6},{5,7},{6,4},{7,5},{8,10},{9,11},{10,... | collective-permute-start | bytes 393224 | tf_op jit(solution)/shard_map/ppermute | solution.py:20
  3.0 2.5 %shard_map.118 = (bf16[32,2048]{1,0:T(8,128)(2,1)S(1)}, bf16[2048,256]{1,0:T(8,128)(2,1)S(1)}, bf16[2048,256]{1,0:T(8,128)(2,1)S(1)}, bf16[2048,256]{1,0:T(8,128...) custom-call(bf16[32,2048]{1,0:T(8,128)(2,1)} %refs_0_.1, ...), custom_call_target="tpu_custom_call" | custom-call | flops 1000000000 | bytes 5000000 | tf_op jit(solution)/shard_map/pallas_call | solution.py:321
  5.5 1.2 %collective-permute-done.t2 = bf16[32,2048]{1,0:T(8,128)(2,1)S(1)} collective-permute-done((bf16[32,2048]{1,0:T(8,128)(2,1)}, bf16[32,2048]{1,0:T(8,128)(2,1)S(1)}, u32[]{:S(2)}, u32[]{:S(2)}) %collective-permute-start) | collective-permute-done | bytes 131104 | tf_op jit(solution)/shard_map/ppermute | solution.py:20
  6.7 1.3 %collective-permute-done.2.t3 = bf16[32,2048]{1,0:T(8,128)(2,1)S(1)} collective-permute-done((bf16[32,2048]{1,0:T(8,128)(2,1)S(1)}, bf16[32,2048]{1,0:T(8,128)(2,1)S(1)}, u32[]{:S(2)}, u32[]{:S(2)}) %collective-permute-start.2) | collective-permute-done | bytes 131104 | tf_op jit(solution)/shard_map/ppermute | solution.py:20
  8.0 0.6 %shard_map.119 = (bf16[136,256]{1,0:T(8,128)(2,1)S(1)}, bf16[152,256]{1,0:T(8,128)(2,1)S(1)}, bf16[256,128]{1,0:T(8,128)(2,1)S(1)}, bf16[128,128]{1,0:T(8,128)(2,1)S(1)}, bf16[32,128]{1,0:T(8,128)(2,1)S(1)}) custom-call(bf16[32,2048]{1,0:T(8,128)(2,1)S(1)} %get-tuple-element.28.t0, bf16[32,2048]{1,0:T(8,128)(2,1)S(1)} %collective-permute-done.1.t1, ...), custom_call_target="tpu_custom_call" | custom-call | flops 402653184 | tf_op jit(solution)/shard_map/pallas_call | solution.py:278
  8.7 3.9 %collective-permute-start.10 = (bf16[136,256]{1,0:T(8,128)(2,1)S(1)}, bf16[136,256]{1,0:T(8,128)(2,1)S(1)}, u32[]{:S(2)}, u32[]{:S(2)}) collective-permute-start(bf16[136,256]{1,0:T(8,128)(2,1)S(1)} %get-tuple-element.43.refs_1_), channel_id=1, source_target_pairs={{0,24},{4,28},{8,16},{12,20},{16,8},{20,12},{24,0},{28,4},{1,25},{... | collective-permute-start | bytes 208904 | tf_op jit(solution)/shard_map/ppermute | solution.py:20
  12.6 0.6 %collective-permute-start.7 = (bf16[136,256]{1,0:T(8,128)(2,1)S(1)}, bf16[136,256]{1,0:T(8,128)(2,1)S(1)}, u32[]{:S(2)}, u32[]{:S(2)}) collective-permute-start(bf16[136,256]{1,0:T(8,128)(2,1)S(1)} %get-tuple-element.43.refs_1_), channel_id=1, source_target_pairs={{0,8},{4,12},{8,0},{12,4},{16,24},{20,28},{24,16},{28,20},{1,9},{5... | collective-permute-start | bytes 208904 | tf_op jit(solution)/shard_map/ppermute | solution.py:20
  13.2 2.1 %collective-permute-done.10.zb = bf16[136,256]{1,0:T(8,128)(2,1)S(1)} collective-permute-done((bf16[136,256]{1,0:T(8,128)(2,1)S(1)}, bf16[136,256]{1,0:T(8,128)(2,1)S(1)}, u32[]{:S(2)}, u32[]{:S(2)}) %collective-permute-start.10) | collective-permute-done | bytes 69664 | tf_op jit(solution)/shard_map/ppermute | solution.py:20
  15.3 3.4 %collective-permute-done.9.za = bf16[136,256]{1,0:T(8,128)(2,1)S(1)} collective-permute-done((bf16[136,256]{1,0:T(8,128)(2,1)S(1)}, bf16[136,256]{1,0:T(8,128)(2,1)S(1)}, u32[]{:S(2)}, u32[]{:S(2)}) %collective-permute-start.9) | collective-permute-done | bytes 69664 | tf_op jit(solution)/shard_map/ppermute | solution.py:20
  18.8 1.6 %collective-permute-start.11 = (bf16[2,136,256]{2,1,0:T(8,128)(2,1)S(1)}, bf16[2,136,256]{2,1,0:T(8,128)(2,1)S(1)}, u32[]{:S(2)}, u32[]{:S(2)}) collective-permute-start(bf16[2,136,256]{2,1,0:T(8,128)(2,1)S(1)} %shard_map.122.refs_4_), channel_id=1, source_target_pairs={{0,4},{4,0},{8,12},{12,8},{16,20},{20,16},{24,28},{28,24},{1,5},{5... | collective-permute-start | bytes 417800 | tf_op jit(solution)/shard_map/ppermute | solution.py:20
  20.3 0.5 %collective-permute-start.4 = (bf16[152,256]{1,0:T(8,128)(2,1)S(1)}, bf16[152,256]{1,0:T(8,128)(2,1)S(1)}, u32[]{:S(2)}, u32[]{:S(2)}) collective-permute-start(bf16[152,256]{1,0:T(8,128)(2,1)S(1)} %get-tuple-element.35), channel_id=1, source_target_pairs={{0,4},{4,0},{8,12},{12,8},{16,20},{20,16},{24,28},{28,24},{1,5},{5... | collective-permute-start | bytes 233480 | tf_op jit(solution)/shard_map/ppermute | solution.py:20
  20.9 1.5 %collective-permute-start.8 = (bf16[136,256]{1,0:T(8,128)(2,1)S(1)}, bf16[136,256]{1,0:T(8,128)(2,1)S(1)}, u32[]{:S(2)}, u32[]{:S(2)}) collective-permute-start(bf16[136,256]{1,0:T(8,128)(2,1)S(1)} %collective-permute-done.7.refs_2_), channel_id=1, source_target_pairs={{0,4},{4,0},{8,12},{12,8},{16,20},{20,16},{24,28},{28,24},{1,5},{5... | collective-permute-start | bytes 208904 | tf_op jit(solution)/shard_map/ppermute | solution.py:20
  22.4 0.6 %collective-permute-start.3 = (bf16[32,128]{1,0:T(8,128)(2,1)S(1)}, bf16[32,128]{1,0:T(8,128)(2,1)S(1)}, u32[]{:S(2)}, u32[]{:S(2)}) collective-permute-start(bf16[32,128]{1,0:T(8,128)(2,1)S(1)} %get-tuple-element.34), channel_id=1, source_target_pairs={{4,8},{8,4},{12,16},{16,12},{20,24},{24,20},{5,9},{9,5},{13,17},{1... | collective-permute-start | bytes 24584 | tf_op jit(solution)/shard_map/ppermute | solution.py:372
  23.0 3.3 %collective-permute-done.4.odd.refs_3_ = bf16[152,256]{1,0:T(8,128)(2,1)S(1)} collective-permute-done((bf16[152,256]{1,0:T(8,128)(2,1)S(1)}, bf16[152,256]{1,0:T(8,128)(2,1)S(1)}, u32[]{:S(2)}, u32[]{:S(2)}) %collective-permute-start.4) | collective-permute-done | bytes 77856 | tf_op jit(solution)/shard_map/ppermute | solution.py:20
  26.3 0.4 shard_map.120
  26.8 0.8 %shard_map.123.refs_4_ = f32[16,256,128]{2,1,0:T(8,128)S(1)} custom-call(bf16[256,128]{1,0:T(8,128)(2,1)S(1)} %get-tuple-element.42.refs_0_.q_ref, bf16[136,256]{1,0:T(8,128)(2,1)S(1)} %get-tuple-element.43.refs_1_, bf16[136,256]{1,0:T(8,128)(2,1)S(1)} %collective-permute-done.7.refs_2_, bf16[152,256]{1,0:T(8,128)(2,1)S(1)} %collective-permute-done.4.odd.refs_3_, ...), custom_call_target="tpu_custom_call" | custom-call | flops 335544320 | tf_op jit(solution)/shard_map/pallas_call | solution.py:278
  27.9 1.5 %collective-permute-start.6 = (f32[8,128]{1,0:T(8,128)S(1)}, f32[8,128]{1,0:T(8,128)S(1)}, u32[]{:S(2)}, u32[]{:S(2)}) collective-permute-start(f32[8,128]{1,0:T(8,128)S(1)} %shard_map.121.near), channel_id=1, source_target_pairs={{0,2},{1,3},{2,0},{3,1},{4,6},{5,7},{6,4},{7,5},{8,10},{9,11},{10,... | collective-permute-start | bytes 12296 | tf_op jit(solution)/shard_map/ppermute | solution.py:20
  29.5 1.1 %shard_map.124 = (f32[128,2048]{1,0:T(8,128)S(1)}, f32[16,256,128]{2,1,0:T(8,128)S(1)}) custom-call(bf16[256,128]{1,0:T(8,128)(2,1)S(1)} %get-tuple-element.42.refs_0_.q_ref, bf16[136,256]{1,0:T(8,128)(2,1)S(1)} %collective-permute-done.8.refs_0_, bf16[2,136,256]{2,1,0:T(8,128)(2,1)S(1)} %collective-permute-done.11.refs_1_, ...), custom_call_target="tpu_custom_call", output_to_operand_aliasing={{1}: (5, {})} | custom-call | flops 201326592 | tf_op jit(solution)/shard_map/pallas_call | solution.py:278
  30.6 0.9 %collective-permute-done.6.far = f32[8,128]{1,0:T(8,128)S(1)} collective-permute-done((f32[8,128]{1,0:T(8,128)S(1)}, f32[8,128]{1,0:T(8,128)S(1)}, u32[]{:S(2)}, u32[]{:S(2)}) %collective-permute-start.6) | collective-permute-done | bytes 4128 | tf_op jit(solution)/shard_map/ppermute | solution.py:20
  31.5 0.4 shard_map.125
  32.0 1.5 %collective-permute-done.12 = bf16[64,2048]{1,0:T(8,128)(2,1)S(1)} collective-permute-done((bf16[64,2048]{1,0:T(8,128)(2,1)S(1)}, bf16[64,2048]{1,0:T(8,128)(2,1)S(1)}, u32[]{:S(2)}, u32[]{:S(2)}) %collective-permute-start.12) | collective-permute-done | bytes 262176 | tf_op jit(solution)/shard_map/ppermute | solution.py:20
  33.6 1.6 %collective-permute-start.13 = (bf16[32,2048]{1,0:T(8,128)(2,1)S(1)}, bf16[32,2048]{1,0:T(8,128)(2,1)S(1)}, u32[]{:S(2)}, u32[]{:S(2)}) collective-permute-start(bf16[32,2048]{1,0:T(8,128)(2,1)S(1)} %fusion), channel_id=1, source_target_pairs={{0,2},{1,3},{2,0},{3,1},{4,6},{5,7},{6,4},{7,5},{8,10},{9,11},{10,... | collective-permute-start | bytes 393224 | tf_op jit(solution)/shard_map/ppermute | solution.py:20
  35.2 4.0 %collective-permute-done.13 = bf16[32,2048]{1,0:T(8,128)(2,1)S(1)} collective-permute-done((bf16[32,2048]{1,0:T(8,128)(2,1)S(1)}, bf16[32,2048]{1,0:T(8,128)(2,1)S(1)}, u32[]{:S(2)}, u32[]{:S(2)}) %collective-permute-start.13) | collective-permute-done | bytes 131104 | tf_op jit(solution)/shard_map/ppermute | solution.py:20
  39.2 0.7 %fusion.2 = bf16[32,2048]{1,0:T(8,128)(2,1)} fusion(f32[32,2048]{1,0:T(8,128)S(1)} %get-tuple-element.46, f32[64,2048]{1,0:T(8,128)S(1)} %convert_element_type.12, bf16[32,2048]{1,0:T(8,128)(2,1)S(1)} %collective-permute-done.13), kind=kLoop, calls=%fused_computation.4 | loop fusion | flops 262144 | bytes 786432 | tf_op jit(solution)/shard_map/convert_element_type | solution.py:430
  (15 shorter events, 0.6 us)
Async XLA Ops:
  0.0 6.7 %collective-permute-start = (bf16[32,2048]{1,0:T(8,128)(2,1)}, bf16[32,2048]{1,0:T(8,128)(2,1)S(1)}, u32[]{:S(2)}, u32[]{:S(2)}) collective-permute-start(bf16[32,2048]{1,0:T(8,128)(2,1)} %refs_0_.1), channel_id=1, source_target_pairs={{0,2},{1,3},{2,0},{3,1},{4,6},{5,7},{6,4},{7,5},{8,10},{9,11},{10,... | collective-permute-start | bytes 393224 | tf_op jit(solution)/shard_map/ppermute | solution.py:20
  3.0 3.7 %collective-permute-start.1 = (bf16[32,2048]{1,0:T(8,128)(2,1)}, bf16[32,2048]{1,0:T(8,128)(2,1)S(1)}, u32[]{:S(2)}, u32[]{:S(2)}) collective-permute-start(bf16[32,2048]{1,0:T(8,128)(2,1)} %refs_0_.1), channel_id=1, source_target_pairs={{0,1},{1,0},{2,3},{3,2},{4,5},{5,4},{6,7},{7,6},{8,9},{9,8},{10,11... | collective-permute-start | bytes 393224 | tf_op jit(solution)/shard_map/ppermute | solution.py:20
  6.7 1.3 %collective-permute-start.2 = (bf16[32,2048]{1,0:T(8,128)(2,1)S(1)}, bf16[32,2048]{1,0:T(8,128)(2,1)S(1)}, u32[]{:S(2)}, u32[]{:S(2)}) collective-permute-start(bf16[32,2048]{1,0:T(8,128)(2,1)S(1)} %collective-permute-done.t2), channel_id=1, source_target_pairs={{0,1},{1,0},{2,3},{3,2},{4,5},{5,4},{6,7},{7,6},{8,9},{9,8},{10,11... | collective-permute-start | bytes 393224 | tf_op jit(solution)/shard_map/ppermute | solution.py:20
  8.7 6.7 %collective-permute-start.10 = (bf16[136,256]{1,0:T(8,128)(2,1)S(1)}, bf16[136,256]{1,0:T(8,128)(2,1)S(1)}, u32[]{:S(2)}, u32[]{:S(2)}) collective-permute-start(bf16[136,256]{1,0:T(8,128)(2,1)S(1)} %get-tuple-element.43.refs_1_), channel_id=1, source_target_pairs={{0,24},{4,28},{8,16},{12,20},{16,8},{20,12},{24,0},{28,4},{1,25},{... | collective-permute-start | bytes 208904 | tf_op jit(solution)/shard_map/ppermute | solution.py:20
  12.6 6.2 %collective-permute-start.9 = (bf16[136,256]{1,0:T(8,128)(2,1)S(1)}, bf16[136,256]{1,0:T(8,128)(2,1)S(1)}, u32[]{:S(2)}, u32[]{:S(2)}) collective-permute-start(bf16[136,256]{1,0:T(8,128)(2,1)S(1)} %get-tuple-element.43.refs_1_), channel_id=1, source_target_pairs={{0,16},{4,20},{8,24},{12,28},{16,0},{20,4},{24,8},{28,12},{1,17},{... | collective-permute-start | bytes 208904 | tf_op jit(solution)/shard_map/ppermute | solution.py:20
  12.6 8.3 %collective-permute-start.7 = (bf16[136,256]{1,0:T(8,128)(2,1)S(1)}, bf16[136,256]{1,0:T(8,128)(2,1)S(1)}, u32[]{:S(2)}, u32[]{:S(2)}) collective-permute-start(bf16[136,256]{1,0:T(8,128)(2,1)S(1)} %get-tuple-element.43.refs_1_), channel_id=1, source_target_pairs={{0,8},{4,12},{8,0},{12,4},{16,24},{20,28},{24,16},{28,20},{1,9},{5... | collective-permute-start | bytes 208904 | tf_op jit(solution)/shard_map/ppermute | solution.py:20
  18.8 10.7 %collective-permute-start.11 = (bf16[2,136,256]{2,1,0:T(8,128)(2,1)S(1)}, bf16[2,136,256]{2,1,0:T(8,128)(2,1)S(1)}, u32[]{:S(2)}, u32[]{:S(2)}) collective-permute-start(bf16[2,136,256]{2,1,0:T(8,128)(2,1)S(1)} %shard_map.122.refs_4_), channel_id=1, source_target_pairs={{0,4},{4,0},{8,12},{12,8},{16,20},{20,16},{24,28},{28,24},{1,5},{5... | collective-permute-start | bytes 417800 | tf_op jit(solution)/shard_map/ppermute | solution.py:20
  20.3 6.0 %collective-permute-start.4 = (bf16[152,256]{1,0:T(8,128)(2,1)S(1)}, bf16[152,256]{1,0:T(8,128)(2,1)S(1)}, u32[]{:S(2)}, u32[]{:S(2)}) collective-permute-start(bf16[152,256]{1,0:T(8,128)(2,1)S(1)} %get-tuple-element.35), channel_id=1, source_target_pairs={{0,4},{4,0},{8,12},{12,8},{16,20},{20,16},{24,28},{28,24},{1,5},{5... | collective-permute-start | bytes 233480 | tf_op jit(solution)/shard_map/ppermute | solution.py:20
  20.9 8.6 %collective-permute-start.8 = (bf16[136,256]{1,0:T(8,128)(2,1)S(1)}, bf16[136,256]{1,0:T(8,128)(2,1)S(1)}, u32[]{:S(2)}, u32[]{:S(2)}) collective-permute-start(bf16[136,256]{1,0:T(8,128)(2,1)S(1)} %collective-permute-done.7.refs_2_), channel_id=1, source_target_pairs={{0,4},{4,0},{8,12},{12,8},{16,20},{20,16},{24,28},{28,24},{1,5},{5... | collective-permute-start | bytes 208904 | tf_op jit(solution)/shard_map/ppermute | solution.py:20
  22.4 0.7 %collective-permute-start.3 = (bf16[32,128]{1,0:T(8,128)(2,1)S(1)}, bf16[32,128]{1,0:T(8,128)(2,1)S(1)}, u32[]{:S(2)}, u32[]{:S(2)}) collective-permute-start(bf16[32,128]{1,0:T(8,128)(2,1)S(1)} %get-tuple-element.34), channel_id=1, source_target_pairs={{4,8},{8,4},{12,16},{16,12},{20,24},{24,20},{5,9},{9,5},{13,17},{1... | collective-permute-start | bytes 24584 | tf_op jit(solution)/shard_map/ppermute | solution.py:372
  26.7 1.2 %collective-permute-start.5 = (f32[8,128]{1,0:T(8,128)S(1)}, f32[8,128]{1,0:T(8,128)S(1)}, u32[]{:S(2)}, u32[]{:S(2)}) collective-permute-start(f32[8,128]{1,0:T(8,128)S(1)} %get-tuple-element.39.stats), channel_id=1, source_target_pairs={{0,1},{1,0},{2,3},{3,2},{4,5},{5,4},{6,7},{7,6},{8,9},{9,8},{10,11... | collective-permute-start | bytes 12296 | tf_op jit(solution)/shard_map/ppermute | solution.py:20
  27.9 3.6 %collective-permute-start.6 = (f32[8,128]{1,0:T(8,128)S(1)}, f32[8,128]{1,0:T(8,128)S(1)}, u32[]{:S(2)}, u32[]{:S(2)}) collective-permute-start(f32[8,128]{1,0:T(8,128)S(1)} %shard_map.121.near), channel_id=1, source_target_pairs={{0,2},{1,3},{2,0},{3,1},{4,6},{5,7},{6,4},{7,5},{8,10},{9,11},{10,... | collective-permute-start | bytes 12296 | tf_op jit(solution)/shard_map/ppermute | solution.py:20
  31.9 1.6 %collective-permute-start.12 = (bf16[64,2048]{1,0:T(8,128)(2,1)S(1)}, bf16[64,2048]{1,0:T(8,128)(2,1)S(1)}, u32[]{:S(2)}, u32[]{:S(2)}) collective-permute-start(bf16[64,2048]{1,0:T(8,128)(2,1)S(1)} %get-tuple-element.47), channel_id=1, source_target_pairs={{0,1},{1,0},{2,3},{3,2},{4,5},{5,4},{6,7},{7,6},{8,9},{9,8},{10,11... | collective-permute-start | bytes 786440 | tf_op jit(solution)/shard_map/ppermute | solution.py:20
  33.6 5.6 %collective-permute-start.13 = (bf16[32,2048]{1,0:T(8,128)(2,1)S(1)}, bf16[32,2048]{1,0:T(8,128)(2,1)S(1)}, u32[]{:S(2)}, u32[]{:S(2)}) collective-permute-start(bf16[32,2048]{1,0:T(8,128)(2,1)S(1)} %fusion), channel_id=1, source_target_pairs={{0,2},{1,3},{2,0},{3,1},{4,6},{5,7},{6,4},{7,5},{8,10},{9,11},{10,... | collective-permute-start | bytes 393224 | tf_op jit(solution)/shard_map/ppermute | solution.py:20

commit v7 on v6

--- a/solution.py
+++ b/solution.py
@@ -57,33 +57,36 @@
         copy.wait()
 
 
-def project_kernel(t0, t1, t2, t3, conv_w, q_w, kv_w, off, pay, pay_x, qs, blend, tail, x_all):
+def keys_kernel(t0, t1, t2, t3, kv_w, off, pay, x_all):
     rows = t0.shape[0]
     me = lax.axis_index("tp")
     for k, t in enumerate((t0, t1, t2, t3)):
         x_all[pl.ds(pl.multiple_of((me ^ k) * rows, rows), rows), :] = t[...]
-    x = x_all[...]
-    n = x.shape[0]
-    ch = conv_w.shape[1] // 2
+    n = x_all.shape[0]
     kv = kv_w.shape[1] // 2
-    rows_kv = dot(x, kv_w[...]).astype(bf16)
-    pay[0:n, :] = rows_kv
-    pay_x[0:n, :] = rows_kv
-    q = dot(x, q_w[...]).astype(bf16)
-    for h in range(q.shape[1] // HEAD_DIM):
-        qs[h * n : (h + 1) * n, :] = q[:, h * HEAD_DIM : (h + 1) * HEAD_DIM]
-    both = dot(x, conv_w[...]).astype(bf16).astype(f32)
-    b = (both[:, 0:ch] * jax.nn.sigmoid(both[:, ch:])).astype(bf16)
-    blend[...] = b
-    tail[...] = b[n - tail.shape[0] :, :]
+    pay[0:n, :] = dot(x_all[...], kv_w[...]).astype(bf16)
     row = lax.broadcasted_iota(jnp.int32, (8, kv), 0)
     offs = off[...].astype(f32)
     head = jnp.zeros((8, kv), f32)
     for h in range(off.shape[0]):
         head = jnp.where(row == h, offs[h : h + 1, :], head)
-    for out in (pay, pay_x):
-        out[n : n + 8, 0:kv] = head.astype(bf16)
-        out[n : n + 8, kv:] = jnp.zeros((8, kv), bf16)
+    pay[n:, 0:kv] = head.astype(bf16)
+    pay[n:, kv:] = jnp.zeros((8, kv), bf16)
+
+
+def project_kernel(x_all, conv_w, q_w, pay, pay_x, qs, blend, tail):
+    x = x_all[...]
+    n = x.shape[0]
+    ch = conv_w.shape[1] // 2
+    kv = pay.shape[1] // 2
+    both = dot(x, conv_w[...]).astype(bf16).astype(f32)
+    q = dot(x, q_w[...]).astype(bf16)
+    for h in range(q.shape[1] // HEAD_DIM):
+        qs[h * n : (h + 1) * n, :] = q[:, h * HEAD_DIM : (h + 1) * HEAD_DIM]
+    b = (both[:, 0:ch] * jax.nn.sigmoid(both[:, ch:])).astype(bf16)
+    blend[...] = b
+    tail[...] = b[n - tail.shape[0] :, :]
+    pay_x[0 : n + 8, :] = pay[...]
     pay_x[n + 8 :, 0:kv] = b[n - 32 : n - 16, :]
     pay_x[n + 8 :, kv:] = b[n - 16 :, :]
 
@@ -122,13 +125,9 @@
     stats[1:2, :] = jnp.transpose(jnp.broadcast_to(m2, (n, 128)))[0:1, :]
 
 
-def both_stats(a, b, count):
-    gap = a[0:1, :] - b[0:1, :]
-    return (a[0:1, :] + b[0:1, :]) / 2, a[1:2, :] + b[1:2, :] + gap * gap * (count / 2)
-
-
-def pair_kernel(stats, peer, out, *, ch):
-    out[0:1, :], out[1:2, :] = both_stats(stats, peer, ch)
+def both_stats(mean_a, m2_a, mean_b, m2_b, count):
+    gap = mean_a - mean_b
+    return (mean_a + mean_b) / 2, m2_a + m2_b + gap * gap * (count / 2)
 
 
 def join_kernel(za, zb, joined):
@@ -252,9 +251,11 @@
     stick[...] = dot(by_slot(mix, n, members), out_w[ch:, :])
 
 
-def finish_kernel(field, near, far, c_gain, out_w, stick, mine, other, send, mix, *, members):
+def finish_kernel(field, own, core, chip, both, c_gain, out_w, stick, mine, other, send, mix, *, members):
     n, ch = field.shape
-    mean, m2 = both_stats(near, far, ch * members // 2)
+    near = both_stats(own[0:1, :], own[1:2, :], core[0:1, :], core[1:2, :], ch)
+    far = both_stats(chip[0:1, :], chip[1:2, :], both[0:1, :], both[1:2, :], ch)
+    mean, m2 = both_stats(*near, *far, 2 * ch)
     rstd = lax.rsqrt(m2 / (ch * members) + norm_eps)
     mean_c = jnp.transpose(jnp.broadcast_to(mean, (ch, n)))
     rstd_c = jnp.transpose(jnp.broadcast_to(rstd, (ch, n)))
@@ -342,18 +343,22 @@
     )(*[pltpu.with_memory_space_constraint(source, pltpu.HBM) for source in sources])
     by_chip, tok = lax.optimization_barrier((by_chip, tok))
     by_both = swap(by_chip, "tp", 1)
-    pay, pay_x, qs, blend, tail = call(
+    pay, x_all = call(
+        keys_kernel,
+        [((n + 8, 2 * kv), bf16), ((n, width), bf16)],
+        [tok, by_core, by_chip, by_both, kv_w, off],
+        flops=2 * n * width * 2 * kv,
+    )
+    pay_x, qs, blend, tail = call(
         project_kernel,
         [
-            ((n + 8, 2 * kv), bf16),
             ((n + 24, 2 * kv), bf16),
             ((per * n, HEAD_DIM), bf16),
             ((n, ch), bf16),
             ((32, ch), bf16),
         ],
-        [tok, by_core, by_chip, by_both, conv_w, q_w, kv_w, off],
-        scratch=[pltpu.VMEM((n, width), bf16)],
-        flops=2 * n * width * (2 * ch + 4 * kv),
+        [x_all, conv_w, q_w, pay],
+        flops=2 * n * width * (2 * ch + query_cols),
     )
     sizes = dict(n=n, per=per)
     heads = per * n
@@ -384,7 +389,8 @@
         64 * n * ch,
     )
     peer = swap(stats, "tp", 1)
-    (near,) = call(functools.partial(pair_kernel, ch=ch), [stat], [stats, peer])
+    chip = swap(stats, "tp", 2)
+    both = swap(stats, "tp", 3)
     if blocks == 8:
         (z46,) = call(join_kernel, [((2, n + 8, 2 * kv), bf16)], [z4, z6])
         x57 = swap(z46, "sp", 1)
@@ -407,7 +413,6 @@
         stick_outs = []
         aliases = {}
         spaces = [True, False, True, True]
-    far = swap(near, "tp", 2)
     stick, *_ = call(
         body,
         [((n, width), f32)] + stick_outs,
@@ -421,7 +426,7 @@
     mine, other, send = call(
         functools.partial(finish_kernel, members=members),
         [((rows, width), f32), ((rows, width), f32), ((2 * rows, width), bf16)],
-        [field, near, far, c_gain, out_w, stick],
+        [field, stats, peer, chip, both, c_gain, out_w, stick],
         scratch=[pltpu.VMEM((n, ch), bf16)],
         flops=2 * n * width * ch,
     )

time: 40.1 us -> 39.5 us (0.985); the launches traced: 39.9 us -> 38.8 us
  waiting for transfers between devices: 18.2 us -> 16.3 us
  starting transfers between devices: 15 us -> 15.6 us
    ppermute x13 -> x14, waiting for transfers between devices: 18.2 us -> 16.3 us  [swap(): return lax.ppermute(value, axis, [(i, i ^ by) for i in range(count)])]
    ppermute x13 -> x14, starting transfers between devices: 14.4 us -> 15 us  [swap(): return lax.ppermute(value, axis, [(i, i ^ by) for i in range(count)])]
  transfers between devices with their start and end apart: 14 -> 15, of which waited for: 9 -> 7; matrix products, arithmetic and copies ran while one was open for 0% -> 0% of each run, Pallas kernels for 12% -> 14%
where the time goes in v7:
time: 39.5 us; the launch traced here: 38.8 us
  waiting for transfers between devices  16.3 us (41%)
  starting transfers between devices  15.6 us (39%)
  Pallas kernels  6.03 us (15%)
  other arithmetic  0.76 us (2%)
    ppermute x14, waiting for transfers between devices, swap(): return lax.ppermute(value, axis, [(i, i ^ by) for i in range(count)])  16.3 us
    ppermute x14, starting transfers between devices, swap(): return lax.ppermute(value, axis, [(i, i ^ by) for i in range(count)])  15 us
    pallas_call x7, Pallas kernels, call(): pl.pallas_call(body, out_shape=[pltpu.VMEM(shape, dtype) for shape, dtype...  3.51 us
    pallas_call x1, Pallas kernels, shards(): pl.pallas_call(load_kernel, out_shape=[pltpu.VMEM(shape, dtype) for shape...  2.52 us
  transfers between devices with their start and end apart: 15, of which 7 were waited for; matrix products, arithmetic and copies ran while one was open for 0% of the time, Pallas kernels for 14%

profile of v7, /device:TPU:0, one launch (start us, length us, event | category | flops | bytes accessed | tf_op | source)
XLA Modules:
  0.0 38.8 jit_solution(821775205520630459)
XLA Ops:
  0.0 3.0 %collective-permute-start = (bf16[32,2048]{1,0:T(8,128)(2,1)}, bf16[32,2048]{1,0:T(8,128)(2,1)S(1)}, u32[]{:S(2)}, u32[]{:S(2)}) collective-permute-start(bf16[32,2048]{1,0:T(8,128)(2,1)} %refs_0_.1), channel_id=1, source_target_pairs={{0,2},{1,3},{2,0},{3,1},{4,6},{5,7},{6,4},{7,5},{8,10},{9,11},{10,... | collective-permute-start | bytes 393224 | tf_op jit(solution)/shard_map/ppermute | solution.py:20
  3.0 2.5 %shard_map.118 = (bf16[32,2048]{1,0:T(8,128)(2,1)S(1)}, bf16[2048,256]{1,0:T(8,128)(2,1)S(1)}, bf16[2048,256]{1,0:T(8,128)(2,1)S(1)}, bf16[2048,256]{1,0:T(8,128...) custom-call(bf16[32,2048]{1,0:T(8,128)(2,1)} %refs_0_.1, ...), custom_call_target="tpu_custom_call" | custom-call | flops 1000000000 | bytes 5000000 | tf_op jit(solution)/shard_map/pallas_call | solution.py:322
  5.5 1.2 %collective-permute-done.t2 = bf16[32,2048]{1,0:T(8,128)(2,1)S(1)} collective-permute-done((bf16[32,2048]{1,0:T(8,128)(2,1)}, bf16[32,2048]{1,0:T(8,128)(2,1)S(1)}, u32[]{:S(2)}, u32[]{:S(2)}) %collective-permute-start) | collective-permute-done | bytes 131104 | tf_op jit(solution)/shard_map/ppermute | solution.py:20
  6.7 1.3 %collective-permute-done.2.t3 = bf16[32,2048]{1,0:T(8,128)(2,1)S(1)} collective-permute-done((bf16[32,2048]{1,0:T(8,128)(2,1)S(1)}, bf16[32,2048]{1,0:T(8,128)(2,1)S(1)}, u32[]{:S(2)}, u32[]{:S(2)}) %collective-permute-start.2) | collective-permute-done | bytes 131104 | tf_op jit(solution)/shard_map/ppermute | solution.py:20
  8.0 0.3 shard_map.119
  8.4 3.9 %collective-permute-start.11 = (bf16[136,256]{1,0:T(8,128)(2,1)S(1)}, bf16[136,256]{1,0:T(8,128)(2,1)S(1)}, u32[]{:S(2)}, u32[]{:S(2)}) collective-permute-start(bf16[136,256]{1,0:T(8,128)(2,1)S(1)} %get-tuple-element.36.pay.refs_1_), channel_id=1, source_target_pairs={{0,24},{4,28},{8,16},{12,20},{16,8},{20,12},{24,0},{28,4},{1,25},{... | collective-permute-start | bytes 208904 | tf_op jit(solution)/shard_map/ppermute | solution.py:20
  12.3 0.6 %collective-permute-start.8 = (bf16[136,256]{1,0:T(8,128)(2,1)S(1)}, bf16[136,256]{1,0:T(8,128)(2,1)S(1)}, u32[]{:S(2)}, u32[]{:S(2)}) collective-permute-start(bf16[136,256]{1,0:T(8,128)(2,1)S(1)} %get-tuple-element.36.pay.refs_1_), channel_id=1, source_target_pairs={{0,8},{4,12},{8,0},{12,4},{16,24},{20,28},{24,16},{28,20},{1,9},{5... | collective-permute-start | bytes 208904 | tf_op jit(solution)/shard_map/ppermute | solution.py:20
  12.9 2.1 %collective-permute-done.11.zb = bf16[136,256]{1,0:T(8,128)(2,1)S(1)} collective-permute-done((bf16[136,256]{1,0:T(8,128)(2,1)S(1)}, bf16[136,256]{1,0:T(8,128)(2,1)S(1)}, u32[]{:S(2)}, u32[]{:S(2)}) %collective-permute-start.11) | collective-permute-done | bytes 69664 | tf_op jit(solution)/shard_map/ppermute | solution.py:20
  15.1 3.4 %collective-permute-done.10.za = bf16[136,256]{1,0:T(8,128)(2,1)S(1)} collective-permute-done((bf16[136,256]{1,0:T(8,128)(2,1)S(1)}, bf16[136,256]{1,0:T(8,128)(2,1)S(1)}, u32[]{:S(2)}, u32[]{:S(2)}) %collective-permute-start.10) | collective-permute-done | bytes 69664 | tf_op jit(solution)/shard_map/ppermute | solution.py:20
  18.5 1.6 %collective-permute-start.12 = (bf16[2,136,256]{2,1,0:T(8,128)(2,1)S(1)}, bf16[2,136,256]{2,1,0:T(8,128)(2,1)S(1)}, u32[]{:S(2)}, u32[]{:S(2)}) collective-permute-start(bf16[2,136,256]{2,1,0:T(8,128)(2,1)S(1)} %shard_map.122.refs_4_), channel_id=1, source_target_pairs={{0,4},{4,0},{8,12},{12,8},{16,20},{20,16},{24,28},{28,24},{1,5},{5... | collective-permute-start | bytes 417800 | tf_op jit(solution)/shard_map/ppermute | solution.py:20
  20.1 0.5 %shard_map.120 = (bf16[152,256]{1,0:T(8,128)(2,1)S(1)}, bf16[256,128]{1,0:T(8,128)(2,1)S(1)}, bf16[128,128]{1,0:T(8,128)(2,1)S(1)}, bf16[32,128]{1,0:T(8,128)(2,1)S(1)}) custom-call(bf16[128,2048]{1,0:T(8,128)(2,1)S(1)} %get-tuple-element.33.x_all, bf16[2048,256]{1,0:T(8,128)(2,1)S(1)} %get-tuple-element.34.conv_w, ...), custom_call_target="tpu_custom_call" | custom-call | flops 268435456 | tf_op jit(solution)/shard_map/pallas_call | solution.py:279
  20.5 0.6 %collective-permute-start.4 = (bf16[152,256]{1,0:T(8,128)(2,1)S(1)}, bf16[152,256]{1,0:T(8,128)(2,1)S(1)}, u32[]{:S(2)}, u32[]{:S(2)}) collective-permute-start(bf16[152,256]{1,0:T(8,128)(2,1)S(1)} %get-tuple-element.38), channel_id=1, source_target_pairs={{0,4},{4,0},{8,12},{12,8},{16,20},{20,16},{24,28},{28,24},{1,5},{5... | collective-permute-start | bytes 233480 | tf_op jit(solution)/shard_map/ppermute | solution.py:20
  21.1 1.5 %collective-permute-start.9 = (bf16[136,256]{1,0:T(8,128)(2,1)S(1)}, bf16[136,256]{1,0:T(8,128)(2,1)S(1)}, u32[]{:S(2)}, u32[]{:S(2)}) collective-permute-start(bf16[136,256]{1,0:T(8,128)(2,1)S(1)} %collective-permute-done.8.refs_2_), channel_id=1, source_target_pairs={{0,4},{4,0},{8,12},{12,8},{16,20},{20,16},{24,28},{28,24},{1,5},{5... | collective-permute-start | bytes 208904 | tf_op jit(solution)/shard_map/ppermute | solution.py:20
  22.6 0.6 %collective-permute-start.3 = (bf16[32,128]{1,0:T(8,128)(2,1)S(1)}, bf16[32,128]{1,0:T(8,128)(2,1)S(1)}, u32[]{:S(2)}, u32[]{:S(2)}) collective-permute-start(bf16[32,128]{1,0:T(8,128)(2,1)S(1)} %get-tuple-element.37), channel_id=1, source_target_pairs={{4,8},{8,4},{12,16},{16,12},{20,24},{24,20},{5,9},{9,5},{13,17},{1... | collective-permute-start | bytes 24584 | tf_op jit(solution)/shard_map/ppermute | solution.py:377
  23.3 2.8 %collective-permute-done.4.odd.refs_3_ = bf16[152,256]{1,0:T(8,128)(2,1)S(1)} collective-permute-done((bf16[152,256]{1,0:T(8,128)(2,1)S(1)}, bf16[152,256]{1,0:T(8,128)(2,1)S(1)}, u32[]{:S(2)}, u32[]{:S(2)}) %collective-permute-start.4) | collective-permute-done | bytes 77856 | tf_op jit(solution)/shard_map/ppermute | solution.py:20
  26.1 0.4 shard_map.121
  26.5 1.6 %collective-permute-start.6 = (f32[8,128]{1,0:T(8,128)S(1)}, f32[8,128]{1,0:T(8,128)S(1)}, u32[]{:S(2)}, u32[]{:S(2)}) collective-permute-start(f32[8,128]{1,0:T(8,128)S(1)} %get-tuple-element.42.own), channel_id=1, source_target_pairs={{0,2},{1,3},{2,0},{3,1},{4,6},{5,7},{6,4},{7,5},{8,10},{9,11},{10,... | collective-permute-start | bytes 12296 | tf_op jit(solution)/shard_map/ppermute | solution.py:20
  28.3 0.8 %shard_map.123.refs_4_ = f32[16,256,128]{2,1,0:T(8,128)S(1)} custom-call(bf16[256,128]{1,0:T(8,128)(2,1)S(1)} %get-tuple-element.45.refs_0_.q_ref, bf16[136,256]{1,0:T(8,128)(2,1)S(1)} %get-tuple-element.36.pay.refs_1_, bf16[136,256]{1,0:T(8,128)(2,1)S(1)} %collective-permute-done.8.refs_2_, bf16[152,256]{1,0:T(8,128)(2,1)S(1)} %collective-permute-done.4.odd.refs_3_, ...), custom_call_target="tpu_custom_call" | custom-call | flops 335544320 | tf_op jit(solution)/shard_map/pallas_call | solution.py:279
  29.1 1.1 %shard_map.124 = (f32[128,2048]{1,0:T(8,128)S(1)}, f32[16,256,128]{2,1,0:T(8,128)S(1)}) custom-call(bf16[256,128]{1,0:T(8,128)(2,1)S(1)} %get-tuple-element.45.refs_0_.q_ref, bf16[136,256]{1,0:T(8,128)(2,1)S(1)} %collective-permute-done.9.refs_0_, bf16[2,136,256]{2,1,0:T(8,128)(2,1)S(1)} %collective-permute-done.12.refs_1_, ...), custom_call_target="tpu_custom_call", output_to_operand_aliasing={{1}: (5, {})} | custom-call | flops 201326592 | tf_op jit(solution)/shard_map/pallas_call | solution.py:279
  30.3 0.4 %shard_map.125 = (f32[32,2048]{1,0:T(8,128)S(1)}, f32[32,2048]{1,0:T(8,128)S(1)}, bf16[64,2048]{1,0:T(8,128)(2,1)S(1)}) custom-call(f32[128,128]{1,0:T(8,128)S(1)} %get-tuple-element.41.field, f32[8,128]{1,0:T(8,128)S(1)} %get-tuple-element.42.own, f32[8,128]{1,0:T(8,128)S(1)} %collective-permute-done.5.core, f32[8,128]{1,0:T(8,128)S(1)} %collective-permute-done.6.chip, ...), custom_call_target="tpu_custom_call" | custom-call | flops 67108864 | tf_op jit(solution)/shard_map/pallas_call | solution.py:279
  31.0 1.3 %collective-permute-done.13 = bf16[64,2048]{1,0:T(8,128)(2,1)S(1)} collective-permute-done((bf16[64,2048]{1,0:T(8,128)(2,1)S(1)}, bf16[64,2048]{1,0:T(8,128)(2,1)S(1)}, u32[]{:S(2)}, u32[]{:S(2)}) %collective-permute-start.13) | collective-permute-done | bytes 262176 | tf_op jit(solution)/shard_map/ppermute | solution.py:20
  32.4 1.6 %collective-permute-start.14 = (bf16[32,2048]{1,0:T(8,128)(2,1)S(1)}, bf16[32,2048]{1,0:T(8,128)(2,1)S(1)}, u32[]{:S(2)}, u32[]{:S(2)}) collective-permute-start(bf16[32,2048]{1,0:T(8,128)(2,1)S(1)} %fusion), channel_id=1, source_target_pairs={{0,2},{1,3},{2,0},{3,1},{4,6},{5,7},{6,4},{7,5},{8,10},{9,11},{10,... | collective-permute-start | bytes 393224 | tf_op jit(solution)/shard_map/ppermute | solution.py:20
  34.0 4.1 %collective-permute-done.14 = bf16[32,2048]{1,0:T(8,128)(2,1)S(1)} collective-permute-done((bf16[32,2048]{1,0:T(8,128)(2,1)S(1)}, bf16[32,2048]{1,0:T(8,128)(2,1)S(1)}, u32[]{:S(2)}, u32[]{:S(2)}) %collective-permute-start.14) | collective-permute-done | bytes 131104 | tf_op jit(solution)/shard_map/ppermute | solution.py:20
  38.1 0.7 %fusion.2 = bf16[32,2048]{1,0:T(8,128)(2,1)} fusion(f32[32,2048]{1,0:T(8,128)S(1)} %get-tuple-element.48, f32[64,2048]{1,0:T(8,128)S(1)} %convert_element_type.12, bf16[32,2048]{1,0:T(8,128)(2,1)S(1)} %collective-permute-done.14), kind=kLoop, calls=%fused_computation.4 | loop fusion | flops 262144 | bytes 786432 | tf_op jit(solution)/shard_map/convert_element_type | solution.py:435
  (17 shorter events, 0.7 us)
Async XLA Ops:
  0.0 6.7 %collective-permute-start = (bf16[32,2048]{1,0:T(8,128)(2,1)}, bf16[32,2048]{1,0:T(8,128)(2,1)S(1)}, u32[]{:S(2)}, u32[]{:S(2)}) collective-permute-start(bf16[32,2048]{1,0:T(8,128)(2,1)} %refs_0_.1), channel_id=1, source_target_pairs={{0,2},{1,3},{2,0},{3,1},{4,6},{5,7},{6,4},{7,5},{8,10},{9,11},{10,... | collective-permute-start | bytes 393224 | tf_op jit(solution)/shard_map/ppermute | solution.py:20
  3.0 3.7 %collective-permute-start.1 = (bf16[32,2048]{1,0:T(8,128)(2,1)}, bf16[32,2048]{1,0:T(8,128)(2,1)S(1)}, u32[]{:S(2)}, u32[]{:S(2)}) collective-permute-start(bf16[32,2048]{1,0:T(8,128)(2,1)} %refs_0_.1), channel_id=1, source_target_pairs={{0,1},{1,0},{2,3},{3,2},{4,5},{5,4},{6,7},{7,6},{8,9},{9,8},{10,11... | collective-permute-start | bytes 393224 | tf_op jit(solution)/shard_map/ppermute | solution.py:20
  6.7 1.3 %collective-permute-start.2 = (bf16[32,2048]{1,0:T(8,128)(2,1)S(1)}, bf16[32,2048]{1,0:T(8,128)(2,1)S(1)}, u32[]{:S(2)}, u32[]{:S(2)}) collective-permute-start(bf16[32,2048]{1,0:T(8,128)(2,1)S(1)} %collective-permute-done.t2), channel_id=1, source_target_pairs={{0,1},{1,0},{2,3},{3,2},{4,5},{5,4},{6,7},{7,6},{8,9},{9,8},{10,11... | collective-permute-start | bytes 393224 | tf_op jit(solution)/shard_map/ppermute | solution.py:20
  8.4 6.7 %collective-permute-start.11 = (bf16[136,256]{1,0:T(8,128)(2,1)S(1)}, bf16[136,256]{1,0:T(8,128)(2,1)S(1)}, u32[]{:S(2)}, u32[]{:S(2)}) collective-permute-start(bf16[136,256]{1,0:T(8,128)(2,1)S(1)} %get-tuple-element.36.pay.refs_1_), channel_id=1, source_target_pairs={{0,24},{4,28},{8,16},{12,20},{16,8},{20,12},{24,0},{28,4},{1,25},{... | collective-permute-start | bytes 208904 | tf_op jit(solution)/shard_map/ppermute | solution.py:20
  12.3 6.2 %collective-permute-start.10 = (bf16[136,256]{1,0:T(8,128)(2,1)S(1)}, bf16[136,256]{1,0:T(8,128)(2,1)S(1)}, u32[]{:S(2)}, u32[]{:S(2)}) collective-permute-start(bf16[136,256]{1,0:T(8,128)(2,1)S(1)} %get-tuple-element.36.pay.refs_1_), channel_id=1, source_target_pairs={{0,16},{4,20},{8,24},{12,28},{16,0},{20,4},{24,8},{28,12},{1,17},{... | collective-permute-start | bytes 208904 | tf_op jit(solution)/shard_map/ppermute | solution.py:20
  12.3 8.8 %collective-permute-start.8 = (bf16[136,256]{1,0:T(8,128)(2,1)S(1)}, bf16[136,256]{1,0:T(8,128)(2,1)S(1)}, u32[]{:S(2)}, u32[]{:S(2)}) collective-permute-start(bf16[136,256]{1,0:T(8,128)(2,1)S(1)} %get-tuple-element.36.pay.refs_1_), channel_id=1, source_target_pairs={{0,8},{4,12},{8,0},{12,4},{16,24},{20,28},{24,16},{28,20},{1,9},{5... | collective-permute-start | bytes 208904 | tf_op jit(solution)/shard_map/ppermute | solution.py:20
  18.5 10.6 %collective-permute-start.12 = (bf16[2,136,256]{2,1,0:T(8,128)(2,1)S(1)}, bf16[2,136,256]{2,1,0:T(8,128)(2,1)S(1)}, u32[]{:S(2)}, u32[]{:S(2)}) collective-permute-start(bf16[2,136,256]{2,1,0:T(8,128)(2,1)S(1)} %shard_map.122.refs_4_), channel_id=1, source_target_pairs={{0,4},{4,0},{8,12},{12,8},{16,20},{20,16},{24,28},{28,24},{1,5},{5... | collective-permute-start | bytes 417800 | tf_op jit(solution)/shard_map/ppermute | solution.py:20
  20.5 5.5 %collective-permute-start.4 = (bf16[152,256]{1,0:T(8,128)(2,1)S(1)}, bf16[152,256]{1,0:T(8,128)(2,1)S(1)}, u32[]{:S(2)}, u32[]{:S(2)}) collective-permute-start(bf16[152,256]{1,0:T(8,128)(2,1)S(1)} %get-tuple-element.38), channel_id=1, source_target_pairs={{0,4},{4,0},{8,12},{12,8},{16,20},{20,16},{24,28},{28,24},{1,5},{5... | collective-permute-start | bytes 233480 | tf_op jit(solution)/shard_map/ppermute | solution.py:20
  21.1 8.0 %collective-permute-start.9 = (bf16[136,256]{1,0:T(8,128)(2,1)S(1)}, bf16[136,256]{1,0:T(8,128)(2,1)S(1)}, u32[]{:S(2)}, u32[]{:S(2)}) collective-permute-start(bf16[136,256]{1,0:T(8,128)(2,1)S(1)} %collective-permute-done.8.refs_2_), channel_id=1, source_target_pairs={{0,4},{4,0},{8,12},{12,8},{16,20},{20,16},{24,28},{28,24},{1,5},{5... | collective-permute-start | bytes 208904 | tf_op jit(solution)/shard_map/ppermute | solution.py:20
  22.6 0.7 %collective-permute-start.3 = (bf16[32,128]{1,0:T(8,128)(2,1)S(1)}, bf16[32,128]{1,0:T(8,128)(2,1)S(1)}, u32[]{:S(2)}, u32[]{:S(2)}) collective-permute-start(bf16[32,128]{1,0:T(8,128)(2,1)S(1)} %get-tuple-element.37), channel_id=1, source_target_pairs={{4,8},{8,4},{12,16},{16,12},{20,24},{24,20},{5,9},{9,5},{13,17},{1... | collective-permute-start | bytes 24584 | tf_op jit(solution)/shard_map/ppermute | solution.py:377
  26.4 3.8 %collective-permute-start.7 = (f32[8,128]{1,0:T(8,128)S(1)}, f32[8,128]{1,0:T(8,128)S(1)}, u32[]{:S(2)}, u32[]{:S(2)}) collective-permute-start(f32[8,128]{1,0:T(8,128)S(1)} %get-tuple-element.42.own), channel_id=1, source_target_pairs={{0,3},{1,2},{2,1},{3,0},{4,7},{5,6},{6,5},{7,4},{8,11},{9,10},{10,... | collective-permute-start | bytes 12296 | tf_op jit(solution)/shard_map/ppermute | solution.py:20
  26.5 3.8 %collective-permute-start.6 = (f32[8,128]{1,0:T(8,128)S(1)}, f32[8,128]{1,0:T(8,128)S(1)}, u32[]{:S(2)}, u32[]{:S(2)}) collective-permute-start(f32[8,128]{1,0:T(8,128)S(1)} %get-tuple-element.42.own), channel_id=1, source_target_pairs={{0,2},{1,3},{2,0},{3,1},{4,6},{5,7},{6,4},{7,5},{8,10},{9,11},{10,... | collective-permute-start | bytes 12296 | tf_op jit(solution)/shard_map/ppermute | solution.py:20
  28.1 2.2 %collective-permute-start.5 = (f32[8,128]{1,0:T(8,128)S(1)}, f32[8,128]{1,0:T(8,128)S(1)}, u32[]{:S(2)}, u32[]{:S(2)}) collective-permute-start(f32[8,128]{1,0:T(8,128)S(1)} %get-tuple-element.42.own), channel_id=1, source_target_pairs={{0,1},{1,0},{2,3},{3,2},{4,5},{5,4},{6,7},{7,6},{8,9},{9,8},{10,11... | collective-permute-start | bytes 12296 | tf_op jit(solution)/shard_map/ppermute | solution.py:20
  30.7 1.6 %collective-permute-start.13 = (bf16[64,2048]{1,0:T(8,128)(2,1)S(1)}, bf16[64,2048]{1,0:T(8,128)(2,1)S(1)}, u32[]{:S(2)}, u32[]{:S(2)}) collective-permute-start(bf16[64,2048]{1,0:T(8,128)(2,1)S(1)} %get-tuple-element.49), channel_id=1, source_target_pairs={{0,1},{1,0},{2,3},{3,2},{4,5},{5,4},{6,7},{7,6},{8,9},{9,8},{10,11... | collective-permute-start | bytes 786440 | tf_op jit(solution)/shard_map/ppermute | solution.py:20
  32.4 5.7 %collective-permute-start.14 = (bf16[32,2048]{1,0:T(8,128)(2,1)S(1)}, bf16[32,2048]{1,0:T(8,128)(2,1)S(1)}, u32[]{:S(2)}, u32[]{:S(2)}) collective-permute-start(bf16[32,2048]{1,0:T(8,128)(2,1)S(1)} %fusion), channel_id=1, source_target_pairs={{0,2},{1,3},{2,0},{3,1},{4,6},{5,7},{6,4},{7,5},{8,10},{9,11},{10,... | collective-permute-start | bytes 393224 | tf_op jit(solution)/shard_map/ppermute | solution.py:20

commit v8 on v7

--- a/solution.py
+++ b/solution.py
@@ -185,10 +185,10 @@
         mix[:, h * HEAD_DIM : (h + 1) * HEAD_DIM] = part.astype(bf16)
 
 
-def by_slot(mix, n, members):
+def by_slot(mix, n, members, slots):
     me = lax.axis_index("tp")
     rows = n // members
-    picks = [mix[pl.ds(pl.multiple_of((me ^ k) * rows, rows), rows), :] for k in (0, 2, 1, 3)]
+    picks = [mix[pl.ds(pl.multiple_of((me ^ k) * rows, rows), rows), :] for k in slots]
     return jnp.concatenate(picks, axis=0)
 
 
@@ -214,9 +214,9 @@
     return flat
 
 
-def stick_kernel(q_ref, *refs, slots, blocks, members, n, per):
-    s_gain, out_w, _, stick, sums, mix = refs[-6:]
-    pays = views(refs[:-6])
+def stick_kernel(q_ref, *refs, slots, blocks, n, per):
+    s_gain, _, mix, sums = refs[-4:]
+    pays = views(refs[:-4])
     me = lax.axis_index("sp")
     late = shares(q_ref[...], pays, [False] * len(slots), n, per, tri_of(n))
     for k, (part, total) in zip(slots, late):
@@ -230,11 +230,9 @@
         if j:
             carry = carry + sums[blocks + j]
     normed_heads(att, s_gain, mix, n, per)
-    ch = out_w.shape[0] - per * HEAD_DIM
-    stick[...] = dot(by_slot(mix, n, members), out_w[ch:, :])
-
-
-def stick_loop_kernel(q_ref, pays, s_gain, out_w, stick, mix, *, members, n, per):
+
+
+def stick_loop_kernel(q_ref, pays, s_gain, mix, *, n, per):
     me = lax.axis_index("sp")
     q = q_ref[...]
     tri = tri_of(n)
@@ -247,11 +245,9 @@
     (start,) = shares(q, [pays.at[me]], [True], n, per, tri)
     att, _ = lax.fori_loop(1, me + 1, step, start)
     normed_heads(att, s_gain, mix, n, per)
-    ch = out_w.shape[0] - per * HEAD_DIM
-    stick[...] = dot(by_slot(mix, n, members), out_w[ch:, :])
-
-
-def finish_kernel(field, own, core, chip, both, c_gain, out_w, stick, mine, other, send, mix, *, members):
+
+
+def send_kernel(field, own, core, chip, both, c_gain, out_w, stick, send, mix, *, members):
     n, ch = field.shape
     near = both_stats(own[0:1, :], own[1:2, :], core[0:1, :], core[1:2, :], ch)
     far = both_stats(chip[0:1, :], chip[1:2, :], both[0:1, :], both[1:2, :], ch)
@@ -260,12 +256,17 @@
     mean_c = jnp.transpose(jnp.broadcast_to(mean, (ch, n)))
     rstd_c = jnp.transpose(jnp.broadcast_to(rstd, (ch, n)))
     z = (field[...] - mean_c) * rstd_c * c_gain[...]
-    mix[...] = (z * jax.nn.sigmoid(z)).astype(bf16)
-    out = dot(by_slot(mix, n, members), out_w[0:ch, :]) + stick[...]
+    mix[:, 0:ch] = (z * jax.nn.sigmoid(z)).astype(bf16)
+    mix[:, ch:] = stick[...]
+    send[...] = dot(by_slot(mix, n, members, (1, 3)), out_w[...]).astype(bf16)
+
+
+def keep_kernel(mix, out_w, mine, other, *, members):
+    n = mix.shape[0]
+    out = dot(by_slot(mix, n, members, (0, 2)), out_w[...])
     rows = n // members
     mine[...] = out[0:rows, :]
-    other[...] = out[rows : 2 * rows, :]
-    send[...] = out[2 * rows :, :].astype(bf16)
+    other[...] = out[rows:, :]
 
 
 def call(body, outs, args, scratch=(), flops=0, spaces=None, limit=2**22, aliases={}):
@@ -362,7 +363,6 @@
     )
     sizes = dict(n=n, per=per)
     heads = per * n
-    mixed = [pltpu.VMEM((n, query_cols), bf16)]
     block_flops = 2 * heads * n * HEAD_DIM * 8
     stat = ((8, n), f32)
     if blocks == 8:
@@ -395,40 +395,44 @@
         (z46,) = call(join_kernel, [((2, n + 8, 2 * kv), bf16)], [z4, z6])
         x57 = swap(z46, "sp", 1)
         (sums,) = call(
-            functools.partial(parts_kernel, slots=(0, 2, 1, 4, 6), blocks=blocks, **sizes),
+            functools.partial(parts_kernel, slots=(0, 2, 1, 3, 4, 6), blocks=blocks, **sizes),
             [((2 * blocks, heads, HEAD_DIM), f32)],
-            [qs, pay, z2, x1, z46],
-            flops=5 * block_flops,
+            [qs, pay, z2, x1, x3, z46],
+            flops=6 * block_flops,
         )
         body = functools.partial(
-            stick_kernel, slots=(3, 5, 7), blocks=blocks, members=members, **sizes
+            stick_kernel, slots=(5, 7), blocks=blocks, **sizes
         )
-        stick_args = [qs, x3, x57, s_gain, out_w, sums]
+        stick_args = [qs, x57, s_gain, sums]
         stick_outs = [((2 * blocks, heads, HEAD_DIM), f32)]
-        aliases = {5: 1}
+        aliases = {3: 1}
         spaces = None
     else:
-        body = functools.partial(stick_loop_kernel, members=members, **sizes)
-        stick_args = [qs, pays, s_gain, out_w]
+        body = functools.partial(stick_loop_kernel, **sizes)
+        stick_args = [qs, pays, s_gain]
         stick_outs = []
         aliases = {}
-        spaces = [True, False, True, True]
+        spaces = [True, False, True]
     stick, *_ = call(
         body,
-        [((n, width), f32)] + stick_outs,
+        [((n, query_cols), bf16)] + stick_outs,
         stick_args,
-        scratch=mixed,
-        flops=block_flops + 2 * n * width * query_cols,
+        flops=block_flops,
         spaces=spaces,
         aliases=aliases,
         limit=2**22 if blocks == 8 else 2**25,
     )
-    mine, other, send = call(
-        functools.partial(finish_kernel, members=members),
-        [((rows, width), f32), ((rows, width), f32), ((2 * rows, width), bf16)],
+    send, mix = call(
+        functools.partial(send_kernel, members=members),
+        [((2 * rows, width), bf16), ((n, ch + query_cols), bf16)],
         [field, stats, peer, chip, both, c_gain, out_w, stick],
-        scratch=[pltpu.VMEM((n, ch), bf16)],
-        flops=2 * n * width * ch,
+        flops=n * width * (ch + query_cols),
+    )
+    mine, other = call(
+        functools.partial(keep_kernel, members=members),
+        [((rows, width), f32), ((rows, width), f32)],
+        [mix, out_w],
+        flops=n * width * (ch + query_cols),
     )
     got = swap(send, "tp", 1).astype(f32)
     chip = swap((other + got[rows:]).astype(bf16), "tp", 2)

time: 39.5 us -> 39.6 us (level)
    pallas_call x7 -> x8, Pallas kernels: 3.51 us -> 3.72 us  [call(): pl.pallas_call(body, out_shape=[pltpu.VMEM(shape, dtype) for shape, dtype...]
  transfers between devices with their start and end apart: 15 -> 15, of which waited for: 7 -> 8; matrix products, arithmetic and copies ran while one was open for 0% -> 0% of each run, Pallas kernels for 14% -> 14%
where the time goes in v8:
time: 39.6 us; the launch traced here: 38.9 us
  waiting for transfers between devices  16.1 us (41%)
  starting transfers between devices  15.8 us (40%)
  Pallas kernels  6.24 us (16%)
  other arithmetic  0.76 us (2%)
    ppermute x14, waiting for transfers between devices, swap(): return lax.ppermute(value, axis, [(i, i ^ by) for i in range(count)])  16.1 us
    ppermute x14, starting transfers between devices, swap(): return lax.ppermute(value, axis, [(i, i ^ by) for i in range(count)])  15.1 us
    pallas_call x8, Pallas kernels, call(): pl.pallas_call(body, out_shape=[pltpu.VMEM(shape, dtype) for shape, dtype...  3.72 us
    pallas_call x1, Pallas kernels, shards(): pl.pallas_call(load_kernel, out_shape=[pltpu.VMEM(shape, dtype) for shape...  2.52 us
  transfers between devices with their start and end apart: 15, of which 8 were waited for; matrix products, arithmetic and copies ran while one was open for 0% of the time, Pallas kernels for 14%

profile of v8, /device:TPU:0, one launch (start us, length us, event | category | flops | bytes accessed | tf_op | source)
XLA Modules:
  0.0 38.9 jit_solution(17890350158257185329)
XLA Ops:
  0.0 3.0 %collective-permute-start = (bf16[32,2048]{1,0:T(8,128)(2,1)}, bf16[32,2048]{1,0:T(8,128)(2,1)S(1)}, u32[]{:S(2)}, u32[]{:S(2)}) collective-permute-start(bf16[32,2048]{1,0:T(8,128)(2,1)} %refs_0_.1), channel_id=1, source_target_pairs={{0,2},{1,3},{2,0},{3,1},{4,6},{5,7},{6,4},{7,5},{8,10},{9,11},{10,... | collective-permute-start | bytes 393224 | tf_op jit(solution)/shard_map/ppermute | solution.py:20
  3.0 2.5 %shard_map.118 = (bf16[32,2048]{1,0:T(8,128)(2,1)S(1)}, bf16[2048,256]{1,0:T(8,128)(2,1)S(1)}, bf16[2048,256]{1,0:T(8,128)(2,1)S(1)}, bf16[2048,256]{1,0:T(8,128...) custom-call(bf16[32,2048]{1,0:T(8,128)(2,1)} %refs_0_.1, ...), custom_call_target="tpu_custom_call" | custom-call | flops 1000000000 | bytes 5000000 | tf_op jit(solution)/shard_map/pallas_call | solution.py:323
  5.5 1.2 %collective-permute-done.t2 = bf16[32,2048]{1,0:T(8,128)(2,1)S(1)} collective-permute-done((bf16[32,2048]{1,0:T(8,128)(2,1)}, bf16[32,2048]{1,0:T(8,128)(2,1)S(1)}, u32[]{:S(2)}, u32[]{:S(2)}) %collective-permute-start) | collective-permute-done | bytes 131104 | tf_op jit(solution)/shard_map/ppermute | solution.py:20
  6.7 1.3 %collective-permute-done.2.t3 = bf16[32,2048]{1,0:T(8,128)(2,1)S(1)} collective-permute-done((bf16[32,2048]{1,0:T(8,128)(2,1)S(1)}, bf16[32,2048]{1,0:T(8,128)(2,1)S(1)}, u32[]{:S(2)}, u32[]{:S(2)}) %collective-permute-start.2) | collective-permute-done | bytes 131104 | tf_op jit(solution)/shard_map/ppermute | solution.py:20
  8.4 3.9 %collective-permute-start.9 = (bf16[136,256]{1,0:T(8,128)(2,1)S(1)}, bf16[136,256]{1,0:T(8,128)(2,1)S(1)}, u32[]{:S(2)}, u32[]{:S(2)}) collective-permute-start(bf16[136,256]{1,0:T(8,128)(2,1)S(1)} %get-tuple-element.37.pay.refs_1_), channel_id=1, source_target_pairs={{0,24},{4,28},{8,16},{12,20},{16,8},{20,12},{24,0},{28,4},{1,25},{... | collective-permute-start | bytes 208904 | tf_op jit(solution)/shard_map/ppermute | solution.py:20
  12.3 0.6 %collective-permute-start.11 = (bf16[136,256]{1,0:T(8,128)(2,1)S(1)}, bf16[136,256]{1,0:T(8,128)(2,1)S(1)}, u32[]{:S(2)}, u32[]{:S(2)}) collective-permute-start(bf16[136,256]{1,0:T(8,128)(2,1)S(1)} %get-tuple-element.37.pay.refs_1_), channel_id=1, source_target_pairs={{0,8},{4,12},{8,0},{12,4},{16,24},{20,28},{24,16},{28,20},{1,9},{5... | collective-permute-start | bytes 208904 | tf_op jit(solution)/shard_map/ppermute | solution.py:20
  12.9 2.1 %collective-permute-done.9.zb = bf16[136,256]{1,0:T(8,128)(2,1)S(1)} collective-permute-done((bf16[136,256]{1,0:T(8,128)(2,1)S(1)}, bf16[136,256]{1,0:T(8,128)(2,1)S(1)}, u32[]{:S(2)}, u32[]{:S(2)}) %collective-permute-start.9) | collective-permute-done | bytes 69664 | tf_op jit(solution)/shard_map/ppermute | solution.py:20
  15.1 3.4 %collective-permute-done.8.za = bf16[136,256]{1,0:T(8,128)(2,1)S(1)} collective-permute-done((bf16[136,256]{1,0:T(8,128)(2,1)S(1)}, bf16[136,256]{1,0:T(8,128)(2,1)S(1)}, u32[]{:S(2)}, u32[]{:S(2)}) %collective-permute-start.8) | collective-permute-done | bytes 69664 | tf_op jit(solution)/shard_map/ppermute | solution.py:20
  18.5 1.6 %collective-permute-start.10 = (bf16[2,136,256]{2,1,0:T(8,128)(2,1)S(1)}, bf16[2,136,256]{2,1,0:T(8,128)(2,1)S(1)}, u32[]{:S(2)}, u32[]{:S(2)}) collective-permute-start(bf16[2,136,256]{2,1,0:T(8,128)(2,1)S(1)} %shard_map.122.refs_5_), channel_id=1, source_target_pairs={{0,4},{4,0},{8,12},{12,8},{16,20},{20,16},{24,28},{28,24},{1,5},{5... | collective-permute-start | bytes 417800 | tf_op jit(solution)/shard_map/ppermute | solution.py:20
  20.1 0.5 %shard_map.120 = (bf16[152,256]{1,0:T(8,128)(2,1)S(1)}, bf16[256,128]{1,0:T(8,128)(2,1)S(1)}, bf16[128,128]{1,0:T(8,128)(2,1)S(1)}, bf16[32,128]{1,0:T(8,128)(2,1)S(1)}) custom-call(bf16[128,2048]{1,0:T(8,128)(2,1)S(1)} %get-tuple-element.34.x_all, bf16[2048,256]{1,0:T(8,128)(2,1)S(1)} %get-tuple-element.35.conv_w, ...), custom_call_target="tpu_custom_call" | custom-call | flops 268435456 | tf_op jit(solution)/shard_map/pallas_call | solution.py:280
  20.5 0.6 %collective-permute-start.4 = (bf16[152,256]{1,0:T(8,128)(2,1)S(1)}, bf16[152,256]{1,0:T(8,128)(2,1)S(1)}, u32[]{:S(2)}, u32[]{:S(2)}) collective-permute-start(bf16[152,256]{1,0:T(8,128)(2,1)S(1)} %get-tuple-element.39), channel_id=1, source_target_pairs={{0,4},{4,0},{8,12},{12,8},{16,20},{20,16},{24,28},{28,24},{1,5},{5... | collective-permute-start | bytes 233480 | tf_op jit(solution)/shard_map/ppermute | solution.py:20
  21.1 1.5 %collective-permute-start.12 = (bf16[136,256]{1,0:T(8,128)(2,1)S(1)}, bf16[136,256]{1,0:T(8,128)(2,1)S(1)}, u32[]{:S(2)}, u32[]{:S(2)}) collective-permute-start(bf16[136,256]{1,0:T(8,128)(2,1)S(1)} %collective-permute-done.11.refs_2_), channel_id=1, source_target_pairs={{0,4},{4,0},{8,12},{12,8},{16,20},{20,16},{24,28},{28,24},{1,5},{5... | collective-permute-start | bytes 208904 | tf_op jit(solution)/shard_map/ppermute | solution.py:20
  22.6 0.6 %collective-permute-start.3 = (bf16[32,128]{1,0:T(8,128)(2,1)S(1)}, bf16[32,128]{1,0:T(8,128)(2,1)S(1)}, u32[]{:S(2)}, u32[]{:S(2)}) collective-permute-start(bf16[32,128]{1,0:T(8,128)(2,1)S(1)} %get-tuple-element.38), channel_id=1, source_target_pairs={{4,8},{8,4},{12,16},{16,12},{20,24},{24,20},{5,9},{9,5},{13,17},{1... | collective-permute-start | bytes 24584 | tf_op jit(solution)/shard_map/ppermute | solution.py:377
  23.3 2.8 %collective-permute-done.4.odd.refs_3_ = bf16[152,256]{1,0:T(8,128)(2,1)S(1)} collective-permute-done((bf16[152,256]{1,0:T(8,128)(2,1)S(1)}, bf16[152,256]{1,0:T(8,128)(2,1)S(1)}, u32[]{:S(2)}, u32[]{:S(2)}) %collective-permute-start.4) | collective-permute-done | bytes 77856 | tf_op jit(solution)/shard_map/ppermute | solution.py:20
  26.5 1.6 %collective-permute-start.6 = (f32[8,128]{1,0:T(8,128)S(1)}, f32[8,128]{1,0:T(8,128)S(1)}, u32[]{:S(2)}, u32[]{:S(2)}) collective-permute-start(f32[8,128]{1,0:T(8,128)S(1)} %get-tuple-element.43.own), channel_id=1, source_target_pairs={{0,2},{1,3},{2,0},{3,1},{4,6},{5,7},{6,4},{7,5},{8,10},{9,11},{10,... | collective-permute-start | bytes 12296 | tf_op jit(solution)/shard_map/ppermute | solution.py:20
  28.3 0.8 %shard_map.123.refs_2_ = f32[16,256,128]{2,1,0:T(8,128)S(1)} custom-call(bf16[256,128]{1,0:T(8,128)(2,1)S(1)} %get-tuple-element.46.refs_0_.q_ref, bf16[136,256]{1,0:T(8,128)(2,1)S(1)} %get-tuple-element.37.pay.refs_1_, bf16[136,256]{1,0:T(8,128)(2,1)S(1)} %collective-permute-done.11.refs_2_, bf16[152,256]{1,0:T(8,128)(2,1)S(1)} %collective-permute-done.4.odd.refs_3_, ...), custom_call_target="tpu_custom_call" | custom-call | flops 402653184 | tf_op jit(solution)/shard_map/pallas_call | solution.py:280
  29.2 0.8 %shard_map.124 = (bf16[128,256]{1,0:T(8,128)(2,1)S(1)}, f32[16,256,128]{2,1,0:T(8,128)S(1)}) custom-call(bf16[256,128]{1,0:T(8,128)(2,1)S(1)} %get-tuple-element.46.refs_0_.q_ref, bf16[2,136,256]{2,1,0:T(8,128)(2,1)S(1)} %collective-permute-done.10.refs_0_, f32[2,128]{1,0:T(2,128)S(1)} %get-tuple-element.47.refs_1_, ...), custom_call_target="tpu_custom_call", output_to_operand_aliasing={{1}: (3, {})} | custom-call | flops 67108864 | tf_op jit(solution)/shard_map/pallas_call | solution.py:280
  30.2 0.5 %shard_map.125 = (bf16[64,2048]{1,0:T(8,128)(2,1)S(1)}, bf16[128,384]{1,0:T(8,128)(2,1)S(1)}) custom-call(f32[128,128]{1,0:T(8,128)S(1)} %get-tuple-element.42.field, f32[8,128]{1,0:T(8,128)S(1)} %get-tuple-element.43.own, f32[8,128]{1,0:T(8,128)S(1)} %collective-permute-done.5.core, f32[8,128]{1,0:T(8,128)S(1)} %collective-permute-done.6.chip, ...), custom_call_target="tpu_custom_call" | custom-call | flops 100663296 | tf_op jit(solution)/shard_map/pallas_call | solution.py:280
  30.7 0.5 %collective-permute-start.13 = (bf16[64,2048]{1,0:T(8,128)(2,1)S(1)}, bf16[64,2048]{1,0:T(8,128)(2,1)S(1)}, u32[]{:S(2)}, u32[]{:S(2)}) collective-permute-start(bf16[64,2048]{1,0:T(8,128)(2,1)S(1)} %get-tuple-element.51), channel_id=1, source_target_pairs={{0,1},{1,0},{2,3},{3,2},{4,5},{5,4},{6,7},{7,6},{8,9},{9,8},{10,11... | collective-permute-start | bytes 786440 | tf_op jit(solution)/shard_map/ppermute | solution.py:20
  31.2 0.4 %shard_map.126 = (f32[32,2048]{1,0:T(8,128)S(1)}, f32[32,2048]{1,0:T(8,128)S(1)}) custom-call(bf16[128,384]{1,0:T(8,128)(2,1)S(1)} %get-tuple-element.49.mix, bf16[384,2048]{1,0:T(8,128)(2,1)S(1)} %get-tuple-element.45.out_w), custom_call_target="tpu_custom_call" | custom-call | flops 100663296 | tf_op jit(solution)/shard_map/pallas_call | solution.py:280
  31.6 0.8 %collective-permute-done.13 = bf16[64,2048]{1,0:T(8,128)(2,1)S(1)} collective-permute-done((bf16[64,2048]{1,0:T(8,128)(2,1)S(1)}, bf16[64,2048]{1,0:T(8,128)(2,1)S(1)}, u32[]{:S(2)}, u32[]{:S(2)}) %collective-permute-start.13) | collective-permute-done | bytes 262176 | tf_op jit(solution)/shard_map/ppermute | solution.py:20
  32.4 1.6 %collective-permute-start.14 = (bf16[32,2048]{1,0:T(8,128)(2,1)S(1)}, bf16[32,2048]{1,0:T(8,128)(2,1)S(1)}, u32[]{:S(2)}, u32[]{:S(2)}) collective-permute-start(bf16[32,2048]{1,0:T(8,128)(2,1)S(1)} %fusion), channel_id=1, source_target_pairs={{0,2},{1,3},{2,0},{3,1},{4,6},{5,7},{6,4},{7,5},{8,10},{9,11},{10,... | collective-permute-start | bytes 393224 | tf_op jit(solution)/shard_map/ppermute | solution.py:20
  33.9 4.3 %collective-permute-done.14 = bf16[32,2048]{1,0:T(8,128)(2,1)S(1)} collective-permute-done((bf16[32,2048]{1,0:T(8,128)(2,1)S(1)}, bf16[32,2048]{1,0:T(8,128)(2,1)S(1)}, u32[]{:S(2)}, u32[]{:S(2)}) %collective-permute-start.14) | collective-permute-done | bytes 131104 | tf_op jit(solution)/shard_map/ppermute | solution.py:20
  38.2 0.7 %fusion.2 = bf16[32,2048]{1,0:T(8,128)(2,1)} fusion(f32[32,2048]{1,0:T(8,128)S(1)} %get-tuple-element.50, f32[64,2048]{1,0:T(8,128)S(1)} %convert_element_type.12, bf16[32,2048]{1,0:T(8,128)(2,1)S(1)} %collective-permute-done.14), kind=kLoop, calls=%fused_computation.4 | loop fusion | flops 262144 | bytes 786432 | tf_op jit(solution)/shard_map/convert_element_type | solution.py:439
  (18 shorter events, 1.3 us)
Async XLA Ops:
  0.0 6.7 %collective-permute-start = (bf16[32,2048]{1,0:T(8,128)(2,1)}, bf16[32,2048]{1,0:T(8,128)(2,1)S(1)}, u32[]{:S(2)}, u32[]{:S(2)}) collective-permute-start(bf16[32,2048]{1,0:T(8,128)(2,1)} %refs_0_.1), channel_id=1, source_target_pairs={{0,2},{1,3},{2,0},{3,1},{4,6},{5,7},{6,4},{7,5},{8,10},{9,11},{10,... | collective-permute-start | bytes 393224 | tf_op jit(solution)/shard_map/ppermute | solution.py:20
  3.0 3.7 %collective-permute-start.1 = (bf16[32,2048]{1,0:T(8,128)(2,1)}, bf16[32,2048]{1,0:T(8,128)(2,1)S(1)}, u32[]{:S(2)}, u32[]{:S(2)}) collective-permute-start(bf16[32,2048]{1,0:T(8,128)(2,1)} %refs_0_.1), channel_id=1, source_target_pairs={{0,1},{1,0},{2,3},{3,2},{4,5},{5,4},{6,7},{7,6},{8,9},{9,8},{10,11... | collective-permute-start | bytes 393224 | tf_op jit(solution)/shard_map/ppermute | solution.py:20
  6.7 1.3 %collective-permute-start.2 = (bf16[32,2048]{1,0:T(8,128)(2,1)S(1)}, bf16[32,2048]{1,0:T(8,128)(2,1)S(1)}, u32[]{:S(2)}, u32[]{:S(2)}) collective-permute-start(bf16[32,2048]{1,0:T(8,128)(2,1)S(1)} %collective-permute-done.t2), channel_id=1, source_target_pairs={{0,1},{1,0},{2,3},{3,2},{4,5},{5,4},{6,7},{7,6},{8,9},{9,8},{10,11... | collective-permute-start | bytes 393224 | tf_op jit(solution)/shard_map/ppermute | solution.py:20
  8.4 6.7 %collective-permute-start.9 = (bf16[136,256]{1,0:T(8,128)(2,1)S(1)}, bf16[136,256]{1,0:T(8,128)(2,1)S(1)}, u32[]{:S(2)}, u32[]{:S(2)}) collective-permute-start(bf16[136,256]{1,0:T(8,128)(2,1)S(1)} %get-tuple-element.37.pay.refs_1_), channel_id=1, source_target_pairs={{0,24},{4,28},{8,16},{12,20},{16,8},{20,12},{24,0},{28,4},{1,25},{... | collective-permute-start | bytes 208904 | tf_op jit(solution)/shard_map/ppermute | solution.py:20
  12.3 6.2 %collective-permute-start.8 = (bf16[136,256]{1,0:T(8,128)(2,1)S(1)}, bf16[136,256]{1,0:T(8,128)(2,1)S(1)}, u32[]{:S(2)}, u32[]{:S(2)}) collective-permute-start(bf16[136,256]{1,0:T(8,128)(2,1)S(1)} %get-tuple-element.37.pay.refs_1_), channel_id=1, source_target_pairs={{0,16},{4,20},{8,24},{12,28},{16,0},{20,4},{24,8},{28,12},{1,17},{... | collective-permute-start | bytes 208904 | tf_op jit(solution)/shard_map/ppermute | solution.py:20
  12.3 8.8 %collective-permute-start.11 = (bf16[136,256]{1,0:T(8,128)(2,1)S(1)}, bf16[136,256]{1,0:T(8,128)(2,1)S(1)}, u32[]{:S(2)}, u32[]{:S(2)}) collective-permute-start(bf16[136,256]{1,0:T(8,128)(2,1)S(1)} %get-tuple-element.37.pay.refs_1_), channel_id=1, source_target_pairs={{0,8},{4,12},{8,0},{12,4},{16,24},{20,28},{24,16},{28,20},{1,9},{5... | collective-permute-start | bytes 208904 | tf_op jit(solution)/shard_map/ppermute | solution.py:20
  18.5 10.7 %collective-permute-start.10 = (bf16[2,136,256]{2,1,0:T(8,128)(2,1)S(1)}, bf16[2,136,256]{2,1,0:T(8,128)(2,1)S(1)}, u32[]{:S(2)}, u32[]{:S(2)}) collective-permute-start(bf16[2,136,256]{2,1,0:T(8,128)(2,1)S(1)} %shard_map.122.refs_5_), channel_id=1, source_target_pairs={{0,4},{4,0},{8,12},{12,8},{16,20},{20,16},{24,28},{28,24},{1,5},{5... | collective-permute-start | bytes 417800 | tf_op jit(solution)/shard_map/ppermute | solution.py:20
  20.5 5.5 %collective-permute-start.4 = (bf16[152,256]{1,0:T(8,128)(2,1)S(1)}, bf16[152,256]{1,0:T(8,128)(2,1)S(1)}, u32[]{:S(2)}, u32[]{:S(2)}) collective-permute-start(bf16[152,256]{1,0:T(8,128)(2,1)S(1)} %get-tuple-element.39), channel_id=1, source_target_pairs={{0,4},{4,0},{8,12},{12,8},{16,20},{20,16},{24,28},{28,24},{1,5},{5... | collective-permute-start | bytes 233480 | tf_op jit(solution)/shard_map/ppermute | solution.py:20
  21.1 7.2 %collective-permute-start.12 = (bf16[136,256]{1,0:T(8,128)(2,1)S(1)}, bf16[136,256]{1,0:T(8,128)(2,1)S(1)}, u32[]{:S(2)}, u32[]{:S(2)}) collective-permute-start(bf16[136,256]{1,0:T(8,128)(2,1)S(1)} %collective-permute-done.11.refs_2_), channel_id=1, source_target_pairs={{0,4},{4,0},{8,12},{12,8},{16,20},{20,16},{24,28},{28,24},{1,5},{5... | collective-permute-start | bytes 208904 | tf_op jit(solution)/shard_map/ppermute | solution.py:20
  22.6 0.7 %collective-permute-start.3 = (bf16[32,128]{1,0:T(8,128)(2,1)S(1)}, bf16[32,128]{1,0:T(8,128)(2,1)S(1)}, u32[]{:S(2)}, u32[]{:S(2)}) collective-permute-start(bf16[32,128]{1,0:T(8,128)(2,1)S(1)} %get-tuple-element.38), channel_id=1, source_target_pairs={{4,8},{8,4},{12,16},{16,12},{20,24},{24,20},{5,9},{9,5},{13,17},{1... | collective-permute-start | bytes 24584 | tf_op jit(solution)/shard_map/ppermute | solution.py:377
  26.4 3.6 %collective-permute-start.7 = (f32[8,128]{1,0:T(8,128)S(1)}, f32[8,128]{1,0:T(8,128)S(1)}, u32[]{:S(2)}, u32[]{:S(2)}) collective-permute-start(f32[8,128]{1,0:T(8,128)S(1)} %get-tuple-element.43.own), channel_id=1, source_target_pairs={{0,3},{1,2},{2,1},{3,0},{4,7},{5,6},{6,5},{7,4},{8,11},{9,10},{10,... | collective-permute-start | bytes 12296 | tf_op jit(solution)/shard_map/ppermute | solution.py:20
  26.5 3.7 %collective-permute-start.6 = (f32[8,128]{1,0:T(8,128)S(1)}, f32[8,128]{1,0:T(8,128)S(1)}, u32[]{:S(2)}, u32[]{:S(2)}) collective-permute-start(f32[8,128]{1,0:T(8,128)S(1)} %get-tuple-element.43.own), channel_id=1, source_target_pairs={{0,2},{1,3},{2,0},{3,1},{4,6},{5,7},{6,4},{7,5},{8,10},{9,11},{10,... | collective-permute-start | bytes 12296 | tf_op jit(solution)/shard_map/ppermute | solution.py:20
  28.1 2.1 %collective-permute-start.5 = (f32[8,128]{1,0:T(8,128)S(1)}, f32[8,128]{1,0:T(8,128)S(1)}, u32[]{:S(2)}, u32[]{:S(2)}) collective-permute-start(f32[8,128]{1,0:T(8,128)S(1)} %get-tuple-element.43.own), channel_id=1, source_target_pairs={{0,1},{1,0},{2,3},{3,2},{4,5},{5,4},{6,7},{7,6},{8,9},{9,8},{10,11... | collective-permute-start | bytes 12296 | tf_op jit(solution)/shard_map/ppermute | solution.py:20
  30.7 1.6 %collective-permute-start.13 = (bf16[64,2048]{1,0:T(8,128)(2,1)S(1)}, bf16[64,2048]{1,0:T(8,128)(2,1)S(1)}, u32[]{:S(2)}, u32[]{:S(2)}) collective-permute-start(bf16[64,2048]{1,0:T(8,128)(2,1)S(1)} %get-tuple-element.51), channel_id=1, source_target_pairs={{0,1},{1,0},{2,3},{3,2},{4,5},{5,4},{6,7},{7,6},{8,9},{9,8},{10,11... | collective-permute-start | bytes 786440 | tf_op jit(solution)/shard_map/ppermute | solution.py:20
  32.4 5.8 %collective-permute-start.14 = (bf16[32,2048]{1,0:T(8,128)(2,1)S(1)}, bf16[32,2048]{1,0:T(8,128)(2,1)S(1)}, u32[]{:S(2)}, u32[]{:S(2)}) collective-permute-start(bf16[32,2048]{1,0:T(8,128)(2,1)S(1)} %fusion), channel_id=1, source_target_pairs={{0,2},{1,3},{2,0},{3,1},{4,6},{5,7},{6,4},{7,5},{8,10},{9,11},{10,... | collective-permute-start | bytes 393224 | tf_op jit(solution)/shard_map/ppermute | solution.py:20

commit v9 on v8

--- a/solution.py
+++ b/solution.py
@@ -147,7 +147,7 @@
         u = s * scale + jnp.concatenate(shift, axis=0)
         soft = jnp.log2(1.0 + jnp.exp2(-jnp.abs(u)))
         take = jnp.minimum(u, 0.0) - soft
-        keep = take - u
+        keep = jnp.minimum(-u, 0.0) - soft
         if mine:
             keep = jnp.where(before(u.shape, n), keep, 0.0)
         hi = keep.astype(bf16)
@@ -434,9 +434,9 @@
         [mix, out_w],
         flops=n * width * (ch + query_cols),
     )
-    got = swap(send, "tp", 1).astype(f32)
-    chip = swap((other + got[rows:]).astype(bf16), "tp", 2)
-    return (mine + got[:rows] + chip.astype(f32)).astype(bf16)
+    got = swap(send, "tp", 1)
+    chip = swap((other + got[rows:].astype(f32)).astype(bf16), "tp", 2)
+    return (mine + got[:rows].astype(f32) + chip.astype(f32)).astype(bf16)
 
 
 def solution(mesh):

time: 39.6 us -> 39.6 us (level)
  no operation moved by 1% of the time
where the time goes in v9:
time: 39.6 us; the launch traced here: 38.9 us
  waiting for transfers between devices  16.1 us (41%)
  starting transfers between devices  15.8 us (40%)
  Pallas kernels  6.24 us (16%)
  other arithmetic  0.72 us (2%)
    ppermute x14, waiting for transfers between devices, swap(): return lax.ppermute(value, axis, [(i, i ^ by) for i in range(count)])  16.1 us
    ppermute x14, starting transfers between devices, swap(): return lax.ppermute(value, axis, [(i, i ^ by) for i in range(count)])  15.1 us
    pallas_call x8, Pallas kernels, call(): pl.pallas_call(body, out_shape=[pltpu.VMEM(shape, dtype) for shape, dtype...  3.72 us
    pallas_call x1, Pallas kernels, shards(): pl.pallas_call(load_kernel, out_shape=[pltpu.VMEM(shape, dtype) for shape...  2.52 us
  transfers between devices with their start and end apart: 15, of which 8 were waited for; matrix products, arithmetic and copies ran while one was open for 0% of the time, Pallas kernels for 14%

profile of v9, /device:TPU:0, one launch (start us, length us, event | category | flops | bytes accessed | tf_op | source)
XLA Modules:
  0.0 38.9 jit_solution(11907579525667743578)
XLA Ops:
  0.0 3.0 %collective-permute-start = (bf16[32,2048]{1,0:T(8,128)(2,1)}, bf16[32,2048]{1,0:T(8,128)(2,1)S(1)}, u32[]{:S(2)}, u32[]{:S(2)}) collective-permute-start(bf16[32,2048]{1,0:T(8,128)(2,1)} %refs_0_.1), channel_id=1, source_target_pairs={{0,2},{1,3},{2,0},{3,1},{4,6},{5,7},{6,4},{7,5},{8,10},{9,11},{10,... | collective-permute-start | bytes 393224 | tf_op jit(solution)/shard_map/ppermute | solution.py:20
  3.0 2.5 %shard_map.118 = (bf16[32,2048]{1,0:T(8,128)(2,1)S(1)}, bf16[2048,256]{1,0:T(8,128)(2,1)S(1)}, bf16[2048,256]{1,0:T(8,128)(2,1)S(1)}, bf16[2048,256]{1,0:T(8,128...) custom-call(bf16[32,2048]{1,0:T(8,128)(2,1)} %refs_0_.1, ...), custom_call_target="tpu_custom_call" | custom-call | flops 1000000000 | bytes 5000000 | tf_op jit(solution)/shard_map/pallas_call | solution.py:323
  5.5 1.2 %collective-permute-done.t2 = bf16[32,2048]{1,0:T(8,128)(2,1)S(1)} collective-permute-done((bf16[32,2048]{1,0:T(8,128)(2,1)}, bf16[32,2048]{1,0:T(8,128)(2,1)S(1)}, u32[]{:S(2)}, u32[]{:S(2)}) %collective-permute-start) | collective-permute-done | bytes 131104 | tf_op jit(solution)/shard_map/ppermute | solution.py:20
  6.7 1.3 %collective-permute-done.2.t3 = bf16[32,2048]{1,0:T(8,128)(2,1)S(1)} collective-permute-done((bf16[32,2048]{1,0:T(8,128)(2,1)S(1)}, bf16[32,2048]{1,0:T(8,128)(2,1)S(1)}, u32[]{:S(2)}, u32[]{:S(2)}) %collective-permute-start.2) | collective-permute-done | bytes 131104 | tf_op jit(solution)/shard_map/ppermute | solution.py:20
  8.4 3.9 %collective-permute-start.9 = (bf16[136,256]{1,0:T(8,128)(2,1)S(1)}, bf16[136,256]{1,0:T(8,128)(2,1)S(1)}, u32[]{:S(2)}, u32[]{:S(2)}) collective-permute-start(bf16[136,256]{1,0:T(8,128)(2,1)S(1)} %get-tuple-element.37.pay.refs_1_), channel_id=1, source_target_pairs={{0,24},{4,28},{8,16},{12,20},{16,8},{20,12},{24,0},{28,4},{1,25},{... | collective-permute-start | bytes 208904 | tf_op jit(solution)/shard_map/ppermute | solution.py:20
  12.3 0.6 %collective-permute-start.11 = (bf16[136,256]{1,0:T(8,128)(2,1)S(1)}, bf16[136,256]{1,0:T(8,128)(2,1)S(1)}, u32[]{:S(2)}, u32[]{:S(2)}) collective-permute-start(bf16[136,256]{1,0:T(8,128)(2,1)S(1)} %get-tuple-element.37.pay.refs_1_), channel_id=1, source_target_pairs={{0,8},{4,12},{8,0},{12,4},{16,24},{20,28},{24,16},{28,20},{1,9},{5... | collective-permute-start | bytes 208904 | tf_op jit(solution)/shard_map/ppermute | solution.py:20
  12.9 2.1 %collective-permute-done.9.zb = bf16[136,256]{1,0:T(8,128)(2,1)S(1)} collective-permute-done((bf16[136,256]{1,0:T(8,128)(2,1)S(1)}, bf16[136,256]{1,0:T(8,128)(2,1)S(1)}, u32[]{:S(2)}, u32[]{:S(2)}) %collective-permute-start.9) | collective-permute-done | bytes 69664 | tf_op jit(solution)/shard_map/ppermute | solution.py:20
  15.1 3.4 %collective-permute-done.8.za = bf16[136,256]{1,0:T(8,128)(2,1)S(1)} collective-permute-done((bf16[136,256]{1,0:T(8,128)(2,1)S(1)}, bf16[136,256]{1,0:T(8,128)(2,1)S(1)}, u32[]{:S(2)}, u32[]{:S(2)}) %collective-permute-start.8) | collective-permute-done | bytes 69664 | tf_op jit(solution)/shard_map/ppermute | solution.py:20
  18.5 1.6 %collective-permute-start.10 = (bf16[2,136,256]{2,1,0:T(8,128)(2,1)S(1)}, bf16[2,136,256]{2,1,0:T(8,128)(2,1)S(1)}, u32[]{:S(2)}, u32[]{:S(2)}) collective-permute-start(bf16[2,136,256]{2,1,0:T(8,128)(2,1)S(1)} %shard_map.122.refs_5_), channel_id=1, source_target_pairs={{0,4},{4,0},{8,12},{12,8},{16,20},{20,16},{24,28},{28,24},{1,5},{5... | collective-permute-start | bytes 417800 | tf_op jit(solution)/shard_map/ppermute | solution.py:20
  20.1 0.5 %shard_map.120 = (bf16[152,256]{1,0:T(8,128)(2,1)S(1)}, bf16[256,128]{1,0:T(8,128)(2,1)S(1)}, bf16[128,128]{1,0:T(8,128)(2,1)S(1)}, bf16[32,128]{1,0:T(8,128)(2,1)S(1)}) custom-call(bf16[128,2048]{1,0:T(8,128)(2,1)S(1)} %get-tuple-element.34.x_all, bf16[2048,256]{1,0:T(8,128)(2,1)S(1)} %get-tuple-element.35.conv_w, ...), custom_call_target="tpu_custom_call" | custom-call | flops 268435456 | tf_op jit(solution)/shard_map/pallas_call | solution.py:280
  20.5 0.6 %collective-permute-start.4 = (bf16[152,256]{1,0:T(8,128)(2,1)S(1)}, bf16[152,256]{1,0:T(8,128)(2,1)S(1)}, u32[]{:S(2)}, u32[]{:S(2)}) collective-permute-start(bf16[152,256]{1,0:T(8,128)(2,1)S(1)} %get-tuple-element.39), channel_id=1, source_target_pairs={{0,4},{4,0},{8,12},{12,8},{16,20},{20,16},{24,28},{28,24},{1,5},{5... | collective-permute-start | bytes 233480 | tf_op jit(solution)/shard_map/ppermute | solution.py:20
  21.1 1.5 %collective-permute-start.12 = (bf16[136,256]{1,0:T(8,128)(2,1)S(1)}, bf16[136,256]{1,0:T(8,128)(2,1)S(1)}, u32[]{:S(2)}, u32[]{:S(2)}) collective-permute-start(bf16[136,256]{1,0:T(8,128)(2,1)S(1)} %collective-permute-done.11.refs_2_), channel_id=1, source_target_pairs={{0,4},{4,0},{8,12},{12,8},{16,20},{20,16},{24,28},{28,24},{1,5},{5... | collective-permute-start | bytes 208904 | tf_op jit(solution)/shard_map/ppermute | solution.py:20
  22.6 0.6 %collective-permute-start.3 = (bf16[32,128]{1,0:T(8,128)(2,1)S(1)}, bf16[32,128]{1,0:T(8,128)(2,1)S(1)}, u32[]{:S(2)}, u32[]{:S(2)}) collective-permute-start(bf16[32,128]{1,0:T(8,128)(2,1)S(1)} %get-tuple-element.38), channel_id=1, source_target_pairs={{4,8},{8,4},{12,16},{16,12},{20,24},{24,20},{5,9},{9,5},{13,17},{1... | collective-permute-start | bytes 24584 | tf_op jit(solution)/shard_map/ppermute | solution.py:377
  23.3 2.8 %collective-permute-done.4.odd.refs_3_ = bf16[152,256]{1,0:T(8,128)(2,1)S(1)} collective-permute-done((bf16[152,256]{1,0:T(8,128)(2,1)S(1)}, bf16[152,256]{1,0:T(8,128)(2,1)S(1)}, u32[]{:S(2)}, u32[]{:S(2)}) %collective-permute-start.4) | collective-permute-done | bytes 77856 | tf_op jit(solution)/shard_map/ppermute | solution.py:20
  26.5 1.6 %collective-permute-start.6 = (f32[8,128]{1,0:T(8,128)S(1)}, f32[8,128]{1,0:T(8,128)S(1)}, u32[]{:S(2)}, u32[]{:S(2)}) collective-permute-start(f32[8,128]{1,0:T(8,128)S(1)} %get-tuple-element.43.own), channel_id=1, source_target_pairs={{0,2},{1,3},{2,0},{3,1},{4,6},{5,7},{6,4},{7,5},{8,10},{9,11},{10,... | collective-permute-start | bytes 12296 | tf_op jit(solution)/shard_map/ppermute | solution.py:20
  28.3 0.9 %shard_map.123.refs_2_ = f32[16,256,128]{2,1,0:T(8,128)S(1)} custom-call(bf16[256,128]{1,0:T(8,128)(2,1)S(1)} %get-tuple-element.46.refs_0_.q_ref, bf16[136,256]{1,0:T(8,128)(2,1)S(1)} %get-tuple-element.37.pay.refs_1_, bf16[136,256]{1,0:T(8,128)(2,1)S(1)} %collective-permute-done.11.refs_2_, bf16[152,256]{1,0:T(8,128)(2,1)S(1)} %collective-permute-done.4.odd.refs_3_, ...), custom_call_target="tpu_custom_call" | custom-call | flops 402653184 | tf_op jit(solution)/shard_map/pallas_call | solution.py:280
  29.2 0.8 %shard_map.124 = (bf16[128,256]{1,0:T(8,128)(2,1)S(1)}, f32[16,256,128]{2,1,0:T(8,128)S(1)}) custom-call(bf16[256,128]{1,0:T(8,128)(2,1)S(1)} %get-tuple-element.46.refs_0_.q_ref, bf16[2,136,256]{2,1,0:T(8,128)(2,1)S(1)} %collective-permute-done.10.refs_0_, f32[2,128]{1,0:T(2,128)S(1)} %get-tuple-element.47.refs_1_, ...), custom_call_target="tpu_custom_call", output_to_operand_aliasing={{1}: (3, {})} | custom-call | flops 67108864 | tf_op jit(solution)/shard_map/pallas_call | solution.py:280
  30.2 0.5 %shard_map.125 = (bf16[64,2048]{1,0:T(8,128)(2,1)S(1)}, bf16[128,384]{1,0:T(8,128)(2,1)S(1)}) custom-call(f32[128,128]{1,0:T(8,128)S(1)} %get-tuple-element.42.field, f32[8,128]{1,0:T(8,128)S(1)} %get-tuple-element.43.own, f32[8,128]{1,0:T(8,128)S(1)} %collective-permute-done.5.core, f32[8,128]{1,0:T(8,128)S(1)} %collective-permute-done.6.chip, ...), custom_call_target="tpu_custom_call" | custom-call | flops 100663296 | tf_op jit(solution)/shard_map/pallas_call | solution.py:280
  30.7 0.5 %collective-permute-start.13 = (bf16[64,2048]{1,0:T(8,128)(2,1)S(1)}, bf16[64,2048]{1,0:T(8,128)(2,1)S(1)}, u32[]{:S(2)}, u32[]{:S(2)}) collective-permute-start(bf16[64,2048]{1,0:T(8,128)(2,1)S(1)} %get-tuple-element.51), channel_id=1, source_target_pairs={{0,1},{1,0},{2,3},{3,2},{4,5},{5,4},{6,7},{7,6},{8,9},{9,8},{10,11... | collective-permute-start | bytes 786440 | tf_op jit(solution)/shard_map/ppermute | solution.py:20
  31.2 0.4 %shard_map.126 = (f32[32,2048]{1,0:T(8,128)S(1)}, f32[32,2048]{1,0:T(8,128)S(1)}) custom-call(bf16[128,384]{1,0:T(8,128)(2,1)S(1)} %get-tuple-element.49.mix, bf16[384,2048]{1,0:T(8,128)(2,1)S(1)} %get-tuple-element.45.out_w), custom_call_target="tpu_custom_call" | custom-call | flops 100663296 | tf_op jit(solution)/shard_map/pallas_call | solution.py:280
  31.6 0.8 %collective-permute-done.13 = bf16[64,2048]{1,0:T(8,128)(2,1)S(1)} collective-permute-done((bf16[64,2048]{1,0:T(8,128)(2,1)S(1)}, bf16[64,2048]{1,0:T(8,128)(2,1)S(1)}, u32[]{:S(2)}, u32[]{:S(2)}) %collective-permute-start.13) | collective-permute-done | bytes 262176 | tf_op jit(solution)/shard_map/ppermute | solution.py:20
  32.3 1.6 %collective-permute-start.14 = (bf16[32,2048]{1,0:T(8,128)(2,1)S(1)}, bf16[32,2048]{1,0:T(8,128)(2,1)S(1)}, u32[]{:S(2)}, u32[]{:S(2)}) collective-permute-start(bf16[32,2048]{1,0:T(8,128)(2,1)S(1)} %add_convert_fusion.1), channel_id=1, source_target_pairs={{0,2},{1,3},{2,0},{3,1},{4,6},{5,7},{6,4},{7,5},{8,10},{9,11},{10,... | collective-permute-start | bytes 393224 | tf_op jit(solution)/shard_map/ppermute | solution.py:20
  33.9 4.3 %collective-permute-done.14 = bf16[32,2048]{1,0:T(8,128)(2,1)S(1)} collective-permute-done((bf16[32,2048]{1,0:T(8,128)(2,1)S(1)}, bf16[32,2048]{1,0:T(8,128)(2,1)S(1)}, u32[]{:S(2)}, u32[]{:S(2)}) %collective-permute-start.14) | collective-permute-done | bytes 131104 | tf_op jit(solution)/shard_map/ppermute | solution.py:20
  38.2 0.7 %add_convert_fusion = bf16[32,2048]{1,0:T(8,128)(2,1)} fusion(bf16[32,2048]{1,0:T(8,128)(2,1)S(1)} %collective-permute-done.14, f32[32,2048]{1,0:T(8,128)S(1)} %get-tuple-element.50, bf16[64,2048]{1,0:T(8,128)(2,1)S(1)} %collective-permute-done.13), kind=kLoop, calls=%fused_computation | loop fusion | flops 327680 | bytes 655360 | tf_op jit(solution)/shard_map/convert_element_type | solution.py:439
  (17 shorter events, 1.2 us)
Async XLA Ops:
  0.0 6.7 %collective-permute-start = (bf16[32,2048]{1,0:T(8,128)(2,1)}, bf16[32,2048]{1,0:T(8,128)(2,1)S(1)}, u32[]{:S(2)}, u32[]{:S(2)}) collective-permute-start(bf16[32,2048]{1,0:T(8,128)(2,1)} %refs_0_.1), channel_id=1, source_target_pairs={{0,2},{1,3},{2,0},{3,1},{4,6},{5,7},{6,4},{7,5},{8,10},{9,11},{10,... | collective-permute-start | bytes 393224 | tf_op jit(solution)/shard_map/ppermute | solution.py:20
  3.0 3.7 %collective-permute-start.1 = (bf16[32,2048]{1,0:T(8,128)(2,1)}, bf16[32,2048]{1,0:T(8,128)(2,1)S(1)}, u32[]{:S(2)}, u32[]{:S(2)}) collective-permute-start(bf16[32,2048]{1,0:T(8,128)(2,1)} %refs_0_.1), channel_id=1, source_target_pairs={{0,1},{1,0},{2,3},{3,2},{4,5},{5,4},{6,7},{7,6},{8,9},{9,8},{10,11... | collective-permute-start | bytes 393224 | tf_op jit(solution)/shard_map/ppermute | solution.py:20
  6.7 1.3 %collective-permute-start.2 = (bf16[32,2048]{1,0:T(8,128)(2,1)S(1)}, bf16[32,2048]{1,0:T(8,128)(2,1)S(1)}, u32[]{:S(2)}, u32[]{:S(2)}) collective-permute-start(bf16[32,2048]{1,0:T(8,128)(2,1)S(1)} %collective-permute-done.t2), channel_id=1, source_target_pairs={{0,1},{1,0},{2,3},{3,2},{4,5},{5,4},{6,7},{7,6},{8,9},{9,8},{10,11... | collective-permute-start | bytes 393224 | tf_op jit(solution)/shard_map/ppermute | solution.py:20
  8.4 6.7 %collective-permute-start.9 = (bf16[136,256]{1,0:T(8,128)(2,1)S(1)}, bf16[136,256]{1,0:T(8,128)(2,1)S(1)}, u32[]{:S(2)}, u32[]{:S(2)}) collective-permute-start(bf16[136,256]{1,0:T(8,128)(2,1)S(1)} %get-tuple-element.37.pay.refs_1_), channel_id=1, source_target_pairs={{0,24},{4,28},{8,16},{12,20},{16,8},{20,12},{24,0},{28,4},{1,25},{... | collective-permute-start | bytes 208904 | tf_op jit(solution)/shard_map/ppermute | solution.py:20
  12.3 6.2 %collective-permute-start.8 = (bf16[136,256]{1,0:T(8,128)(2,1)S(1)}, bf16[136,256]{1,0:T(8,128)(2,1)S(1)}, u32[]{:S(2)}, u32[]{:S(2)}) collective-permute-start(bf16[136,256]{1,0:T(8,128)(2,1)S(1)} %get-tuple-element.37.pay.refs_1_), channel_id=1, source_target_pairs={{0,16},{4,20},{8,24},{12,28},{16,0},{20,4},{24,8},{28,12},{1,17},{... | collective-permute-start | bytes 208904 | tf_op jit(solution)/shard_map/ppermute | solution.py:20
  12.3 8.8 %collective-permute-start.11 = (bf16[136,256]{1,0:T(8,128)(2,1)S(1)}, bf16[136,256]{1,0:T(8,128)(2,1)S(1)}, u32[]{:S(2)}, u32[]{:S(2)}) collective-permute-start(bf16[136,256]{1,0:T(8,128)(2,1)S(1)} %get-tuple-element.37.pay.refs_1_), channel_id=1, source_target_pairs={{0,8},{4,12},{8,0},{12,4},{16,24},{20,28},{24,16},{28,20},{1,9},{5... | collective-permute-start | bytes 208904 | tf_op jit(solution)/shard_map/ppermute | solution.py:20
  18.5 10.7 %collective-permute-start.10 = (bf16[2,136,256]{2,1,0:T(8,128)(2,1)S(1)}, bf16[2,136,256]{2,1,0:T(8,128)(2,1)S(1)}, u32[]{:S(2)}, u32[]{:S(2)}) collective-permute-start(bf16[2,136,256]{2,1,0:T(8,128)(2,1)S(1)} %shard_map.122.refs_5_), channel_id=1, source_target_pairs={{0,4},{4,0},{8,12},{12,8},{16,20},{20,16},{24,28},{28,24},{1,5},{5... | collective-permute-start | bytes 417800 | tf_op jit(solution)/shard_map/ppermute | solution.py:20
  20.5 5.5 %collective-permute-start.4 = (bf16[152,256]{1,0:T(8,128)(2,1)S(1)}, bf16[152,256]{1,0:T(8,128)(2,1)S(1)}, u32[]{:S(2)}, u32[]{:S(2)}) collective-permute-start(bf16[152,256]{1,0:T(8,128)(2,1)S(1)} %get-tuple-element.39), channel_id=1, source_target_pairs={{0,4},{4,0},{8,12},{12,8},{16,20},{20,16},{24,28},{28,24},{1,5},{5... | collective-permute-start | bytes 233480 | tf_op jit(solution)/shard_map/ppermute | solution.py:20
  21.1 7.2 %collective-permute-start.12 = (bf16[136,256]{1,0:T(8,128)(2,1)S(1)}, bf16[136,256]{1,0:T(8,128)(2,1)S(1)}, u32[]{:S(2)}, u32[]{:S(2)}) collective-permute-start(bf16[136,256]{1,0:T(8,128)(2,1)S(1)} %collective-permute-done.11.refs_2_), channel_id=1, source_target_pairs={{0,4},{4,0},{8,12},{12,8},{16,20},{20,16},{24,28},{28,24},{1,5},{5... | collective-permute-start | bytes 208904 | tf_op jit(solution)/shard_map/ppermute | solution.py:20
  22.6 0.7 %collective-permute-start.3 = (bf16[32,128]{1,0:T(8,128)(2,1)S(1)}, bf16[32,128]{1,0:T(8,128)(2,1)S(1)}, u32[]{:S(2)}, u32[]{:S(2)}) collective-permute-start(bf16[32,128]{1,0:T(8,128)(2,1)S(1)} %get-tuple-element.38), channel_id=1, source_target_pairs={{4,8},{8,4},{12,16},{16,12},{20,24},{24,20},{5,9},{9,5},{13,17},{1... | collective-permute-start | bytes 24584 | tf_op jit(solution)/shard_map/ppermute | solution.py:377
  26.4 3.6 %collective-permute-start.7 = (f32[8,128]{1,0:T(8,128)S(1)}, f32[8,128]{1,0:T(8,128)S(1)}, u32[]{:S(2)}, u32[]{:S(2)}) collective-permute-start(f32[8,128]{1,0:T(8,128)S(1)} %get-tuple-element.43.own), channel_id=1, source_target_pairs={{0,3},{1,2},{2,1},{3,0},{4,7},{5,6},{6,5},{7,4},{8,11},{9,10},{10,... | collective-permute-start | bytes 12296 | tf_op jit(solution)/shard_map/ppermute | solution.py:20
  26.5 3.7 %collective-permute-start.6 = (f32[8,128]{1,0:T(8,128)S(1)}, f32[8,128]{1,0:T(8,128)S(1)}, u32[]{:S(2)}, u32[]{:S(2)}) collective-permute-start(f32[8,128]{1,0:T(8,128)S(1)} %get-tuple-element.43.own), channel_id=1, source_target_pairs={{0,2},{1,3},{2,0},{3,1},{4,6},{5,7},{6,4},{7,5},{8,10},{9,11},{10,... | collective-permute-start | bytes 12296 | tf_op jit(solution)/shard_map/ppermute | solution.py:20
  28.1 2.1 %collective-permute-start.5 = (f32[8,128]{1,0:T(8,128)S(1)}, f32[8,128]{1,0:T(8,128)S(1)}, u32[]{:S(2)}, u32[]{:S(2)}) collective-permute-start(f32[8,128]{1,0:T(8,128)S(1)} %get-tuple-element.43.own), channel_id=1, source_target_pairs={{0,1},{1,0},{2,3},{3,2},{4,5},{5,4},{6,7},{7,6},{8,9},{9,8},{10,11... | collective-permute-start | bytes 12296 | tf_op jit(solution)/shard_map/ppermute | solution.py:20
  30.7 1.6 %collective-permute-start.13 = (bf16[64,2048]{1,0:T(8,128)(2,1)S(1)}, bf16[64,2048]{1,0:T(8,128)(2,1)S(1)}, u32[]{:S(2)}, u32[]{:S(2)}) collective-permute-start(bf16[64,2048]{1,0:T(8,128)(2,1)S(1)} %get-tuple-element.51), channel_id=1, source_target_pairs={{0,1},{1,0},{2,3},{3,2},{4,5},{5,4},{6,7},{7,6},{8,9},{9,8},{10,11... | collective-permute-start | bytes 786440 | tf_op jit(solution)/shard_map/ppermute | solution.py:20
  32.3 5.8 %collective-permute-start.14 = (bf16[32,2048]{1,0:T(8,128)(2,1)S(1)}, bf16[32,2048]{1,0:T(8,128)(2,1)S(1)}, u32[]{:S(2)}, u32[]{:S(2)}) collective-permute-start(bf16[32,2048]{1,0:T(8,128)(2,1)S(1)} %add_convert_fusion.1), channel_id=1, source_target_pairs={{0,2},{1,3},{2,0},{3,1},{4,6},{5,7},{6,4},{7,5},{8,10},{9,11},{10,... | collective-permute-start | bytes 393224 | tf_op jit(solution)/shard_map/ppermute | solution.py:20
